TPU v7x, 512 devices: a 4x2x32 block of a 4x8x32 slice. The times are simulated.
512 devices in a mesh: grp: 2 (over y), kv: 32 (over z), tp: 8 (over x, core).
Axes of the slice: x: 4, y: 2, z: 32, core: 2. Of those that a mesh axis runs over, the one named last changes fastest.
The devices are a block of a 4x8x32 slice.
Arguments:
- tokens: bfloat16 [1536, 4096], P('grp', 'kv'), parts along dimension 0, may hold values from -40 to 40
- norm_gain: bfloat16 [4096], P('kv'), may hold values from 0.099609375 to 1.8984375
- w_query: bfloat16 [4096, 2048], P('kv', 'tp'), may hold values from -0.09375 to 0.09375
- w_key: bfloat16 [4096, 2048], P('kv', 'tp'), may hold values from -0.09375 to 0.09375
- w_value: bfloat16 [4096, 2048], P('kv', 'tp'), may hold values from -0.09375 to 0.09375
- w_gate: bfloat16 [4096, 2048], P('kv', 'tp'), may hold values from -0.09375 to 0.09375
- w_beta: bfloat16 [4096, 16], replicated, may hold values from -0.09375 to 0.09375
- w_decay: bfloat16 [4096, 16], replicated, may hold values from -0.09375 to 0.09375
- decay_rate: float32 [16], P('tp'), may hold values from 0.05 to 1.5
- out_gain: bfloat16 [128], replicated, may hold values from 0.099609375 to 1.8984375
- w_out: bfloat16 [2048, 4096], P('tp', 'kv'), may hold values from -0.125 to 0.125
- state: float32 [512, 16, 128, 128], P(('grp', 'kv'), 'tp'), parts along dimension 0, may hold values from -6 to 6
- prev_keys: bfloat16 [512, 3, 16, 128], P(('grp', 'kv'), None, 'tp'), parts along dimension 0, may hold values from -6 to 6
- prev_values: bfloat16 [512, 3, 16, 128], P(('grp', 'kv'), None, 'tp'), parts along dimension 0, may hold values from -6 to 6
- prev_beta: float32 [512, 3, 16], P(('grp', 'kv'), None, 'tp'), parts along dimension 0, may hold values from 0.2 to 1
- prev_logdecay: float32 [512, 3, 16], P(('grp', 'kv'), None, 'tp'), parts along dimension 0, may hold values from -1.5 to -0.05
- accepted: int32 [512], P(('grp', 'kv')), parts along dimension 0, may hold values from 0 to 3
Outputs:
- mixed: bfloat16 [1536, 4096], P('grp', 'kv'), parts along dimension 0
- new_state: float32 [512, 16, 128, 128], P(('grp', 'kv'), 'tp'), parts along dimension 0
There are 2 independent parts, one for each index of `grp`. A program takes and returns all parts, laid end to end along the dimension named above; an argument that names none is the same for every part. Nothing has to cross between parts.
All inputs are finite; a program needn't handle non-finite values.
Results may differ from a plain program's by a relative error of at most 0.0071.
Values may be sent and summed in bfloat16 or wider, within the bound.
No kernel may reach another device: no remote copies, remote signals or barrier semaphores. Data moves between devices by JAX's collectives and lax.ppermute only.
A program may use at most 64 MiB of HBM per device.

v0:
```python
import jax
import jax.numpy as jnp
from jax import lax
from jax.experimental import pallas as pl
from jax.experimental.pallas import tpu as pltpu
from jax.sharding import PartitionSpec as P


EPS = 1e-06
WINDOW = (-1, 0, 1, 2)
JUMP = len(WINDOW)
NEAR_OUT = 8
AHEAD = (0, JUMP, -JUMP, 2 * JUMP, -2 * JUMP, 3 * JUMP, -3 * JUMP, 4 * JUMP)
GATHER = "near"
LANES = 128
HALF = LANES // 2
F32 = jnp.float32
BF16 = jnp.bfloat16


def near_memory(array):
    return pltpu.with_memory_space_constraint(array, pltpu.MemorySpace.VMEM)


def kernel(body, scalars, arrays, shapes, scratch=(), in_near=True, out_near=True):
    smem = pl.BlockSpec(memory_space=pltpu.SMEM)
    vmem = pl.BlockSpec(memory_space=pltpu.VMEM)
    kind = pltpu.VMEM if out_near else jax.ShapeDtypeStruct
    return pl.pallas_call(
        body,
        in_specs=[smem] * len(scalars) + [vmem] * len(arrays),
        out_specs=[vmem] * len(shapes),
        out_shape=[kind(shape, dtype) for shape, dtype in shapes],
        scratch_shapes=list(scratch),
    )(*scalars, *[near_memory(array) if in_near else array for array in arrays])


def shift(table, axis_size, by):
    return lax.ppermute(table, "kv", [(i, (i + by) % axis_size) for i in range(axis_size)])


def replay_body(keys_ref, values_ref, beta_ref, logdecay_ref, accepted_ref, state_ref, out_ref):
    seq = pl.program_id(0)
    heads_here, depth = state_ref.shape[1], state_ref.shape[2]
    span_size = keys_ref.shape[1] // heads_here
    for head in range(heads_here):
        carry = state_ref[0, head]
        for position in range(span_size):
            row = position * heads_here + head
            active = accepted_ref[seq] > position
            spot = seq * span_size * heads_here + row
            logdecay = jnp.where(active, logdecay_ref[spot], F32(0.0))
            strength = jnp.where(active, beta_ref[spot], F32(0.0))
            factor = jnp.exp(jnp.full((1, depth), logdecay, F32))
            key = keys_ref[0, row : row + 1, :]
            key = key * lax.rsqrt(jnp.sum(key * key, axis=-1, keepdims=True) + EPS)
            key_columns = jnp.transpose(jnp.broadcast_to(key, (depth, depth)))
            carry = factor * carry
            predicted = jnp.sum(key_columns * carry, axis=0, keepdims=True)
            update = strength * (values_ref[0, row : row + 1, :] - predicted)
            carry = carry + key_columns * update
        out_ref[0, head] = carry


def replay(state, prev_keys, prev_values, prev_beta, prev_logdecay, accepted):
    seq_count, heads_here, depth, _ = state.shape
    rows = prev_keys.shape[1] * heads_here
    keys = prev_keys.astype(F32).reshape(seq_count, rows, depth)
    values = prev_values.astype(F32).reshape(seq_count, rows, depth)
    row_spec = pl.BlockSpec((1, rows, depth), lambda b: (b, 0, 0))
    state_spec = pl.BlockSpec((1, heads_here, depth, depth), lambda b: (b, 0, 0, 0))
    smem = pl.BlockSpec(memory_space=pltpu.SMEM)
    return pl.pallas_call(
        replay_body,
        grid=(seq_count,),
        in_specs=[row_spec, row_spec, smem, smem, smem, state_spec],
        out_specs=state_spec,
        out_shape=jax.ShapeDtypeStruct(state.shape, F32),
        name="replay",
    )(keys, values, prev_beta.reshape(-1), prev_logdecay.reshape(-1), accepted, state)


def rows_for(wide_ref, device, kv_size, own_rows):
    owners = [(device + ahead + 2 * kv_size) % kv_size for ahead in AHEAD]
    pieces = [wide_ref[pl.ds(pl.multiple_of(owner * own_rows, 8), own_rows), :] for owner in owners]
    return jnp.concatenate(pieces, axis=0)


def side_by_side(rows):
    half = rows.shape[0] // 2
    return jnp.concatenate([rows[:half], rows[half:]], axis=1).astype(BF16)


def layout(columns, own_rows):
    weights_at = 0 if GATHER == "near" else columns
    gain_at = weights_at + 4 * columns
    rows_at = gain_at + 16
    return weights_at, gain_at, rows_at, len(AHEAD) * own_rows // 2


def pack_body(
    kv_size, own_rows, tokens_ref, gain_ref, wq_ref, wk_ref, wv_ref, wg_ref, wo_ref, next_ref, previous_ref, own_ref, wide_ref
):
    columns = gain_ref.shape[1]
    weights_at, gain_at, rows_at, half = layout(columns, own_rows)
    shard_kv = lax.axis_index("kv")
    wide_ref[...] = tokens_ref[...].astype(F32)
    own_ref[...] = rows_for(wide_ref, shard_kv, kv_size, own_rows)
    gain = jnp.concatenate([gain_ref[...]] * (wq_ref.shape[1] // columns), axis=1)
    gain = jnp.broadcast_to(gain, (16, wq_ref.shape[1]))
    for out_ref, stops in ((next_ref, (1,)), (previous_ref, (-2, -1))):
        if GATHER != "near":
            out_ref[:columns, :columns] = wo_ref[:columns, :]
            out_ref[:columns, columns:] = wo_ref[columns:, :]
        for j, weight_ref in enumerate((wq_ref, wk_ref, wv_ref, wg_ref)):
            out_ref[weights_at + j * columns : weights_at + (j + 1) * columns, :] = weight_ref[...]
        out_ref[gain_at:rows_at, :] = gain
        for at, stop in enumerate(stops):
            rows = side_by_side(rows_for(wide_ref, shard_kv + stop, kv_size, own_rows))
            out_ref[rows_at + at * half : rows_at + (at + 1) * half, :] = rows


def pack(tokens, gain, weights, w_out, kv_size, own_rows):
    columns = tokens.shape[1]
    _, _, rows_at, half = layout(columns, own_rows)
    wide = weights[0].shape[1]

    def body(*refs):
        pack_body(kv_size, own_rows, *refs)

    shapes = [((rows_at + stops * half, wide), BF16) for stops in (1, 2)] + [((2 * half, columns), F32)]
    scratch = [pltpu.VMEM(tokens.shape, F32)]
    return kernel(body, [], [tokens, gain, *weights, w_out], shapes, scratch, in_near=False)


def split(values, wide):
    small = values[:, wide:]
    lane = lax.broadcasted_iota(jnp.int32, small.shape, 1)
    coarse = small.astype(BF16).astype(F32)
    rest = pltpu.roll(small - coarse, HALF, 1)
    return values[:, :wide].astype(BF16), jnp.where(lane < HALF, coarse, rest).astype(BF16)


def joined(terms, wide):
    small = terms[:, wide:].astype(F32)
    lane = lax.broadcasted_iota(jnp.int32, small.shape, 1)
    small = jnp.where(lane < HALF, small + pltpu.roll(small, HALF, 1), F32(0.0))
    return terms[:, :wide].astype(F32), small


def project_body(
    kv_size, own_rows, columns, own_rows_ref, small_ref, own_ref, before_ref, after_ref, after2_ref, up_ref, down_ref, across_ref, kept_ref, sums_ref
):
    wide = own_ref.shape[1]
    weights_at, gain_at, rows_at, half = layout(columns, own_rows)
    shard_kv = lax.axis_index("kv")

    def taken(pay_ref, at):
        weights = [pay_ref[weights_at + j * columns : weights_at + (j + 1) * columns, :] for j in range(4)]
        gain = pay_ref[gain_at:rows_at, :columns].astype(F32)[:1]
        if at is None:
            return own_rows_ref[...], gain, weights
        both = pay_ref[rows_at + at * half : rows_at + (at + 1) * half, :].astype(F32)
        return jnp.concatenate([both[:, :columns], both[:, columns:]], axis=0), gain, weights

    parts = [taken(before_ref, 0), taken(own_ref, None), taken(after_ref, 1), taken(after2_ref, 0)]
    sums = [None] * 4
    small = None
    squares = None
    for at, (widened, gain, weights) in enumerate(parts):
        term = jnp.sum(widened * widened, axis=1, keepdims=True)
        squares = term if squares is None else squares + term
        scaled = (widened * gain).astype(BF16)
        for j in range(4):
            term = jnp.dot(scaled, weights[j], preferred_element_type=F32)
            sums[j] = term if sums[j] is None else sums[j] + term
        small_at = pl.multiple_of((shard_kv + WINDOW[at] + kv_size) % kv_size * columns, columns)
        term = jnp.dot(scaled, small_ref[pl.ds(small_at, columns), :], preferred_element_type=F32)
        small = term if small is None else small + term
    lane = lax.broadcasted_iota(jnp.int32, small.shape, 1)
    small = jnp.where(lane == HALF - 1, squares, small)
    for j in range(4):
        sums_ref[:, j * wide : (j + 1) * wide] = sums[j]
    sums_ref[:, 4 * wide :] = small

    def block(ahead):
        start = AHEAD.index(ahead) * own_rows
        return sums_ref[start : start + own_rows, :]

    for out_ref, at, ahead in (
        (up_ref, 0, JUMP),
        (up_ref, 1, 3 * JUMP),
        (down_ref, 0, -JUMP),
        (down_ref, 1, -3 * JUMP),
        (across_ref, 0, 4 * JUMP),
    ):
        big, little = split(block(ahead), 4 * wide)
        out_ref[at, :, : 4 * wide] = big
        out_ref[at, :, 4 * wide :] = little
    for at, ahead in enumerate((0, 2 * JUMP, -2 * JUMP)):
        kept_ref[at] = block(ahead)


def project(own_rows_wide, small_weights, packets, kv_size, own_rows):
    columns = own_rows_wide.shape[1]
    across = 4 * packets[0].shape[1] + LANES
    shapes = [((count, own_rows, across), BF16) for count in (2, 2, 1)] + [((3, own_rows, across), F32)]

    def body(*refs):
        project_body(kv_size, own_rows, columns, *refs)

    scratch = [pltpu.VMEM((len(AHEAD) * own_rows, across), F32)]
    return kernel(body, [], [own_rows_wide, small_weights, *packets], shapes, scratch)


def combine_body(wide, kept_ref, up_ref, down_ref, across_ref, carried_ref, ahead_ref, behind_ref):
    del carried_ref
    for at, pieces, out_ref in ((1, (up_ref[1], across_ref[0]), ahead_ref), (2, (down_ref[1],), behind_ref)):
        big = kept_ref[at][:, :wide]
        small = kept_ref[at][:, wide:]
        for piece in pieces:
            more_big, more_small = joined(piece, wide)
            big = big + more_big
            small = small + more_small
        big, little = split(jnp.concatenate([big, small], axis=1), wide)
        out_ref[:, :wide] = big
        out_ref[:, wide:] = little


def combine(kept, up, down, across, carried):
    wide = kept.shape[2] - LANES

    def body(*refs):
        combine_body(wide, *refs)

    shapes = [(kept.shape[1:], BF16)] * 2
    return kernel(body, [], [kept, up, down, across, carried], shapes)


def deliver_body(*refs):
    *row_refs, wo_ref, before_ref, after_ref, after2_ref, out_ref = refs
    rows = jnp.concatenate([ref[...] for ref in row_refs], axis=0)
    columns = wo_ref.shape[1]
    for at, packet_ref in enumerate((before_ref, None, after_ref, after2_ref)):
        if packet_ref is None:
            weight = wo_ref[...]
        else:
            weight = jnp.concatenate([packet_ref[:columns, :columns], packet_ref[:columns, columns:]], axis=0)
        product = jnp.dot(rows, weight, preferred_element_type=F32)
        out_ref[:, at * columns : (at + 1) * columns] = product.astype(BF16)


def deliver(pieces, w_out, packets):
    shape = (sum(piece.shape[0] for piece in pieces), JUMP * w_out.shape[1])
    (partial,) = kernel(deliver_body, [], [*pieces, w_out, *packets], [(shape, BF16)])
    return partial


def deliver_near_body(kv_size, weight_ref, left_ref, three_ref, right_ref, out_ref):
    shard_kv = lax.axis_index("kv")
    own_rows = out_ref.shape[1]
    far_members = kv_size // NEAR_OUT
    pieces = [left_ref[0], left_ref[1], left_ref[2], three_ref[0], three_ref[1], three_ref[2], right_ref[0], right_ref[1]]
    for n, piece in enumerate(pieces):
        product = jnp.dot(piece, weight_ref[...], preferred_element_type=F32)
        for j in range(far_members):
            owner = (shard_kv + n - 4 + NEAR_OUT * (j - 2) + kv_size) % kv_size
            out_ref[owner] = product[j * own_rows : (j + 1) * own_rows].astype(BF16)


def deliver_near(w_out, left, three, right, kv_size, own_rows):
    def body(*refs):
        deliver_near_body(kv_size, *refs)

    shape = (kv_size, own_rows, w_out.shape[1])
    (partial,) = kernel(body, [], [w_out, left, three, right], [(shape, BF16)])
    return partial


def reduce_all_body(terms_ref, out_ref):
    total = terms_ref[0].astype(F32)
    for member in range(1, terms_ref.shape[0]):
        total = total + terms_ref[member].astype(F32)
    for member in range(terms_ref.shape[0]):
        out_ref[member] = total.astype(BF16)


def reduce_all(terms):
    (copies,) = kernel(reduce_all_body, [], [terms], [(terms.shape, BF16)])
    return copies


def stack_body(*refs):
    out_ref = refs[-1]
    for at, ref in enumerate(refs[:-1]):
        out_ref[at] = ref[...]


def stacked(pieces):
    (out,) = kernel(stack_body, [], pieces, [((len(pieces), *pieces[0].shape), BF16)])
    return out


def reduce_body(terms_ref, *out_refs):
    columns = out_refs[0].shape[1]
    for at, out_ref in enumerate(out_refs):
        total = terms_ref[0, :, at * columns : (at + 1) * columns].astype(F32)
        for member in range(1, terms_ref.shape[0]):
            total = total + terms_ref[member, :, at * columns : (at + 1) * columns].astype(F32)
        out_ref[...] = total.astype(BF16)


def reduce_terms(terms):
    _, rows, wide = terms.shape
    return kernel(reduce_body, [], [terms], [((rows, wide // JUMP), BF16)] * JUMP)


def spread_body(*refs):
    out_ref = refs[-1]
    for at, piece_ref in enumerate(refs[:-1]):
        for member in range(out_ref.shape[0]):
            out_ref[member, at] = piece_ref[...]


def spread(pieces, copies):
    (out,) = kernel(spread_body, [], pieces, [((copies, len(pieces), *pieces[0].shape), BF16)])
    return out


def settle_body(blocks_ref, out_ref):
    shard_kv = lax.axis_index("kv")
    kv_size = blocks_ref.shape[0]
    for n in range(kv_size):
        if GATHER == "exchange":
            owner = (shard_kv + n % JUMP + JUMP - WINDOW[-1]) % JUMP + n // JUMP * JUMP
        else:
            owner = (shard_kv + n + 2 * kv_size - WINDOW[-1] - 3 * JUMP) % kv_size
        out_ref[owner] = blocks_ref[n]


def settle(blocks):
    (out,) = kernel(settle_body, [], [blocks], [(blocks.shape, BF16)], out_near=False)
    return out


def propose_body(
    span_size, total_heads, model_width, rate_ref, gain_ref, kept_ref, up_ref, down_ref, ahead_ref, behind_ref, state_ref, out_ref
):
    rows = kept_ref.shape[1]
    seq_count, heads_here, depth = state_ref.shape[0], state_ref.shape[1], state_ref.shape[2]
    wide = heads_here * depth

    def total(at, size):
        summed = kept_ref[0, :, at : at + size]
        for piece in (up_ref[0], down_ref[0], ahead_ref[...], behind_ref[...]):
            summed = summed + piece[:, at : at + size].astype(F32)
        return summed

    small = total(4 * wide, LANES)
    small = small + pltpu.roll(small, HALF, 1)
    lane = lax.broadcasted_iota(jnp.int32, small.shape, 1)

    def column(at):
        return jnp.sum(jnp.where(lane == at, small, F32(0.0)), axis=1, keepdims=True)

    inverse = lax.rsqrt(column(HALF - 1) / model_width + EPS)
    row = lax.broadcasted_iota(jnp.int32, (rows, 1), 0)
    place = row % span_size
    out_gain = gain_ref[...].astype(F32)

    def back(values, by):
        moved = pltpu.roll(values, by, 0)
        return jnp.where(place >= by, moved, F32(0.0))

    def dots(left, right):
        return jnp.sum(left * right, axis=1, keepdims=True)

    def unit(vectors):
        return vectors * lax.rsqrt(dots(vectors, vectors) + EPS)

    def over_lanes(values):
        return jnp.broadcast_to(values, (rows, depth))

    for head in range(heads_here):
        first = head * depth
        queries = unit(total(first, depth) * inverse) * F32(depth ** (-0.5))
        keys = unit(total(wide + first, depth) * inverse)
        values = total(2 * wide + first, depth) * inverse
        gate = total(3 * wide + first, depth) * inverse
        head_at = lax.axis_index("tp") * heads_here + head
        beta = over_lanes(jax.nn.sigmoid(column(head_at) * inverse))
        logit = over_lanes(column(total_heads + head_at) * inverse)
        softplus = jnp.maximum(logit, F32(0.0)) + jnp.log1p(jnp.exp(-jnp.abs(logit)))
        log_decay = -rate_ref[head] * softplus
        cumulative = log_decay
        for by in range(1, span_size):
            cumulative = cumulative + back(log_decay, by)
        grown = jnp.exp(cumulative)
        moved_keys = [keys] + [back(keys, by) for by in range(1, span_size)]
        within = [None] + [
            jnp.where(place >= by, jnp.exp(jnp.where(place >= by, cumulative - back(cumulative, by), F32(0.0))), F32(0.0))
            for by in range(1, span_size)
        ]
        lower = [None] + [beta * dots(keys, moved_keys[by]) * within[by] for by in range(1, span_size)]
        pushed = beta * values
        weighted = beta * grown * keys
        for step in range(1, span_size):
            at_step = place == step
            push_less = jnp.zeros_like(pushed)
            weight_less = jnp.zeros_like(weighted)
            for by in range(1, step + 1):
                push_less = push_less + lower[by] * back(pushed, by)
                weight_less = weight_less + lower[by] * back(weighted, by)
            pushed = pushed - jnp.where(at_step, push_less, F32(0.0))
            weighted = weighted - jnp.where(at_step, weight_less, F32(0.0))
        left = jnp.concatenate([weighted, queries * grown], axis=0)
        sequence = lax.broadcasted_iota(jnp.int32, (2 * rows, 1), 0) % rows // span_size
        read = jnp.zeros((2 * rows, depth), F32)
        for seq in range(seq_count):
            term = jnp.dot(left, state_ref[seq, head], precision=lax.Precision.HIGHEST, preferred_element_type=F32)
            read = jnp.where(sequence == seq, term, read)
        corrections = pushed - read[:rows]
        outputs = read[rows:] + dots(queries, keys) * corrections
        for by in range(1, span_size):
            outputs = outputs + dots(queries, moved_keys[by]) * within[by] * back(corrections, by)
        scale = lax.rsqrt(dots(outputs, outputs) / depth + EPS)
        finished = (outputs * scale * out_gain * (gate * jax.nn.sigmoid(gate))).astype(BF16)
        for copy in range(out_ref.shape[0] // rows):
            out_ref[copy * rows : (copy + 1) * rows, first : first + depth] = finished


def propose(decay_rate, out_gain, terms, carried, span_size, total_heads, model_width, copies):
    def body(*refs):
        propose_body(span_size, total_heads, model_width, *refs)

    wide = carried.shape[1] * carried.shape[2]
    shape = (copies * terms[0].shape[1], wide)
    operands = [out_gain.reshape(1, -1), *terms, carried]
    (hidden,) = kernel(body, [decay_rate], operands, [(shape, BF16)])
    return hidden


def shards(
    tokens,
    norm_gain,
    w_query,
    w_key,
    w_value,
    w_gate,
    w_beta,
    w_decay,
    decay_rate,
    out_gain,
    w_out,
    state,
    prev_keys,
    prev_values,
    prev_beta,
    prev_logdecay,
    accepted,
    kv_size,
    tp_size,
):
    seq_count = state.shape[0]
    span_size = prev_keys.shape[1]
    own_rows = seq_count * span_size
    model_width, total_heads = w_beta.shape
    weights = [w_query, w_key, w_value, w_gate]
    to_next, to_previous, own_rows_wide = pack(tokens, norm_gain[None, :], weights, w_out, kv_size, own_rows)
    before = shift(to_next, kv_size, 1)
    after = shift(to_previous, kv_size, -1)
    after2 = shift(after[: to_next.shape[0]], kv_size, -1)

    carried = replay(state, prev_keys, prev_values, prev_beta, prev_logdecay, accepted)
    small_weights = jnp.concatenate(
        [w_beta, w_decay, jnp.zeros((model_width, LANES - 2 * total_heads), w_beta.dtype)], axis=1
    )
    packets = (to_next, before, after, after2)
    up, down, across, kept = project(own_rows_wide, small_weights, packets, kv_size, own_rows)
    across = shift(across, kv_size, 2 * JUMP)
    up = shift(up, kv_size, JUMP)
    down = shift(down, kv_size, -JUMP)
    ahead, behind = combine(kept, up, down, across, carried)
    ahead = shift(ahead, kv_size, 2 * JUMP)
    behind = shift(behind, kv_size, -2 * JUMP)
    terms = (kept, up, down, ahead, behind)
    members = kv_size // JUMP
    copies = members if GATHER == "exchange" else 1
    hidden = propose(decay_rate, out_gain, terms, carried, span_size, total_heads, model_width, copies)

    if GATHER == "near":
        below = shift(hidden, kv_size, NEAR_OUT)
        above = shift(hidden, kv_size, -NEAR_OUT)
        opposite = shift(below, kv_size, NEAR_OUT)
        block = stacked([opposite, below, hidden, above]).reshape(4 * own_rows, -1)
        left = shift(block, kv_size, 1)
        right = shift(block, kv_size, -1)
        three = stacked([left, block, right])
        near_left = shift(three, kv_size, 3)
        near_right = shift(three[:2], kv_size, -3)
        partial = deliver_near(w_out, near_left, three, near_right, kv_size, own_rows)
        exchanged = lax.all_to_all(partial.reshape(kv_size * own_rows, -1), "tp", 0, 0, tiled=True)
        copies = reduce_all(exchanged.reshape(tp_size, -1, exchanged.shape[1]))
        mixed = lax.all_to_all(copies.reshape(exchanged.shape), "tp", 0, 0, tiled=True)
        return (mixed, carried)
    if GATHER == "exchange":
        groups = [list(range(first, kv_size, JUMP)) for first in range(JUMP)]
        pieces = (lax.all_to_all(hidden, "kv", 0, 0, tiled=True, axis_index_groups=groups),)
    else:
        below = shift(hidden, kv_size, JUMP)
        above = shift(hidden, kv_size, -JUMP)
        three = jnp.concatenate([below, hidden, above], axis=0)
        low = shift(three[own_rows:], kv_size, 3 * JUMP)
        high = shift(three, kv_size, -3 * JUMP)
        pieces = (low, three, high)
    partial = deliver(pieces, w_out, (before, after, after2))
    exchanged = lax.all_to_all(partial, "tp", 0, 0, tiled=True)
    finished = reduce_terms(exchanged.reshape(tp_size, own_rows, -1))
    landed = [
        piece if offset == 0 else shift(piece, kv_size, offset) for offset, piece in zip(WINDOW, finished)
    ][::-1]
    copies = spread(landed, tp_size).reshape(kv_size * own_rows, -1)
    mixed = lax.all_to_all(copies, "tp", 0, 0, tiled=True)
    mixed = settle(mixed.reshape(kv_size, own_rows, -1)).reshape(kv_size * own_rows, -1)
    return (mixed, carried)


def solution(mesh):
    in_specs = (
        P("grp", "kv"),
        P("kv"),
        P("kv", "tp"),
        P("kv", "tp"),
        P("kv", "tp"),
        P("kv", "tp"),
        P(),
        P(),
        P("tp"),
        P(),
        P("tp", "kv"),
        P(("grp", "kv"), "tp", None, None),
        P(("grp", "kv"), None, "tp", None),
        P(("grp", "kv"), None, "tp", None),
        P(("grp", "kv"), None, "tp"),
        P(("grp", "kv"), None, "tp"),
        P(("grp", "kv")),
    )
    out_specs = (P("grp", "kv"), P(("grp", "kv"), "tp", None, None))

    def per_device(*arguments):
        return shards(*arguments, kv_size=mesh.shape["kv"], tp_size=mesh.shape["tp"])

    return jax.shard_map(per_device, mesh=mesh, in_specs=in_specs, out_specs=out_specs, check_vma=False)
```

profile of v0, /device:TPU:40, one launch (start us, length us, event | category | flops | bytes accessed | tf_op | source)
XLA Modules:
  0.0 193.5 jit_solution(9275515190294160222)
XLA Ops:
  0.6 1.2 shard_map.176
  1.9 45.3 %collective-permute-start.1 = (bf16[720,256]{1,0:T(8,128)(2,1)S(1)}, bf16[720,256]{1,0:T(8,128)(2,1)S(1)}, u32[]{:S(2)}, u32[]{:S(2)}) collective-permute-start(bf16[720,256]{1,0:T(8,128)(2,1)S(1)} %get-tuple-element.13), channel_id=1, source_target_pairs={{0,248},{8,0},{16,8},{24,16},{32,24},{40,32},{48,40},{56,48},{64,5... | collective-permute-start | bytes 1105928 | tf_op jit(solution)/shard_map/ppermute | solution.py:39
  47.2 2.0 %collective-permute-start = (bf16[624,256]{1,0:T(8,128)(2,1)S(1)}, bf16[624,256]{1,0:T(8,128)(2,1)S(1)}, u32[]{:S(2)}, u32[]{:S(2)}) collective-permute-start(bf16[624,256]{1,0:T(8,128)(2,1)S(1)} %get-tuple-element.12.refs_2_), channel_id=1, source_target_pairs={{0,8},{8,16},{16,24},{24,32},{32,40},{40,48},{48,56},{56,64},{64,7... | collective-permute-start | bytes 958472 | tf_op jit(solution)/shard_map/ppermute | solution.py:39
  49.2 2.2 %copy.24 = bf16[4096,16]{1,0:T(8,128)(2,1)} copy(bf16[4096,16]{0,1:T(8,128)(2,1)} %param.24) | data formatting | bytes 262144 | tf_op args[7]
  51.4 1.3 copy.23
  52.8 2.3 %collective-permute-done.1.refs_4_ = bf16[720,256]{1,0:T(8,128)(2,1)S(1)} collective-permute-done((bf16[720,256]{1,0:T(8,128)(2,1)S(1)}, bf16[720,256]{1,0:T(8,128)(2,1)S(1)}, u32[]{:S(2)}, u32[]{:S(2)}) %collective-permute-start.1) | collective-permute-done | bytes 368672 | tf_op jit(solution)/shard_map/ppermute | solution.py:39
  55.2 5.6 %collective-permute-start.2 = (bf16[624,256]{1,0:T(8,128)(2,1)S(1)}, bf16[624,256]{1,0:T(8,128)(2,1)S(1)}, u32[]{:S(2)}, u32[]{:S(2)}) collective-permute-start(bf16[624,256]{1,0:T(8,128)(2,1)S(1)} %slice.8), channel_id=1, source_target_pairs={{0,248},{8,0},{16,8},{24,16},{32,24},{40,32},{48,40},{56,48},{64,5... | collective-permute-start | bytes 958472 | tf_op jit(solution)/shard_map/ppermute | solution.py:39
  60.8 2.2 %maximum_maximum_fusion.refs_1_ = bf16[4096,128]{1,0:T(8,128)(2,1)S(1)} fusion(bf16[4096,16]{1,0:T(8,128)(2,1)} %copy.24, bf16[4096,16]{1,0:T(8,128)(2,1)} %copy.23, bf16[128]{0:T(256)(128)(2,1)S(1)} %pad.2.clone), kind=kLoop, calls=%fused_computation | loop fusion | flops 3145728 | bytes 1310976 | tf_op jit(solution)/shard_map/concatenate | solution.py:475
  63.1 3.7 %collective-permute-done.2.refs_5_ = bf16[624,256]{1,0:T(8,128)(2,1)S(1)} collective-permute-done((bf16[624,256]{1,0:T(8,128)(2,1)S(1)}, bf16[624,256]{1,0:T(8,128)(2,1)S(1)}, u32[]{:S(2)}, u32[]{:S(2)}) %collective-permute-start.2) | collective-permute-done | bytes 319520 | tf_op jit(solution)/shard_map/ppermute | solution.py:39
  67.5 1.9 %collective-permute-start.3 = (bf16[2,24,1152]{2,1,0:T(8,128)(2,1)S(1)}, bf16[2,24,1152]{2,1,0:T(8,128)(2,1)S(1)}, u32[]{:S(2)}, u32[]{:S(2)}) collective-permute-start(bf16[2,24,1152]{2,1,0:T(8,128)(2,1)S(1)} %get-tuple-element.15), channel_id=1, source_target_pairs={{0,32},{8,40},{16,48},{24,56},{32,64},{40,72},{48,80},{56,88},{64,... | collective-permute-start | bytes 331784 | tf_op jit(solution)/shard_map/ppermute | solution.py:39
  69.4 7.9 %collective-permute-start.4 = (bf16[2,24,1152]{2,1,0:T(8,128)(2,1)S(1)}, bf16[2,24,1152]{2,1,0:T(8,128)(2,1)S(1)}, u32[]{:S(2)}, u32[]{:S(2)}) collective-permute-start(bf16[2,24,1152]{2,1,0:T(8,128)(2,1)S(1)} %get-tuple-element.16), channel_id=1, source_target_pairs={{0,224},{8,232},{16,240},{24,248},{32,0},{40,8},{48,16},{56,24},{6... | collective-permute-start | bytes 331784 | tf_op jit(solution)/shard_map/ppermute | solution.py:39
  77.3 2.0 %collective-permute-start.5 = (bf16[1,24,1152]{2,1,0:T(8,128)(2,1)S(1)}, bf16[1,24,1152]{2,1,0:T(8,128)(2,1)S(1)}, u32[]{:S(2)}, u32[]{:S(2)}) collective-permute-start(bf16[1,24,1152]{2,1,0:T(8,128)(2,1)S(1)} %get-tuple-element.17), channel_id=1, source_target_pairs={{0,64},{8,72},{16,80},{24,88},{32,96},{40,104},{48,112},{56,120},{... | collective-permute-start | bytes 165896 | tf_op jit(solution)/shard_map/ppermute | solution.py:39
  82.1 6.4 %replay.1.refs_4_.refs_7_ = f32[8,2,128,128]{3,2,1,0:T(8,128)} custom-call(f32[8,6,128]{2,1,0:T(8,128)} %copy.29.keys_ref, f32[8,6,128]{2,1,0:T(8,128)} %copy.30.values_ref, f32[48]{0:T(128)} %reshape.41.beta_ref, f32[48]{0:T(128)} %reshape.42.logdecay_ref, s32[8]{0:T(128)} %accepted_ref.1, f32[8,2,128,128]{3,2,1,0:T(8,128)} %state_ref.1), custom_call_target="tpu_custom_call" | custom-call | tf_op jit(solution)/shard_map/replay/pallas_call | solution.py:73
  88.5 9.9 %collective-permute-done.5.refs_3_ = bf16[1,24,1152]{2,1,0:T(8,128)(2,1)S(1)} collective-permute-done((bf16[1,24,1152]{2,1,0:T(8,128)(2,1)S(1)}, bf16[1,24,1152]{2,1,0:T(8,128)(2,1)S(1)}, u32[]{:S(2)}, u32[]{:S(2)}) %collective-permute-start.5) | collective-permute-done | bytes 55328 | tf_op jit(solution)/shard_map/ppermute | solution.py:39
  98.4 1.2 copy-done
  99.8 1.9 %collective-permute-start.6 = (bf16[24,1152]{1,0:T(8,128)(2,1)S(1)}, bf16[24,1152]{1,0:T(8,128)(2,1)S(1)}, u32[]{:S(2)}, u32[]{:S(2)}) collective-permute-start(bf16[24,1152]{1,0:T(8,128)(2,1)S(1)} %get-tuple-element.18), channel_id=1, source_target_pairs={{0,64},{8,72},{16,80},{24,88},{32,96},{40,104},{48,112},{56,120},{... | collective-permute-start | bytes 165896 | tf_op jit(solution)/shard_map/ppermute | solution.py:39
  101.8 12.7 %collective-permute-start.7 = (bf16[24,1152]{1,0:T(8,128)(2,1)S(1)}, bf16[24,1152]{1,0:T(8,128)(2,1)S(1)}, u32[]{:S(2)}, u32[]{:S(2)}) collective-permute-start(bf16[24,1152]{1,0:T(8,128)(2,1)S(1)} %get-tuple-element.19), channel_id=1, source_target_pairs={{0,192},{8,200},{16,208},{24,216},{32,224},{40,232},{48,240},{56,2... | collective-permute-start | bytes 165896 | tf_op jit(solution)/shard_map/ppermute | solution.py:39
  114.5 1.4 collective-permute-done.6.refs_5_
  115.9 1.1 collective-permute-done.7.refs_6_
  117.0 2.2 %shard_map.179.refs_2_ = bf16[24,256]{1,0:T(8,128)(2,1)S(1)} custom-call(f32[2]{0:T(128)} %refs_0_.4, bf16[1,128]{1,0:T(2,128)(2,1)S(1)} %bitcast.15, f32[3,24,1152]{2,1,0:T(8,128)S(1)} %get-tuple-element.14.refs_0_.refs_2_, bf16[2,24,1152]{2,1,0:T(8,128)(2,1)S(1)} %collective-permute-done.3.refs_1_.refs_3_, ...), custom_call_target="tpu_custom_call" | custom-call | tf_op jit(solution)/shard_map/pallas_call | solution.py:29
  119.2 3.0 %collective-permute-start.8 = (bf16[24,256]{1,0:T(8,128)(2,1)S(1)}, bf16[24,256]{1,0:T(8,128)(2,1)S(1)}, u32[]{:S(2)}, u32[]{:S(2)}) collective-permute-start(bf16[24,256]{1,0:T(8,128)(2,1)S(1)} %shard_map.179.refs_2_), channel_id=1, source_target_pairs={{0,64},{8,72},{16,80},{24,88},{32,96},{40,104},{48,112},{56,120},{... | collective-permute-start | bytes 36872 | tf_op jit(solution)/shard_map/ppermute | solution.py:39
  122.2 11.7 %collective-permute-start.10 = (bf16[24,256]{1,0:T(8,128)(2,1)S(1)}, bf16[24,256]{1,0:T(8,128)(2,1)S(1)}, u32[]{:S(2)}, u32[]{:S(2)}) collective-permute-start(bf16[24,256]{1,0:T(8,128)(2,1)S(1)} %shard_map.179.refs_2_), channel_id=1, source_target_pairs={{0,192},{8,200},{16,208},{24,216},{32,224},{40,232},{48,240},{56,2... | collective-permute-start | bytes 36872 | tf_op jit(solution)/shard_map/ppermute | solution.py:39
  133.8 5.1 %collective-permute-start.9 = (bf16[24,256]{1,0:T(8,128)(2,1)S(1)}, bf16[24,256]{1,0:T(8,128)(2,1)S(1)}, u32[]{:S(2)}, u32[]{:S(2)}) collective-permute-start(bf16[24,256]{1,0:T(8,128)(2,1)S(1)} %collective-permute-done.8.refs_1_), channel_id=1, source_target_pairs={{0,64},{8,72},{16,80},{24,88},{32,96},{40,104},{48,112},{56,120},{... | collective-permute-start | bytes 36872 | tf_op jit(solution)/shard_map/ppermute | solution.py:39
  139.0 9.3 %collective-permute-done.9.refs_0_ = bf16[24,256]{1,0:T(8,128)(2,1)S(1)} collective-permute-done((bf16[24,256]{1,0:T(8,128)(2,1)S(1)}, bf16[24,256]{1,0:T(8,128)(2,1)S(1)}, u32[]{:S(2)}, u32[]{:S(2)}) %collective-permute-start.9) | collective-permute-done | bytes 12320 | tf_op jit(solution)/shard_map/ppermute | solution.py:39
  148.3 1.9 %collective-permute-start.11 = (bf16[96,256]{1,0:T(8,128)(2,1)S(1)}, bf16[96,256]{1,0:T(8,128)(2,1)S(1)}, u32[]{:S(2)}, u32[]{:S(2)}) collective-permute-start(bf16[96,256]{1,0:T(8,128)(2,1)S(1)} %bitcast.12), channel_id=1, source_target_pairs={{0,8},{8,16},{16,24},{24,32},{32,40},{40,48},{48,56},{56,64},{64,7... | collective-permute-start | bytes 147464 | tf_op jit(solution)/shard_map/ppermute | solution.py:39
  150.3 5.8 %collective-permute-start.12 = (bf16[96,256]{1,0:T(8,128)(2,1)S(1)}, bf16[96,256]{1,0:T(8,128)(2,1)S(1)}, u32[]{:S(2)}, u32[]{:S(2)}) collective-permute-start(bf16[96,256]{1,0:T(8,128)(2,1)S(1)} %bitcast.13), channel_id=1, source_target_pairs={{0,248},{8,0},{16,8},{24,16},{32,24},{40,32},{48,40},{56,48},{64,5... | collective-permute-start | bytes 147464 | tf_op jit(solution)/shard_map/ppermute | solution.py:39
  156.2 1.6 collective-permute-done.12.refs_2_
  157.9 3.7 %collective-permute-start.13 = (bf16[3,96,256]{2,1,0:T(8,128)(2,1)S(1)}, bf16[3,96,256]{2,1,0:T(8,128)(2,1)S(1)}, u32[]{:S(2)}, u32[]{:S(2)}) collective-permute-start(bf16[3,96,256]{2,1,0:T(8,128)(2,1)S(1)} %shard_map.181.refs_2_), channel_id=1, source_target_pairs={{0,24},{8,32},{16,40},{24,48},{32,56},{40,64},{48,72},{56,80},{64,... | collective-permute-start | bytes 442376 | tf_op jit(solution)/shard_map/ppermute | solution.py:39
  161.6 5.2 %collective-permute-start.14 = (bf16[2,96,256]{2,1,0:T(8,128)(2,1)S(1)}, bf16[2,96,256]{2,1,0:T(8,128)(2,1)S(1)}, u32[]{:S(2)}, u32[]{:S(2)}) collective-permute-start(bf16[2,96,256]{2,1,0:T(8,128)(2,1)S(1)} %slice.9), channel_id=1, source_target_pairs={{0,232},{8,240},{16,248},{24,0},{32,8},{40,16},{48,24},{56,32},{64... | collective-permute-start | bytes 294920 | tf_op jit(solution)/shard_map/ppermute | solution.py:39
  166.8 5.3 %collective-permute-done.14.refs_3_ = bf16[2,96,256]{2,1,0:T(8,128)(2,1)S(1)} collective-permute-done((bf16[2,96,256]{2,1,0:T(8,128)(2,1)S(1)}, bf16[2,96,256]{2,1,0:T(8,128)(2,1)S(1)}, u32[]{:S(2)}, u32[]{:S(2)}) %collective-permute-start.14) | collective-permute-done | bytes 98336 | tf_op jit(solution)/shard_map/ppermute | solution.py:39
  172.3 11.2 %all_to_all.18.terms_ref = bf16[8,96,128]{2,1,0:T(8,128)(2,1)S(1)} all-to-all(bf16[8,96,128]{2,1,0:T(8,128)(2,1)S(1)} %bitcast.11), channel_id=1, replica_groups=mesh['grp'=2,'kv'=32,'tp'=8] {'tp'}, dimensions={0} | all-to-all | bytes 393216 | tf_op jit(solution)/shard_map/all_to_all | solution.py:502
  183.6 9.3 %all_to_all.19 = bf16[8,96,128]{2,1,0:T(8,128)(2,1)S(1)} all-to-all(bf16[8,96,128]{2,1,0:T(8,128)(2,1)S(1)} %shard_map.183), channel_id=1, replica_groups=mesh['grp'=2,'kv'=32,'tp'=8] {'tp'}, dimensions={0} | all-to-all | bytes 393216 | tf_op jit(solution)/shard_map/all_to_all | solution.py:504
  (43 shorter events, 4.9 us)
Async XLA Ops:
  0.6 50.8 %copy-start.3 = (bf16[4096,16]{0,1:T(8,128)(2,1)S(1)}, bf16[4096,16]{0,1:T(8,128)(2,1)}, u32[]{:S(2)}) copy-start(bf16[4096,16]{0,1:T(8,128)(2,1)} %param.23) | copy-start | bytes 393220
  1.9 53.2 %collective-permute-start.1 = (bf16[720,256]{1,0:T(8,128)(2,1)S(1)}, bf16[720,256]{1,0:T(8,128)(2,1)S(1)}, u32[]{:S(2)}, u32[]{:S(2)}) collective-permute-start(bf16[720,256]{1,0:T(8,128)(2,1)S(1)} %get-tuple-element.13), channel_id=1, source_target_pairs={{0,248},{8,0},{16,8},{24,16},{32,24},{40,32},{48,40},{56,48},{64,5... | collective-permute-start | bytes 1105928 | tf_op jit(solution)/shard_map/ppermute | solution.py:39
  47.2 15.8 %collective-permute-start = (bf16[624,256]{1,0:T(8,128)(2,1)S(1)}, bf16[624,256]{1,0:T(8,128)(2,1)S(1)}, u32[]{:S(2)}, u32[]{:S(2)}) collective-permute-start(bf16[624,256]{1,0:T(8,128)(2,1)S(1)} %get-tuple-element.12.refs_2_), channel_id=1, source_target_pairs={{0,8},{8,16},{16,24},{24,32},{32,40},{40,48},{48,56},{56,64},{64,7... | collective-permute-start | bytes 958472 | tf_op jit(solution)/shard_map/ppermute | solution.py:39
  55.1 7.9 %copy-start.4 = (bf16[8,3,2,128]{3,2,1,0:T(2,128)(2,1)S(1)}, bf16[8,3,2,128]{3,2,1,0:T(2,128)(2,1)}, u32[]{:S(2)}) copy-start(bf16[8,3,2,128]{3,2,1,0:T(2,128)(2,1)} %param.29) | copy-start | bytes 36868
  55.1 7.9 %copy-start.5 = (bf16[8,3,2,128]{3,2,1,0:T(2,128)(2,1)S(1)}, bf16[8,3,2,128]{3,2,1,0:T(2,128)(2,1)}, u32[]{:S(2)}) copy-start(bf16[8,3,2,128]{3,2,1,0:T(2,128)(2,1)} %param.30) | copy-start | bytes 36868
  55.2 11.6 %collective-permute-start.2 = (bf16[624,256]{1,0:T(8,128)(2,1)S(1)}, bf16[624,256]{1,0:T(8,128)(2,1)S(1)}, u32[]{:S(2)}, u32[]{:S(2)}) collective-permute-start(bf16[624,256]{1,0:T(8,128)(2,1)S(1)} %slice.8), channel_id=1, source_target_pairs={{0,248},{8,0},{16,8},{24,16},{32,24},{40,32},{48,40},{56,48},{64,5... | collective-permute-start | bytes 958472 | tf_op jit(solution)/shard_map/ppermute | solution.py:39
  66.8 13.7 %copy-start.6 = (f32[8,3,2]{0,2,1:T(2,128)S(1)}, f32[8,3,2]{0,2,1:T(2,128)}, u32[]{:S(2)}) copy-start(f32[8,3,2]{0,2,1:T(2,128)} %param.31) | copy-start | bytes 580
  66.8 14.5 %copy-start.7 = (f32[8,3,2]{0,2,1:T(2,128)S(1)}, f32[8,3,2]{0,2,1:T(2,128)}, u32[]{:S(2)}) copy-start(f32[8,3,2]{0,2,1:T(2,128)} %param.32) | copy-start | bytes 580
  67.5 31.0 %collective-permute-start.3 = (bf16[2,24,1152]{2,1,0:T(8,128)(2,1)S(1)}, bf16[2,24,1152]{2,1,0:T(8,128)(2,1)S(1)}, u32[]{:S(2)}, u32[]{:S(2)}) collective-permute-start(bf16[2,24,1152]{2,1,0:T(8,128)(2,1)S(1)} %get-tuple-element.15), channel_id=1, source_target_pairs={{0,32},{8,40},{16,48},{24,56},{32,64},{40,72},{48,80},{56,88},{64,... | collective-permute-start | bytes 331784 | tf_op jit(solution)/shard_map/ppermute | solution.py:39
  69.4 29.0 %collective-permute-start.4 = (bf16[2,24,1152]{2,1,0:T(8,128)(2,1)S(1)}, bf16[2,24,1152]{2,1,0:T(8,128)(2,1)S(1)}, u32[]{:S(2)}, u32[]{:S(2)}) collective-permute-start(bf16[2,24,1152]{2,1,0:T(8,128)(2,1)S(1)} %get-tuple-element.16), channel_id=1, source_target_pairs={{0,224},{8,232},{16,240},{24,248},{32,0},{40,8},{48,16},{56,24},{6... | collective-permute-start | bytes 331784 | tf_op jit(solution)/shard_map/ppermute | solution.py:39
  77.3 21.1 %collective-permute-start.5 = (bf16[1,24,1152]{2,1,0:T(8,128)(2,1)S(1)}, bf16[1,24,1152]{2,1,0:T(8,128)(2,1)S(1)}, u32[]{:S(2)}, u32[]{:S(2)}) collective-permute-start(bf16[1,24,1152]{2,1,0:T(8,128)(2,1)S(1)} %get-tuple-element.17), channel_id=1, source_target_pairs={{0,64},{8,72},{16,80},{24,88},{32,96},{40,104},{48,112},{56,120},{... | collective-permute-start | bytes 165896 | tf_op jit(solution)/shard_map/ppermute | solution.py:39
  88.5 28.5 %copy-start.2 = (bf16[128]{0:T(256)(128)(2,1)S(1)}, bf16[128]{0:T(256)(128)(2,1)}, u32[]{:S(2)}) copy-start(bf16[128]{0:T(256)(128)(2,1)} %param.26) | copy-start | bytes 772
  98.4 1.2 copy-start
  99.8 16.0 %collective-permute-start.6 = (bf16[24,1152]{1,0:T(8,128)(2,1)S(1)}, bf16[24,1152]{1,0:T(8,128)(2,1)S(1)}, u32[]{:S(2)}, u32[]{:S(2)}) collective-permute-start(bf16[24,1152]{1,0:T(8,128)(2,1)S(1)} %get-tuple-element.18), channel_id=1, source_target_pairs={{0,64},{8,72},{16,80},{24,88},{32,96},{40,104},{48,112},{56,120},{... | collective-permute-start | bytes 165896 | tf_op jit(solution)/shard_map/ppermute | solution.py:39
  101.8 15.2 %collective-permute-start.7 = (bf16[24,1152]{1,0:T(8,128)(2,1)S(1)}, bf16[24,1152]{1,0:T(8,128)(2,1)S(1)}, u32[]{:S(2)}, u32[]{:S(2)}) collective-permute-start(bf16[24,1152]{1,0:T(8,128)(2,1)S(1)} %get-tuple-element.19), channel_id=1, source_target_pairs={{0,192},{8,200},{16,208},{24,216},{32,224},{40,232},{48,240},{56,2... | collective-permute-start | bytes 165896 | tf_op jit(solution)/shard_map/ppermute | solution.py:39
  117.0 55.1 %copy-start.1 = (bf16[256,128]{1,0:T(8,128)(2,1)S(1)}, bf16[256,128]{1,0:T(8,128)(2,1)}, u32[]{:S(2)}) copy-start(bf16[256,128]{1,0:T(8,128)(2,1)} %refs_0_.5) | copy-start | bytes 196612
  119.2 14.6 %collective-permute-start.8 = (bf16[24,256]{1,0:T(8,128)(2,1)S(1)}, bf16[24,256]{1,0:T(8,128)(2,1)S(1)}, u32[]{:S(2)}, u32[]{:S(2)}) collective-permute-start(bf16[24,256]{1,0:T(8,128)(2,1)S(1)} %shard_map.179.refs_2_), channel_id=1, source_target_pairs={{0,64},{8,72},{16,80},{24,88},{32,96},{40,104},{48,112},{56,120},{... | collective-permute-start | bytes 36872 | tf_op jit(solution)/shard_map/ppermute | solution.py:39
  122.2 16.8 %collective-permute-start.10 = (bf16[24,256]{1,0:T(8,128)(2,1)S(1)}, bf16[24,256]{1,0:T(8,128)(2,1)S(1)}, u32[]{:S(2)}, u32[]{:S(2)}) collective-permute-start(bf16[24,256]{1,0:T(8,128)(2,1)S(1)} %shard_map.179.refs_2_), channel_id=1, source_target_pairs={{0,192},{8,200},{16,208},{24,216},{32,224},{40,232},{48,240},{56,2... | collective-permute-start | bytes 36872 | tf_op jit(solution)/shard_map/ppermute | solution.py:39
  133.8 14.5 %collective-permute-start.9 = (bf16[24,256]{1,0:T(8,128)(2,1)S(1)}, bf16[24,256]{1,0:T(8,128)(2,1)S(1)}, u32[]{:S(2)}, u32[]{:S(2)}) collective-permute-start(bf16[24,256]{1,0:T(8,128)(2,1)S(1)} %collective-permute-done.8.refs_1_), channel_id=1, source_target_pairs={{0,64},{8,72},{16,80},{24,88},{32,96},{40,104},{48,112},{56,120},{... | collective-permute-start | bytes 36872 | tf_op jit(solution)/shard_map/ppermute | solution.py:39
  148.3 7.9 %collective-permute-start.11 = (bf16[96,256]{1,0:T(8,128)(2,1)S(1)}, bf16[96,256]{1,0:T(8,128)(2,1)S(1)}, u32[]{:S(2)}, u32[]{:S(2)}) collective-permute-start(bf16[96,256]{1,0:T(8,128)(2,1)S(1)} %bitcast.12), channel_id=1, source_target_pairs={{0,8},{8,16},{16,24},{24,32},{32,40},{40,48},{48,56},{56,64},{64,7... | collective-permute-start | bytes 147464 | tf_op jit(solution)/shard_map/ppermute | solution.py:39
  150.3 7.6 %collective-permute-start.12 = (bf16[96,256]{1,0:T(8,128)(2,1)S(1)}, bf16[96,256]{1,0:T(8,128)(2,1)S(1)}, u32[]{:S(2)}, u32[]{:S(2)}) collective-permute-start(bf16[96,256]{1,0:T(8,128)(2,1)S(1)} %bitcast.13), channel_id=1, source_target_pairs={{0,248},{8,0},{16,8},{24,16},{32,24},{40,32},{48,40},{56,48},{64,5... | collective-permute-start | bytes 147464 | tf_op jit(solution)/shard_map/ppermute | solution.py:39
  157.9 14.2 %collective-permute-start.13 = (bf16[3,96,256]{2,1,0:T(8,128)(2,1)S(1)}, bf16[3,96,256]{2,1,0:T(8,128)(2,1)S(1)}, u32[]{:S(2)}, u32[]{:S(2)}) collective-permute-start(bf16[3,96,256]{2,1,0:T(8,128)(2,1)S(1)} %shard_map.181.refs_2_), channel_id=1, source_target_pairs={{0,24},{8,32},{16,40},{24,48},{32,56},{40,64},{48,72},{56,80},{64,... | collective-permute-start | bytes 442376 | tf_op jit(solution)/shard_map/ppermute | solution.py:39
  161.6 10.4 %collective-permute-start.14 = (bf16[2,96,256]{2,1,0:T(8,128)(2,1)S(1)}, bf16[2,96,256]{2,1,0:T(8,128)(2,1)S(1)}, u32[]{:S(2)}, u32[]{:S(2)}) collective-permute-start(bf16[2,96,256]{2,1,0:T(8,128)(2,1)S(1)} %slice.9), channel_id=1, source_target_pairs={{0,232},{8,240},{16,248},{24,0},{32,8},{40,16},{48,24},{56,32},{64... | collective-permute-start | bytes 294920 | tf_op jit(solution)/shard_map/ppermute | solution.py:39
where the time goes:
time: 195 us; the launch traced here: 194 us
  starting transfers between devices  116 us (59%)
  waiting for transfers between devices  34.8 us (18%)
  blocking collectives  20.5 us (11%)
  Pallas kernels  11 us (6%)
  local copies, waits for them, and re-layouts  8.43 us (4%)
  other arithmetic  2.21 us (1%)
    ppermute x15, starting transfers between devices, shift(): lax.ppermute(table, 'kv', [(i, (i + by) % axis_size) for i in range(axis_...  116 us
    ppermute x15, waiting for transfers between devices, shift(): lax.ppermute(table, 'kv', [(i, (i + by) % axis_size) for i in range(axis_...  34.8 us
    all_to_all x1, blocking collectives, shards(): lax.all_to_all(partial.reshape(kv_size * own_rows, -1), 'tp', 0, 0, tiled...  11.2 us
    all_to_all x1, blocking collectives, shards(): lax.all_to_all(copies.reshape(exchanged.shape), 'tp', 0, 0, tiled=True)  9.28 us
    pallas_call x1, Pallas kernels, replay(): pl.pallas_call(replay_body, grid=(seq_count,), in_specs=[row_spec, row_sp...  6.44 us
    unnamed x23, local copies, waits for them, and re-layouts  5.71 us
    pallas_call x8, Pallas kernels, kernel(): pl.pallas_call(body, in_specs=[smem] * len(scalars) + [vmem] * len(arrays...  4.57 us
  transfers between devices with their start and end apart: 15, of which 9 were waited for; matrix products, arithmetic and copies ran while one was open for 5% of the time, Pallas kernels for 3%

commit v1 on v0

--- a/solution.py
+++ b/solution.py
@@ -9,9 +9,7 @@
 EPS = 1e-06
 WINDOW = (-1, 0, 1, 2)
 JUMP = len(WINDOW)
-NEAR_OUT = 8
 AHEAD = (0, JUMP, -JUMP, 2 * JUMP, -2 * JUMP, 3 * JUMP, -3 * JUMP, 4 * JUMP)
-GATHER = "near"
 LANES = 128
 HALF = LANES // 2
 F32 = jnp.float32
@@ -39,45 +37,42 @@
     return lax.ppermute(table, "kv", [(i, (i + by) % axis_size) for i in range(axis_size)])
 
 
-def replay_body(keys_ref, values_ref, beta_ref, logdecay_ref, accepted_ref, state_ref, out_ref):
-    seq = pl.program_id(0)
-    heads_here, depth = state_ref.shape[1], state_ref.shape[2]
-    span_size = keys_ref.shape[1] // heads_here
-    for head in range(heads_here):
-        carry = state_ref[0, head]
+def replay_body(beta_ref, logdecay_ref, accepted_ref, keys_ref, values_ref, state_ref, out_ref, rows_ref):
+    seq_count, span_size, heads_here, depth = keys_ref.shape
+    rows_ref[...] = jnp.zeros(rows_ref.shape, F32)
+
+    def one(seq, carry):
         for position in range(span_size):
-            row = position * heads_here + head
-            active = accepted_ref[seq] > position
-            spot = seq * span_size * heads_here + row
-            logdecay = jnp.where(active, logdecay_ref[spot], F32(0.0))
-            strength = jnp.where(active, beta_ref[spot], F32(0.0))
-            factor = jnp.exp(jnp.full((1, depth), logdecay, F32))
-            key = keys_ref[0, row : row + 1, :]
-            key = key * lax.rsqrt(jnp.sum(key * key, axis=-1, keepdims=True) + EPS)
-            key_columns = jnp.transpose(jnp.broadcast_to(key, (depth, depth)))
-            carry = factor * carry
-            predicted = jnp.sum(key_columns * carry, axis=0, keepdims=True)
-            update = strength * (values_ref[0, row : row + 1, :] - predicted)
-            carry = carry + key_columns * update
-        out_ref[0, head] = carry
-
-
-def replay(state, prev_keys, prev_values, prev_beta, prev_logdecay, accepted):
-    seq_count, heads_here, depth, _ = state.shape
-    rows = prev_keys.shape[1] * heads_here
-    keys = prev_keys.astype(F32).reshape(seq_count, rows, depth)
-    values = prev_values.astype(F32).reshape(seq_count, rows, depth)
-    row_spec = pl.BlockSpec((1, rows, depth), lambda b: (b, 0, 0))
-    state_spec = pl.BlockSpec((1, heads_here, depth, depth), lambda b: (b, 0, 0, 0))
-    smem = pl.BlockSpec(memory_space=pltpu.SMEM)
-    return pl.pallas_call(
-        replay_body,
-        grid=(seq_count,),
-        in_specs=[row_spec, row_spec, smem, smem, smem, state_spec],
-        out_specs=state_spec,
-        out_shape=jax.ShapeDtypeStruct(state.shape, F32),
-        name="replay",
-    )(keys, values, prev_beta.reshape(-1), prev_logdecay.reshape(-1), accepted, state)
+            first = position * heads_here
+            keys = keys_ref[seq, position].astype(F32)
+            keys = keys * lax.rsqrt(jnp.sum(keys * keys, axis=-1, keepdims=True) + EPS)
+            rows_ref[first : first + heads_here, :] = keys
+        key_columns = jnp.transpose(rows_ref[...])
+        for head in range(heads_here):
+            state = state_ref[seq, head]
+            for position in range(span_size):
+                row = position * heads_here + head
+                spot = seq * span_size * heads_here + row
+                active = accepted_ref[seq] > position
+                logdecay = jnp.where(active, logdecay_ref[spot], F32(0.0))
+                strength = jnp.where(active, beta_ref[spot], F32(0.0))
+                column = jnp.broadcast_to(key_columns[:, row : row + 1], (depth, depth))
+                state = jnp.exp(jnp.full((1, depth), logdecay, F32)) * state
+                predicted = jnp.sum(column * state, axis=0, keepdims=True)
+                value = values_ref[seq, position].astype(F32)[head : head + 1]
+                state = state + column * (strength * (value - predicted))
+            out_ref[seq, head] = state
+        return carry
+
+    lax.fori_loop(0, seq_count, one, 0)
+
+
+def replay(state, prev_keys, prev_values, beta, logdecay, accepted):
+    rows = -(-prev_keys.shape[1] * prev_keys.shape[2] // 8) * 8
+    scratch = [pltpu.VMEM((rows, state.shape[-1]), F32)]
+    scalars = [beta, logdecay, accepted]
+    (carried,) = kernel(replay_body, scalars, [prev_keys, prev_values, state], [(state.shape, F32)], scratch)
+    return carried
 
 
 def rows_for(wide_ref, device, kv_size, own_rows):
@@ -92,7 +87,7 @@
 
 
 def layout(columns, own_rows):
-    weights_at = 0 if GATHER == "near" else columns
+    weights_at = columns
     gain_at = weights_at + 4 * columns
     rows_at = gain_at + 16
     return weights_at, gain_at, rows_at, len(AHEAD) * own_rows // 2
@@ -109,9 +104,8 @@
     gain = jnp.concatenate([gain_ref[...]] * (wq_ref.shape[1] // columns), axis=1)
     gain = jnp.broadcast_to(gain, (16, wq_ref.shape[1]))
     for out_ref, stops in ((next_ref, (1,)), (previous_ref, (-2, -1))):
-        if GATHER != "near":
-            out_ref[:columns, :columns] = wo_ref[:columns, :]
-            out_ref[:columns, columns:] = wo_ref[columns:, :]
+        out_ref[:columns, :columns] = wo_ref[:columns, :]
+        out_ref[:columns, columns:] = wo_ref[columns:, :]
         for j, weight_ref in enumerate((wq_ref, wk_ref, wv_ref, wg_ref)):
             out_ref[weights_at + j * columns : weights_at + (j + 1) * columns, :] = weight_ref[...]
         out_ref[gain_at:rows_at, :] = gain
@@ -149,8 +143,26 @@
 
 
 def project_body(
-    kv_size, own_rows, columns, own_rows_ref, small_ref, own_ref, before_ref, after_ref, after2_ref, up_ref, down_ref, across_ref, kept_ref, sums_ref
+    kv_size,
+    own_rows,
+    columns,
+    own_rows_ref,
+    small_ref,
+    own_ref,
+    before_ref,
+    after_ref,
+    after2_ref,
+    up_ref,
+    down_ref,
+    across_ref,
+    kept_ref,
+    w_out_ref,
+    sums_ref,
 ):
+    for at, packet_ref in enumerate((before_ref, own_ref, after_ref, after2_ref)):
+        for part in range(w_out_ref.shape[0] // columns):
+            piece = packet_ref[:columns, part * columns : (part + 1) * columns]
+            w_out_ref[part * columns : (part + 1) * columns, at * columns : (at + 1) * columns] = piece
     wide = own_ref.shape[1]
     weights_at, gain_at, rows_at, half = layout(columns, own_rows)
     shard_kv = lax.axis_index("kv")
@@ -175,13 +187,15 @@
             term = jnp.dot(scaled, weights[j], preferred_element_type=F32)
             sums[j] = term if sums[j] is None else sums[j] + term
         small_at = pl.multiple_of((shard_kv + WINDOW[at] + kv_size) % kv_size * columns, columns)
-        term = jnp.dot(scaled, small_ref[pl.ds(small_at, columns), :], preferred_element_type=F32)
+        term = lax.dot_general(
+            scaled, small_ref[:, pl.ds(small_at, columns)], (((1,), (1,)), ((), ())), preferred_element_type=F32
+        )
         small = term if small is None else small + term
-    lane = lax.broadcasted_iota(jnp.int32, small.shape, 1)
-    small = jnp.where(lane == HALF - 1, squares, small)
     for j in range(4):
         sums_ref[:, j * wide : (j + 1) * wide] = sums[j]
-    sums_ref[:, 4 * wide :] = small
+    lane = lax.broadcasted_iota(jnp.int32, (small.shape[0], LANES), 1)
+    sums_ref[:, 4 * wide :] = jnp.where(lane == HALF - 1, squares, F32(0.0))
+    sums_ref[:, 4 * wide : 4 * wide + small.shape[1]] = small
 
     def block(ahead):
         start = AHEAD.index(ahead) * own_rows
@@ -205,6 +219,7 @@
     columns = own_rows_wide.shape[1]
     across = 4 * packets[0].shape[1] + LANES
     shapes = [((count, own_rows, across), BF16) for count in (2, 2, 1)] + [((3, own_rows, across), F32)]
+    shapes.append(((packets[0].shape[1], JUMP * columns), BF16))
 
     def body(*refs):
         project_body(kv_size, own_rows, columns, *refs)
@@ -237,68 +252,13 @@
     return kernel(body, [], [kept, up, down, across, carried], shapes)
 
 
-def deliver_body(*refs):
-    *row_refs, wo_ref, before_ref, after_ref, after2_ref, out_ref = refs
-    rows = jnp.concatenate([ref[...] for ref in row_refs], axis=0)
-    columns = wo_ref.shape[1]
-    for at, packet_ref in enumerate((before_ref, None, after_ref, after2_ref)):
-        if packet_ref is None:
-            weight = wo_ref[...]
-        else:
-            weight = jnp.concatenate([packet_ref[:columns, :columns], packet_ref[:columns, columns:]], axis=0)
-        product = jnp.dot(rows, weight, preferred_element_type=F32)
-        out_ref[:, at * columns : (at + 1) * columns] = product.astype(BF16)
-
-
-def deliver(pieces, w_out, packets):
-    shape = (sum(piece.shape[0] for piece in pieces), JUMP * w_out.shape[1])
-    (partial,) = kernel(deliver_body, [], [*pieces, w_out, *packets], [(shape, BF16)])
+def deliver_body(rows_ref, weight_ref, out_ref):
+    out_ref[...] = jnp.dot(rows_ref[...], weight_ref[...], preferred_element_type=F32).astype(BF16)
+
+
+def deliver(rows, weight):
+    (partial,) = kernel(deliver_body, [], [rows, weight], [((rows.shape[0], weight.shape[1]), BF16)])
     return partial
-
-
-def deliver_near_body(kv_size, weight_ref, left_ref, three_ref, right_ref, out_ref):
-    shard_kv = lax.axis_index("kv")
-    own_rows = out_ref.shape[1]
-    far_members = kv_size // NEAR_OUT
-    pieces = [left_ref[0], left_ref[1], left_ref[2], three_ref[0], three_ref[1], three_ref[2], right_ref[0], right_ref[1]]
-    for n, piece in enumerate(pieces):
-        product = jnp.dot(piece, weight_ref[...], preferred_element_type=F32)
-        for j in range(far_members):
-            owner = (shard_kv + n - 4 + NEAR_OUT * (j - 2) + kv_size) % kv_size
-            out_ref[owner] = product[j * own_rows : (j + 1) * own_rows].astype(BF16)
-
-
-def deliver_near(w_out, left, three, right, kv_size, own_rows):
-    def body(*refs):
-        deliver_near_body(kv_size, *refs)
-
-    shape = (kv_size, own_rows, w_out.shape[1])
-    (partial,) = kernel(body, [], [w_out, left, three, right], [(shape, BF16)])
-    return partial
-
-
-def reduce_all_body(terms_ref, out_ref):
-    total = terms_ref[0].astype(F32)
-    for member in range(1, terms_ref.shape[0]):
-        total = total + terms_ref[member].astype(F32)
-    for member in range(terms_ref.shape[0]):
-        out_ref[member] = total.astype(BF16)
-
-
-def reduce_all(terms):
-    (copies,) = kernel(reduce_all_body, [], [terms], [(terms.shape, BF16)])
-    return copies
-
-
-def stack_body(*refs):
-    out_ref = refs[-1]
-    for at, ref in enumerate(refs[:-1]):
-        out_ref[at] = ref[...]
-
-
-def stacked(pieces):
-    (out,) = kernel(stack_body, [], pieces, [((len(pieces), *pieces[0].shape), BF16)])
-    return out
 
 
 def reduce_body(terms_ref, *out_refs):
@@ -331,10 +291,7 @@
     shard_kv = lax.axis_index("kv")
     kv_size = blocks_ref.shape[0]
     for n in range(kv_size):
-        if GATHER == "exchange":
-            owner = (shard_kv + n % JUMP + JUMP - WINDOW[-1]) % JUMP + n // JUMP * JUMP
-        else:
-            owner = (shard_kv + n + 2 * kv_size - WINDOW[-1] - 3 * JUMP) % kv_size
+        owner = (shard_kv + n % JUMP + JUMP - WINDOW[-1]) % JUMP + n // JUMP * JUMP
         out_ref[owner] = blocks_ref[n]
 
 
@@ -471,12 +428,12 @@
     after = shift(to_previous, kv_size, -1)
     after2 = shift(after[: to_next.shape[0]], kv_size, -1)
 
-    carried = replay(state, prev_keys, prev_values, prev_beta, prev_logdecay, accepted)
-    small_weights = jnp.concatenate(
-        [w_beta, w_decay, jnp.zeros((model_width, LANES - 2 * total_heads), w_beta.dtype)], axis=1
-    )
+    beta = prev_beta.reshape(-1)
+    logdecay = prev_logdecay.reshape(-1)
+    carried = replay(state, prev_keys, prev_values, beta, logdecay, accepted)
+    small_weights = jnp.concatenate([w_beta.T, w_decay.T], axis=0)
     packets = (to_next, before, after, after2)
-    up, down, across, kept = project(own_rows_wide, small_weights, packets, kv_size, own_rows)
+    up, down, across, kept, w_out_near = project(own_rows_wide, small_weights, packets, kv_size, own_rows)
     across = shift(across, kv_size, 2 * JUMP)
     up = shift(up, kv_size, JUMP)
     down = shift(down, kv_size, -JUMP)
@@ -485,35 +442,10 @@
     behind = shift(behind, kv_size, -2 * JUMP)
     terms = (kept, up, down, ahead, behind)
     members = kv_size // JUMP
-    copies = members if GATHER == "exchange" else 1
-    hidden = propose(decay_rate, out_gain, terms, carried, span_size, total_heads, model_width, copies)
-
-    if GATHER == "near":
-        below = shift(hidden, kv_size, NEAR_OUT)
-        above = shift(hidden, kv_size, -NEAR_OUT)
-        opposite = shift(below, kv_size, NEAR_OUT)
-        block = stacked([opposite, below, hidden, above]).reshape(4 * own_rows, -1)
-        left = shift(block, kv_size, 1)
-        right = shift(block, kv_size, -1)
-        three = stacked([left, block, right])
-        near_left = shift(three, kv_size, 3)
-        near_right = shift(three[:2], kv_size, -3)
-        partial = deliver_near(w_out, near_left, three, near_right, kv_size, own_rows)
-        exchanged = lax.all_to_all(partial.reshape(kv_size * own_rows, -1), "tp", 0, 0, tiled=True)
-        copies = reduce_all(exchanged.reshape(tp_size, -1, exchanged.shape[1]))
-        mixed = lax.all_to_all(copies.reshape(exchanged.shape), "tp", 0, 0, tiled=True)
-        return (mixed, carried)
-    if GATHER == "exchange":
-        groups = [list(range(first, kv_size, JUMP)) for first in range(JUMP)]
-        pieces = (lax.all_to_all(hidden, "kv", 0, 0, tiled=True, axis_index_groups=groups),)
-    else:
-        below = shift(hidden, kv_size, JUMP)
-        above = shift(hidden, kv_size, -JUMP)
-        three = jnp.concatenate([below, hidden, above], axis=0)
-        low = shift(three[own_rows:], kv_size, 3 * JUMP)
-        high = shift(three, kv_size, -3 * JUMP)
-        pieces = (low, three, high)
-    partial = deliver(pieces, w_out, (before, after, after2))
+    hidden = propose(decay_rate, out_gain, terms, carried, span_size, total_heads, model_width, members)
+    groups = [list(range(first, kv_size, JUMP)) for first in range(JUMP)]
+    rows_all = lax.all_to_all(hidden, "kv", 0, 0, tiled=True, axis_index_groups=groups)
+    partial = deliver(rows_all, w_out_near)
     exchanged = lax.all_to_all(partial, "tp", 0, 0, tiled=True)
     finished = reduce_terms(exchanged.reshape(tp_size, own_rows, -1))
     landed = [

time: 195 us -> 199 us (1.021)
  blocking collectives: 20.5 us -> 49.9 us
  starting transfers between devices: 116 us -> 92.4 us
  waiting for transfers between devices: 34.8 us -> 40.3 us
  local copies, waits for them, and re-layouts: 8.43 us -> 3.86 us
  other arithmetic: 2.21 us -> 0.03 us
    all_to_all x2, blocking collectives: 20.5 us -> 49.9 us  [the longest x1 37.2 us: shards(): lax.all_to_all(hidden, 'kv', 0, 0, tiled=True, axis_index_groups=groups)]
    ppermute x15 -> x11, starting transfers between devices: 116 us -> 88.8 us  [shift(): lax.ppermute(table, 'kv', [(i, (i + by) % axis_size) for i in range(axis_...]
    pallas_call x1 -> x0, Pallas kernels: 6.44 us -> none  [replay(): pl.pallas_call(replay_body, grid=(seq_count,), in_specs=[row_spec, row_sp...]
    pallas_call x8 -> x9, Pallas kernels: 4.57 us -> 10.5 us  [kernel(): pl.pallas_call(body, in_specs=[smem] * len(scalars) + [vmem] * len(arrays...]
    all_to_all x0 -> x1, waiting for transfers between devices: none -> 5.61 us  [shards(): mixed = lax.all_to_all(copies, 'tp', 0, 0, tiled=True)]
    all_to_all x0 -> x1, starting transfers between devices: none -> 3.6 us  [shards(): mixed = lax.all_to_all(copies, 'tp', 0, 0, tiled=True)]
    unnamed x23 -> x19, local copies, waits for them, and re-layouts: 5.71 us -> 2.5 us
    concatenate x1, other arithmetic: 2.19 us -> 0.03 us  [shards(): small_weights = jnp.concatenate([w_beta.T, w_decay.T], axis=0)]
  transfers between devices with their start and end apart: 15 -> 12, of which waited for: 9 -> 8; matrix products, arithmetic and copies ran while one was open for 5% -> 1% of each run, Pallas kernels for 3% -> 2%
where the time goes in v1:
time: 199 us; the launch traced here: 198 us
  starting transfers between devices  92.4 us (46%)
  blocking collectives  49.9 us (25%)
  waiting for transfers between devices  40.3 us (20%)
  Pallas kernels  10.5 us (5%)
  local copies, waits for them, and re-layouts  3.86 us (2%)
    ppermute x11, starting transfers between devices, shift(): lax.ppermute(table, 'kv', [(i, (i + by) % axis_size) for i in range(axis_...  88.8 us
    all_to_all x1, blocking collectives, shards(): lax.all_to_all(hidden, 'kv', 0, 0, tiled=True, axis_index_groups=groups)  37.2 us
    ppermute x11, waiting for transfers between devices, shift(): lax.ppermute(table, 'kv', [(i, (i + by) % axis_size) for i in range(axis_...  34.7 us
    all_to_all x1, blocking collectives, shards(): exchanged = lax.all_to_all(partial, 'tp', 0, 0, tiled=True)  12.8 us
    pallas_call x9, Pallas kernels, kernel(): pl.pallas_call(body, in_specs=[smem] * len(scalars) + [vmem] * len(arrays...  10.5 us
    all_to_all x1, waiting for transfers between devices, shards(): mixed = lax.all_to_all(copies, 'tp', 0, 0, tiled=True)  5.61 us
  transfers between devices with their start and end apart: 12, of which 8 were waited for; matrix products, arithmetic and copies ran while one was open for 1% of the time, Pallas kernels for 2%

profile of v1, /device:TPU:40, one launch (start us, length us, event | category | flops | bytes accessed | tf_op | source)
XLA Modules:
  0.0 197.9 jit_solution(13492922755443327481)
XLA Ops:
  0.6 1.2 shard_map.176
  1.8 45.3 %collective-permute-start.1 = (bf16[848,256]{1,0:T(8,128)(2,1)S(1)}, bf16[848,256]{1,0:T(8,128)(2,1)S(1)}, u32[]{:S(2)}, u32[]{:S(2)}) collective-permute-start(bf16[848,256]{1,0:T(8,128)(2,1)S(1)} %get-tuple-element.18), channel_id=1, source_target_pairs={{0,248},{8,0},{16,8},{24,16},{32,24},{40,32},{48,40},{56,48},{64,5... | collective-permute-start | bytes 1302536 | tf_op jit(solution)/shard_map/ppermute | solution.py:37
  47.2 2.1 %collective-permute-start = (bf16[752,256]{1,0:T(8,128)(2,1)S(1)}, bf16[752,256]{1,0:T(8,128)(2,1)S(1)}, u32[]{:S(2)}, u32[]{:S(2)}) collective-permute-start(bf16[752,256]{1,0:T(8,128)(2,1)S(1)} %get-tuple-element.17.refs_2_), channel_id=1, source_target_pairs={{0,8},{8,16},{16,24},{24,32},{32,40},{40,48},{48,56},{56,64},{64,7... | collective-permute-start | bytes 1155080 | tf_op jit(solution)/shard_map/ppermute | solution.py:37
  49.3 7.2 %collective-permute-done.1.refs_4_ = bf16[848,256]{1,0:T(8,128)(2,1)S(1)} collective-permute-done((bf16[848,256]{1,0:T(8,128)(2,1)S(1)}, bf16[848,256]{1,0:T(8,128)(2,1)S(1)}, u32[]{:S(2)}, u32[]{:S(2)}) %collective-permute-start.1) | collective-permute-done | bytes 434208 | tf_op jit(solution)/shard_map/ppermute | solution.py:37
  56.5 5.6 %collective-permute-start.2 = (bf16[752,256]{1,0:T(8,128)(2,1)S(1)}, bf16[752,256]{1,0:T(8,128)(2,1)S(1)}, u32[]{:S(2)}, u32[]{:S(2)}) collective-permute-start(bf16[752,256]{1,0:T(8,128)(2,1)S(1)} %slice.4), channel_id=1, source_target_pairs={{0,248},{8,0},{16,8},{24,16},{32,24},{40,32},{48,40},{56,48},{64,5... | collective-permute-start | bytes 1155080 | tf_op jit(solution)/shard_map/ppermute | solution.py:37
  62.2 7.3 %collective-permute-done.2.refs_5_ = bf16[752,256]{1,0:T(8,128)(2,1)S(1)} collective-permute-done((bf16[752,256]{1,0:T(8,128)(2,1)S(1)}, bf16[752,256]{1,0:T(8,128)(2,1)S(1)}, u32[]{:S(2)}, u32[]{:S(2)}) %collective-permute-start.2) | collective-permute-done | bytes 385056 | tf_op jit(solution)/shard_map/ppermute | solution.py:37
  69.5 1.4 shard_map.177
  71.0 2.1 %collective-permute-start.3 = (bf16[2,24,1152]{2,1,0:T(8,128)(2,1)}, bf16[2,24,1152]{2,1,0:T(8,128)(2,1)S(1)}, u32[]{:S(2)}, u32[]{:S(2)}) collective-permute-start(bf16[2,24,1152]{2,1,0:T(8,128)(2,1)} %get-tuple-element.20), channel_id=1, source_target_pairs={{0,32},{8,40},{16,48},{24,56},{32,64},{40,72},{48,80},{56,88},{64,... | collective-permute-start | bytes 331784 | tf_op jit(solution)/shard_map/ppermute | solution.py:37
  73.0 7.9 %collective-permute-start.4 = (bf16[2,24,1152]{2,1,0:T(8,128)(2,1)}, bf16[2,24,1152]{2,1,0:T(8,128)(2,1)S(1)}, u32[]{:S(2)}, u32[]{:S(2)}) collective-permute-start(bf16[2,24,1152]{2,1,0:T(8,128)(2,1)} %get-tuple-element.21), channel_id=1, source_target_pairs={{0,224},{8,232},{16,240},{24,248},{32,0},{40,8},{48,16},{56,24},{6... | collective-permute-start | bytes 331784 | tf_op jit(solution)/shard_map/ppermute | solution.py:37
  80.9 2.0 collective-permute-start.5
  83.0 0.7 reshape.31.beta_ref
  83.8 0.6 reshape.32.logdecay_ref
  84.5 1.2 copy-done
  85.7 4.0 %shard_map.178.refs_4_.refs_7_ = f32[8,2,128,128]{3,2,1,0:T(8,128)S(1)} custom-call(f32[48]{0:T(128)} %reshape.31.beta_ref, f32[48]{0:T(128)} %reshape.32.logdecay_ref, s32[8]{0:T(128)} %accepted_ref.1, bf16[8,3,2,128]{3,2,1,0:T(2,128)(2,1)S(1)} %copy-done.1, bf16[8,3,2,128]{3,2,1,0:T(2,128)(2,1)S(1)} %copy-done.2, f32[8,2,128,128]{3,2,1,0:T(8,128)S(1)} %copy-done), custom_call_target="tpu_custom_call" | custom-call | tf_op jit(solution)/shard_map/pallas_call | solution.py:27
  89.8 12.5 %collective-permute-done.5.refs_3_ = bf16[1,24,1152]{2,1,0:T(8,128)(2,1)S(1)} collective-permute-done((bf16[1,24,1152]{2,1,0:T(8,128)(2,1)}, bf16[1,24,1152]{2,1,0:T(8,128)(2,1)S(1)}, u32[]{:S(2)}, u32[]{:S(2)}) %collective-permute-start.5) | collective-permute-done | bytes 55328 | tf_op jit(solution)/shard_map/ppermute | solution.py:37
  102.5 1.9 collective-permute-start.6
  104.4 12.7 %collective-permute-start.7 = (bf16[24,1152]{1,0:T(8,128)(2,1)S(1)}, bf16[24,1152]{1,0:T(8,128)(2,1)S(1)}, u32[]{:S(2)}, u32[]{:S(2)}) collective-permute-start(bf16[24,1152]{1,0:T(8,128)(2,1)S(1)} %get-tuple-element.24), channel_id=1, source_target_pairs={{0,192},{8,200},{16,208},{24,216},{32,224},{40,232},{48,240},{56,2... | collective-permute-start | bytes 165896 | tf_op jit(solution)/shard_map/ppermute | solution.py:37
  117.1 2.5 %collective-permute-done.6.refs_5_ = bf16[24,1152]{1,0:T(8,128)(2,1)S(1)} collective-permute-done((bf16[24,1152]{1,0:T(8,128)(2,1)S(1)}, bf16[24,1152]{1,0:T(8,128)(2,1)S(1)}, u32[]{:S(2)}, u32[]{:S(2)}) %collective-permute-start.6) | collective-permute-done | bytes 55328 | tf_op jit(solution)/shard_map/ppermute | solution.py:37
  119.6 0.4 collective-permute-done.7.refs_6_
  119.9 2.1 %shard_map.180 = bf16[192,256]{1,0:T(8,128)(2,1)S(1)} custom-call(f32[2]{0:T(128)} %refs_0_.3, bf16[1,128]{1,0:T(2,128)(2,1)S(1)} %bitcast.14, f32[3,24,1152]{2,1,0:T(8,128)S(1)} %get-tuple-element.19.refs_0_.refs_2_, bf16[2,24,1152]{2,1,0:T(8,128)(2,1)S(1)} %collective-permute-done.3.refs_1_.refs_3_, ...), custom_call_target="tpu_custom_call" | custom-call | tf_op jit(solution)/shard_map/pallas_call | solution.py:27
  122.0 37.2 %all_to_all.29 = bf16[8,24,256]{2,1,0:T(8,128)(2,1)S(1)} all-to-all(bf16[8,24,256]{2,1,0:T(8,128)(2,1)S(1)} %bitcast.12), channel_id=1, replica_groups={{0,32,64,96,128,160,192,224},{8,40,72,104,136,168,200,232},{16,48,80,11..., dimensions={0} | all-to-all | bytes 196608 | tf_op jit(solution)/shard_map/all_to_all | solution.py:447
  159.4 12.8 %all_to_all.30.terms_ref = bf16[8,24,512]{2,1,0:T(8,128)(2,1)S(1)} all-to-all(bf16[8,24,512]{2,1,0:T(8,128)(2,1)S(1)} %bitcast.11), channel_id=1, replica_groups=mesh['grp'=2,'kv'=32,'tp'=8] {'tp'}, dimensions={0} | all-to-all | bytes 393216 | tf_op jit(solution)/shard_map/all_to_all | solution.py:449
  172.2 2.0 collective-permute-start.10
  174.1 5.4 %collective-permute-start.8 = (bf16[24,128]{1,0:T(8,128)(2,1)S(1)}, bf16[24,128]{1,0:T(8,128)(2,1)S(1)}, u32[]{:S(2)}, u32[]{:S(2)}) collective-permute-start(bf16[24,128]{1,0:T(8,128)(2,1)S(1)} %get-tuple-element.26), channel_id=1, source_target_pairs={{0,16},{8,24},{16,32},{24,40},{32,48},{40,56},{48,64},{56,72},{64,... | collective-permute-start | bytes 18440 | tf_op jit(solution)/shard_map/ppermute | solution.py:37
  179.5 2.0 collective-permute-start.9
  181.5 0.3 collective-permute-done.8.refs_0_
  181.8 4.5 %collective-permute-done.9.refs_1_ = bf16[24,128]{1,0:T(8,128)(2,1)S(1)} collective-permute-done((bf16[24,128]{1,0:T(8,128)(2,1)S(1)}, bf16[24,128]{1,0:T(8,128)(2,1)S(1)}, u32[]{:S(2)}, u32[]{:S(2)}) %collective-permute-start.9) | collective-permute-done | bytes 6176 | tf_op jit(solution)/shard_map/ppermute | solution.py:37
  186.3 0.7 shard_map.183
  187.0 3.6 %all-to-all-start.2 = ((bf16[8,96,128]{2,1,0:T(8,128)(2,1)}), bf16[8,96,128]{2,1,0:T(8,128)(2,1)S(1)}, u32[]{:S(2)}, u32[]{:S(2)}) async-start(bf16[8,96,128]{2,1,0:T(8,128)(2,1)} %bitcast.7), calls=%async_computation.2 | async-start | bytes 393216 | tf_op jit(solution)/shard_map/all_to_all | solution.py:455
  190.6 1.0 copy.23
  191.6 5.6 %all-to-all-done.2 = bf16[8,96,128]{2,1,0:T(8,128)(2,1)S(1)} async-done(((bf16[8,96,128]{2,1,0:T(8,128)(2,1)}), bf16[8,96,128]{2,1,0:T(8,128)(2,1)S(1)}, u32[]{:S(2)}, u32[]{:S(2)}) %all-to-all-start.2) | async-done | bytes 196640 | tf_op jit(solution)/shard_map/all_to_all | solution.py:455
  197.2 0.7 shard_map.184
  (26 shorter events, 0.8 us)
Async XLA Ops:
  1.8 54.6 %collective-permute-start.1 = (bf16[848,256]{1,0:T(8,128)(2,1)S(1)}, bf16[848,256]{1,0:T(8,128)(2,1)S(1)}, u32[]{:S(2)}, u32[]{:S(2)}) collective-permute-start(bf16[848,256]{1,0:T(8,128)(2,1)S(1)} %get-tuple-element.18), channel_id=1, source_target_pairs={{0,248},{8,0},{16,8},{24,16},{32,24},{40,32},{48,40},{56,48},{64,5... | collective-permute-start | bytes 1302536 | tf_op jit(solution)/shard_map/ppermute | solution.py:37
  47.2 15.0 %copy-start.4 = (bf16[4096,16]{0,1:T(8,128)(2,1)S(1)}, bf16[4096,16]{0,1:T(8,128)(2,1)}, u32[]{:S(2)}) copy-start(bf16[4096,16]{0,1:T(8,128)(2,1)} %param.24) | copy-start | bytes 393220
  47.2 15.0 %copy-start.5 = (bf16[4096,16]{0,1:T(8,128)(2,1)S(1)}, bf16[4096,16]{0,1:T(8,128)(2,1)}, u32[]{:S(2)}) copy-start(bf16[4096,16]{0,1:T(8,128)(2,1)} %param.23) | copy-start | bytes 393220
  47.2 15.0 %collective-permute-start = (bf16[752,256]{1,0:T(8,128)(2,1)S(1)}, bf16[752,256]{1,0:T(8,128)(2,1)S(1)}, u32[]{:S(2)}, u32[]{:S(2)}) collective-permute-start(bf16[752,256]{1,0:T(8,128)(2,1)S(1)} %get-tuple-element.17.refs_2_), channel_id=1, source_target_pairs={{0,8},{8,16},{16,24},{24,32},{32,40},{40,48},{48,56},{56,64},{64,7... | collective-permute-start | bytes 1155080 | tf_op jit(solution)/shard_map/ppermute | solution.py:37
  56.5 13.0 %collective-permute-start.2 = (bf16[752,256]{1,0:T(8,128)(2,1)S(1)}, bf16[752,256]{1,0:T(8,128)(2,1)S(1)}, u32[]{:S(2)}, u32[]{:S(2)}) collective-permute-start(bf16[752,256]{1,0:T(8,128)(2,1)S(1)} %slice.4), channel_id=1, source_target_pairs={{0,248},{8,0},{16,8},{24,16},{32,24},{40,32},{48,40},{56,48},{64,5... | collective-permute-start | bytes 1155080 | tf_op jit(solution)/shard_map/ppermute | solution.py:37
  71.0 11.9 %copy-start.6 = (f32[8,3,2]{0,2,1:T(2,128)S(1)}, f32[8,3,2]{0,2,1:T(2,128)}, u32[]{:S(2)}) copy-start(f32[8,3,2]{0,2,1:T(2,128)} %param.31) | copy-start | bytes 580
  71.0 31.3 %collective-permute-start.3 = (bf16[2,24,1152]{2,1,0:T(8,128)(2,1)}, bf16[2,24,1152]{2,1,0:T(8,128)(2,1)S(1)}, u32[]{:S(2)}, u32[]{:S(2)}) collective-permute-start(bf16[2,24,1152]{2,1,0:T(8,128)(2,1)} %get-tuple-element.20), channel_id=1, source_target_pairs={{0,32},{8,40},{16,48},{24,56},{32,64},{40,72},{48,80},{56,88},{64,... | collective-permute-start | bytes 331784 | tf_op jit(solution)/shard_map/ppermute | solution.py:37
  73.0 29.3 %collective-permute-start.4 = (bf16[2,24,1152]{2,1,0:T(8,128)(2,1)}, bf16[2,24,1152]{2,1,0:T(8,128)(2,1)S(1)}, u32[]{:S(2)}, u32[]{:S(2)}) collective-permute-start(bf16[2,24,1152]{2,1,0:T(8,128)(2,1)} %get-tuple-element.21), channel_id=1, source_target_pairs={{0,224},{8,232},{16,240},{24,248},{32,0},{40,8},{48,16},{56,24},{6... | collective-permute-start | bytes 331784 | tf_op jit(solution)/shard_map/ppermute | solution.py:37
  80.9 21.4 %collective-permute-start.5 = (bf16[1,24,1152]{2,1,0:T(8,128)(2,1)}, bf16[1,24,1152]{2,1,0:T(8,128)(2,1)S(1)}, u32[]{:S(2)}, u32[]{:S(2)}) collective-permute-start(bf16[1,24,1152]{2,1,0:T(8,128)(2,1)} %get-tuple-element.22), channel_id=1, source_target_pairs={{0,64},{8,72},{16,80},{24,88},{32,96},{40,104},{48,112},{56,120},{... | collective-permute-start | bytes 165896 | tf_op jit(solution)/shard_map/ppermute | solution.py:37
  82.9 1.6 copy-start.2
  83.0 0.7 copy-start.7
  83.8 0.7 copy-start.1
  84.5 1.2 copy-start
  102.5 17.1 %collective-permute-start.6 = (bf16[24,1152]{1,0:T(8,128)(2,1)S(1)}, bf16[24,1152]{1,0:T(8,128)(2,1)S(1)}, u32[]{:S(2)}, u32[]{:S(2)}) collective-permute-start(bf16[24,1152]{1,0:T(8,128)(2,1)S(1)} %get-tuple-element.23), channel_id=1, source_target_pairs={{0,64},{8,72},{16,80},{24,88},{32,96},{40,104},{48,112},{56,120},{... | collective-permute-start | bytes 165896 | tf_op jit(solution)/shard_map/ppermute | solution.py:37
  104.4 15.5 %copy-start.3 = (bf16[128]{0:T(256)(128)(2,1)S(1)}, bf16[128]{0:T(256)(128)(2,1)}, u32[]{:S(2)}) copy-start(bf16[128]{0:T(256)(128)(2,1)} %param.26) | copy-start | bytes 772
  104.4 15.5 %collective-permute-start.7 = (bf16[24,1152]{1,0:T(8,128)(2,1)S(1)}, bf16[24,1152]{1,0:T(8,128)(2,1)S(1)}, u32[]{:S(2)}, u32[]{:S(2)}) collective-permute-start(bf16[24,1152]{1,0:T(8,128)(2,1)S(1)} %get-tuple-element.24), channel_id=1, source_target_pairs={{0,192},{8,200},{16,208},{24,216},{32,224},{40,232},{48,240},{56,2... | collective-permute-start | bytes 165896 | tf_op jit(solution)/shard_map/ppermute | solution.py:37
  172.2 9.3 %collective-permute-start.10 = (bf16[24,128]{1,0:T(8,128)(2,1)S(1)}, bf16[24,128]{1,0:T(8,128)(2,1)S(1)}, u32[]{:S(2)}, u32[]{:S(2)}) collective-permute-start(bf16[24,128]{1,0:T(8,128)(2,1)S(1)} %get-tuple-element.29), channel_id=1, source_target_pairs={{0,248},{8,0},{16,8},{24,16},{32,24},{40,32},{48,40},{56,48},{64,5... | collective-permute-start | bytes 18440 | tf_op jit(solution)/shard_map/ppermute | solution.py:37
  174.1 7.7 %collective-permute-start.8 = (bf16[24,128]{1,0:T(8,128)(2,1)S(1)}, bf16[24,128]{1,0:T(8,128)(2,1)S(1)}, u32[]{:S(2)}, u32[]{:S(2)}) collective-permute-start(bf16[24,128]{1,0:T(8,128)(2,1)S(1)} %get-tuple-element.26), channel_id=1, source_target_pairs={{0,16},{8,24},{16,32},{24,40},{32,48},{40,56},{48,64},{56,72},{64,... | collective-permute-start | bytes 18440 | tf_op jit(solution)/shard_map/ppermute | solution.py:37
  179.5 6.8 %collective-permute-start.9 = (bf16[24,128]{1,0:T(8,128)(2,1)S(1)}, bf16[24,128]{1,0:T(8,128)(2,1)S(1)}, u32[]{:S(2)}, u32[]{:S(2)}) collective-permute-start(bf16[24,128]{1,0:T(8,128)(2,1)S(1)} %get-tuple-element.27), channel_id=1, source_target_pairs={{0,8},{8,16},{16,24},{24,32},{32,40},{40,48},{48,56},{56,64},{64,7... | collective-permute-start | bytes 18440 | tf_op jit(solution)/shard_map/ppermute | solution.py:37
  187.0 10.2 %all-to-all-start.2 = ((bf16[8,96,128]{2,1,0:T(8,128)(2,1)}), bf16[8,96,128]{2,1,0:T(8,128)(2,1)S(1)}, u32[]{:S(2)}, u32[]{:S(2)}) async-start(bf16[8,96,128]{2,1,0:T(8,128)(2,1)} %bitcast.7), calls=%async_computation.2 | async-start | bytes 393216 | tf_op jit(solution)/shard_map/all_to_all | solution.py:455

commit v2 on v1

--- a/solution.py
+++ b/solution.py
@@ -9,6 +9,7 @@
 EPS = 1e-06
 WINDOW = (-1, 0, 1, 2)
 JUMP = len(WINDOW)
+NEAR_OUT = 8
 AHEAD = (0, JUMP, -JUMP, 2 * JUMP, -2 * JUMP, 3 * JUMP, -3 * JUMP, 4 * JUMP)
 LANES = 128
 HALF = LANES // 2
@@ -87,14 +88,14 @@
 
 
 def layout(columns, own_rows):
-    weights_at = columns
+    weights_at = 0
     gain_at = weights_at + 4 * columns
     rows_at = gain_at + 16
     return weights_at, gain_at, rows_at, len(AHEAD) * own_rows // 2
 
 
 def pack_body(
-    kv_size, own_rows, tokens_ref, gain_ref, wq_ref, wk_ref, wv_ref, wg_ref, wo_ref, next_ref, previous_ref, own_ref, wide_ref
+    kv_size, own_rows, tokens_ref, gain_ref, wq_ref, wk_ref, wv_ref, wg_ref, next_ref, previous_ref, own_ref, wide_ref
 ):
     columns = gain_ref.shape[1]
     weights_at, gain_at, rows_at, half = layout(columns, own_rows)
@@ -104,8 +105,6 @@
     gain = jnp.concatenate([gain_ref[...]] * (wq_ref.shape[1] // columns), axis=1)
     gain = jnp.broadcast_to(gain, (16, wq_ref.shape[1]))
     for out_ref, stops in ((next_ref, (1,)), (previous_ref, (-2, -1))):
-        out_ref[:columns, :columns] = wo_ref[:columns, :]
-        out_ref[:columns, columns:] = wo_ref[columns:, :]
         for j, weight_ref in enumerate((wq_ref, wk_ref, wv_ref, wg_ref)):
             out_ref[weights_at + j * columns : weights_at + (j + 1) * columns, :] = weight_ref[...]
         out_ref[gain_at:rows_at, :] = gain
@@ -114,7 +113,7 @@
             out_ref[rows_at + at * half : rows_at + (at + 1) * half, :] = rows
 
 
-def pack(tokens, gain, weights, w_out, kv_size, own_rows):
+def pack(tokens, gain, weights, kv_size, own_rows):
     columns = tokens.shape[1]
     _, _, rows_at, half = layout(columns, own_rows)
     wide = weights[0].shape[1]
@@ -124,7 +123,7 @@
 
     shapes = [((rows_at + stops * half, wide), BF16) for stops in (1, 2)] + [((2 * half, columns), F32)]
     scratch = [pltpu.VMEM(tokens.shape, F32)]
-    return kernel(body, [], [tokens, gain, *weights, w_out], shapes, scratch, in_near=False)
+    return kernel(body, [], [tokens, gain, *weights], shapes, scratch, in_near=False)
 
 
 def split(values, wide):
@@ -156,13 +155,8 @@
     down_ref,
     across_ref,
     kept_ref,
-    w_out_ref,
     sums_ref,
 ):
-    for at, packet_ref in enumerate((before_ref, own_ref, after_ref, after2_ref)):
-        for part in range(w_out_ref.shape[0] // columns):
-            piece = packet_ref[:columns, part * columns : (part + 1) * columns]
-            w_out_ref[part * columns : (part + 1) * columns, at * columns : (at + 1) * columns] = piece
     wide = own_ref.shape[1]
     weights_at, gain_at, rows_at, half = layout(columns, own_rows)
     shard_kv = lax.axis_index("kv")
@@ -219,7 +213,6 @@
     columns = own_rows_wide.shape[1]
     across = 4 * packets[0].shape[1] + LANES
     shapes = [((count, own_rows, across), BF16) for count in (2, 2, 1)] + [((3, own_rows, across), F32)]
-    shapes.append(((packets[0].shape[1], JUMP * columns), BF16))
 
     def body(*refs):
         project_body(kv_size, own_rows, columns, *refs)
@@ -252,51 +245,48 @@
     return kernel(body, [], [kept, up, down, across, carried], shapes)
 
 
-def deliver_body(rows_ref, weight_ref, out_ref):
-    out_ref[...] = jnp.dot(rows_ref[...], weight_ref[...], preferred_element_type=F32).astype(BF16)
-
-
-def deliver(rows, weight):
-    (partial,) = kernel(deliver_body, [], [rows, weight], [((rows.shape[0], weight.shape[1]), BF16)])
+def deliver_near_body(kv_size, weight_ref, left_ref, three_ref, right_ref, out_ref):
+    shard_kv = lax.axis_index("kv")
+    own_rows = out_ref.shape[1]
+    far_members = kv_size // NEAR_OUT
+    pieces = [left_ref[0], left_ref[1], left_ref[2], three_ref[0], three_ref[1], three_ref[2], right_ref[0], right_ref[1]]
+    for n, piece in enumerate(pieces):
+        product = jnp.dot(piece, weight_ref[...], preferred_element_type=F32)
+        for j in range(far_members):
+            owner = (shard_kv + n - 4 + NEAR_OUT * (j - 2) + kv_size) % kv_size
+            out_ref[owner] = product[j * own_rows : (j + 1) * own_rows].astype(BF16)
+
+
+def deliver_near(w_out, left, three, right, kv_size, own_rows):
+    def body(*refs):
+        deliver_near_body(kv_size, *refs)
+
+    shape = (kv_size, own_rows, w_out.shape[1])
+    (partial,) = kernel(body, [], [w_out, left, three, right], [(shape, BF16)])
     return partial
 
 
-def reduce_body(terms_ref, *out_refs):
-    columns = out_refs[0].shape[1]
-    for at, out_ref in enumerate(out_refs):
-        total = terms_ref[0, :, at * columns : (at + 1) * columns].astype(F32)
-        for member in range(1, terms_ref.shape[0]):
-            total = total + terms_ref[member, :, at * columns : (at + 1) * columns].astype(F32)
-        out_ref[...] = total.astype(BF16)
-
-
-def reduce_terms(terms):
-    _, rows, wide = terms.shape
-    return kernel(reduce_body, [], [terms], [((rows, wide // JUMP), BF16)] * JUMP)
-
-
-def spread_body(*refs):
+def reduce_all_body(terms_ref, out_ref):
+    total = terms_ref[0].astype(F32)
+    for member in range(1, terms_ref.shape[0]):
+        total = total + terms_ref[member].astype(F32)
+    for member in range(terms_ref.shape[0]):
+        out_ref[member] = total.astype(BF16)
+
+
+def reduce_all(terms):
+    (copies,) = kernel(reduce_all_body, [], [terms], [(terms.shape, BF16)])
+    return copies
+
+
+def stack_body(*refs):
     out_ref = refs[-1]
-    for at, piece_ref in enumerate(refs[:-1]):
-        for member in range(out_ref.shape[0]):
-            out_ref[member, at] = piece_ref[...]
-
-
-def spread(pieces, copies):
-    (out,) = kernel(spread_body, [], pieces, [((copies, len(pieces), *pieces[0].shape), BF16)])
-    return out
-
-
-def settle_body(blocks_ref, out_ref):
-    shard_kv = lax.axis_index("kv")
-    kv_size = blocks_ref.shape[0]
-    for n in range(kv_size):
-        owner = (shard_kv + n % JUMP + JUMP - WINDOW[-1]) % JUMP + n // JUMP * JUMP
-        out_ref[owner] = blocks_ref[n]
-
-
-def settle(blocks):
-    (out,) = kernel(settle_body, [], [blocks], [(blocks.shape, BF16)], out_near=False)
+    for at, ref in enumerate(refs[:-1]):
+        out_ref[at] = ref[...]
+
+
+def stacked(pieces):
+    (out,) = kernel(stack_body, [], pieces, [((len(pieces), *pieces[0].shape), BF16)])
     return out
 
 
@@ -382,16 +372,15 @@
             outputs = outputs + dots(queries, moved_keys[by]) * within[by] * back(corrections, by)
         scale = lax.rsqrt(dots(outputs, outputs) / depth + EPS)
         finished = (outputs * scale * out_gain * (gate * jax.nn.sigmoid(gate))).astype(BF16)
-        for copy in range(out_ref.shape[0] // rows):
-            out_ref[copy * rows : (copy + 1) * rows, first : first + depth] = finished
-
-
-def propose(decay_rate, out_gain, terms, carried, span_size, total_heads, model_width, copies):
+        out_ref[:, first : first + depth] = finished
+
+
+def propose(decay_rate, out_gain, terms, carried, span_size, total_heads, model_width):
     def body(*refs):
         propose_body(span_size, total_heads, model_width, *refs)
 
     wide = carried.shape[1] * carried.shape[2]
-    shape = (copies * terms[0].shape[1], wide)
+    shape = (terms[0].shape[1], wide)
     operands = [out_gain.reshape(1, -1), *terms, carried]
     (hidden,) = kernel(body, [decay_rate], operands, [(shape, BF16)])
     return hidden
@@ -423,7 +412,7 @@
     own_rows = seq_count * span_size
     model_width, total_heads = w_beta.shape
     weights = [w_query, w_key, w_value, w_gate]
-    to_next, to_previous, own_rows_wide = pack(tokens, norm_gain[None, :], weights, w_out, kv_size, own_rows)
+    to_next, to_previous, own_rows_wide = pack(tokens, norm_gain[None, :], weights, kv_size, own_rows)
     before = shift(to_next, kv_size, 1)
     after = shift(to_previous, kv_size, -1)
     after2 = shift(after[: to_next.shape[0]], kv_size, -1)
@@ -433,7 +422,7 @@
     carried = replay(state, prev_keys, prev_values, beta, logdecay, accepted)
     small_weights = jnp.concatenate([w_beta.T, w_decay.T], axis=0)
     packets = (to_next, before, after, after2)
-    up, down, across, kept, w_out_near = project(own_rows_wide, small_weights, packets, kv_size, own_rows)
+    up, down, across, kept = project(own_rows_wide, small_weights, packets, kv_size, own_rows)
     across = shift(across, kv_size, 2 * JUMP)
     up = shift(up, kv_size, JUMP)
     down = shift(down, kv_size, -JUMP)
@@ -441,19 +430,21 @@
     ahead = shift(ahead, kv_size, 2 * JUMP)
     behind = shift(behind, kv_size, -2 * JUMP)
     terms = (kept, up, down, ahead, behind)
-    members = kv_size // JUMP
-    hidden = propose(decay_rate, out_gain, terms, carried, span_size, total_heads, model_width, members)
-    groups = [list(range(first, kv_size, JUMP)) for first in range(JUMP)]
-    rows_all = lax.all_to_all(hidden, "kv", 0, 0, tiled=True, axis_index_groups=groups)
-    partial = deliver(rows_all, w_out_near)
+    hidden = propose(decay_rate, out_gain, terms, carried, span_size, total_heads, model_width)
+    below = shift(hidden, kv_size, NEAR_OUT)
+    above = shift(hidden, kv_size, -NEAR_OUT)
+    opposite = shift(below, kv_size, NEAR_OUT)
+    block = stacked([opposite, below, hidden, above]).reshape(4 * own_rows, -1)
+    left = shift(block, kv_size, 1)
+    right = shift(block, kv_size, -1)
+    three = stacked([left, block, right])
+    near_left = shift(three, kv_size, 3)
+    near_right = shift(three[:2], kv_size, -3)
+    partial = deliver_near(w_out, near_left, three, near_right, kv_size, own_rows)
+    partial = partial.reshape(kv_size * own_rows, -1)
     exchanged = lax.all_to_all(partial, "tp", 0, 0, tiled=True)
-    finished = reduce_terms(exchanged.reshape(tp_size, own_rows, -1))
-    landed = [
-        piece if offset == 0 else shift(piece, kv_size, offset) for offset, piece in zip(WINDOW, finished)
-    ][::-1]
-    copies = spread(landed, tp_size).reshape(kv_size * own_rows, -1)
-    mixed = lax.all_to_all(copies, "tp", 0, 0, tiled=True)
-    mixed = settle(mixed.reshape(kv_size, own_rows, -1)).reshape(kv_size * own_rows, -1)
+    copies = reduce_all(exchanged.reshape(tp_size, -1, exchanged.shape[1]))
+    mixed = lax.all_to_all(copies.reshape(exchanged.shape), "tp", 0, 0, tiled=True)
     return (mixed, carried)
 
 

time: 199 us -> 194 us (0.975)
  blocking collectives: 49.9 us -> 11.2 us
  starting transfers between devices: 92.4 us -> 118 us
  waiting for transfers between devices: 40.3 us -> 48.8 us
    all_to_all x1 -> x0, blocking collectives: 37.2 us -> none  [shards(): lax.all_to_all(hidden, 'kv', 0, 0, tiled=True, axis_index_groups=groups)]
    ppermute x11 -> x15, starting transfers between devices: 88.8 us -> 114 us  [shift(): lax.ppermute(table, 'kv', [(i, (i + by) % axis_size) for i in range(axis_...]
    ppermute x11 -> x15, waiting for transfers between devices: 34.7 us -> 43.2 us  [shift(): lax.ppermute(table, 'kv', [(i, (i + by) % axis_size) for i in range(axis_...]
  transfers between devices with their start and end apart: 12 -> 16, of which waited for: 8 -> 10; matrix products, arithmetic and copies ran while one was open for 1% -> 1% of each run, Pallas kernels for 2% -> 2%
where the time goes in v2:
time: 194 us; the launch traced here: 192 us
  starting transfers between devices  118 us (61%)
  waiting for transfers between devices  48.8 us (25%)
  blocking collectives  11.2 us (6%)
  Pallas kernels  9.08 us (5%)
  local copies, waits for them, and re-layouts  4.53 us (2%)
    ppermute x15, starting transfers between devices, shift(): lax.ppermute(table, 'kv', [(i, (i + by) % axis_size) for i in range(axis_...  114 us
    ppermute x15, waiting for transfers between devices, shift(): lax.ppermute(table, 'kv', [(i, (i + by) % axis_size) for i in range(axis_...  43.2 us
    all_to_all x1, blocking collectives, shards(): exchanged = lax.all_to_all(partial, 'tp', 0, 0, tiled=True)  11.2 us
    pallas_call x9, Pallas kernels, kernel(): pl.pallas_call(body, in_specs=[smem] * len(scalars) + [vmem] * len(arrays...  9.08 us
    all_to_all x1, waiting for transfers between devices, shards(): lax.all_to_all(copies.reshape(exchanged.shape), 'tp', 0, 0, tiled=True)  5.61 us
  transfers between devices with their start and end apart: 16, of which 10 were waited for; matrix products, arithmetic and copies ran while one was open for 1% of the time, Pallas kernels for 2%

profile of v2, /device:TPU:40, one launch (start us, length us, event | category | flops | bytes accessed | tf_op | source)
XLA Modules:
  0.0 192.2 jit_solution(8897419797504008484)
XLA Ops:
  0.6 1.2 shard_map.176
  1.8 45.3 %collective-permute-start.1 = (bf16[720,256]{1,0:T(8,128)(2,1)S(1)}, bf16[720,256]{1,0:T(8,128)(2,1)S(1)}, u32[]{:S(2)}, u32[]{:S(2)}) collective-permute-start(bf16[720,256]{1,0:T(8,128)(2,1)S(1)} %get-tuple-element.13), channel_id=1, source_target_pairs={{0,248},{8,0},{16,8},{24,16},{32,24},{40,32},{48,40},{56,48},{64,5... | collective-permute-start | bytes 1105928 | tf_op jit(solution)/shard_map/ppermute | solution.py:38
  47.2 2.1 %collective-permute-start = (bf16[624,256]{1,0:T(8,128)(2,1)S(1)}, bf16[624,256]{1,0:T(8,128)(2,1)S(1)}, u32[]{:S(2)}, u32[]{:S(2)}) collective-permute-start(bf16[624,256]{1,0:T(8,128)(2,1)S(1)} %get-tuple-element.12.refs_2_), channel_id=1, source_target_pairs={{0,8},{8,16},{16,24},{24,32},{32,40},{40,48},{48,56},{56,64},{64,7... | collective-permute-start | bytes 958472 | tf_op jit(solution)/shard_map/ppermute | solution.py:38
  49.2 5.8 %collective-permute-done.1.refs_4_ = bf16[720,256]{1,0:T(8,128)(2,1)S(1)} collective-permute-done((bf16[720,256]{1,0:T(8,128)(2,1)S(1)}, bf16[720,256]{1,0:T(8,128)(2,1)S(1)}, u32[]{:S(2)}, u32[]{:S(2)}) %collective-permute-start.1) | collective-permute-done | bytes 368672 | tf_op jit(solution)/shard_map/ppermute | solution.py:38
  55.1 5.6 %collective-permute-start.2 = (bf16[624,256]{1,0:T(8,128)(2,1)S(1)}, bf16[624,256]{1,0:T(8,128)(2,1)S(1)}, u32[]{:S(2)}, u32[]{:S(2)}) collective-permute-start(bf16[624,256]{1,0:T(8,128)(2,1)S(1)} %slice.8), channel_id=1, source_target_pairs={{0,248},{8,0},{16,8},{24,16},{32,24},{40,32},{48,40},{56,48},{64,5... | collective-permute-start | bytes 958472 | tf_op jit(solution)/shard_map/ppermute | solution.py:38
  60.7 5.9 %collective-permute-done.2.refs_5_ = bf16[624,256]{1,0:T(8,128)(2,1)S(1)} collective-permute-done((bf16[624,256]{1,0:T(8,128)(2,1)S(1)}, bf16[624,256]{1,0:T(8,128)(2,1)S(1)}, u32[]{:S(2)}, u32[]{:S(2)}) %collective-permute-start.2) | collective-permute-done | bytes 319520 | tf_op jit(solution)/shard_map/ppermute | solution.py:38
  66.7 0.7 shard_map.177
  67.4 2.0 %collective-permute-start.3 = (bf16[2,24,1152]{2,1,0:T(8,128)(2,1)S(1)}, bf16[2,24,1152]{2,1,0:T(8,128)(2,1)S(1)}, u32[]{:S(2)}, u32[]{:S(2)}) collective-permute-start(bf16[2,24,1152]{2,1,0:T(8,128)(2,1)S(1)} %get-tuple-element.15), channel_id=1, source_target_pairs={{0,32},{8,40},{16,48},{24,56},{32,64},{40,72},{48,80},{56,88},{64,... | collective-permute-start | bytes 331784 | tf_op jit(solution)/shard_map/ppermute | solution.py:38
  69.3 7.9 %collective-permute-start.4 = (bf16[2,24,1152]{2,1,0:T(8,128)(2,1)S(1)}, bf16[2,24,1152]{2,1,0:T(8,128)(2,1)S(1)}, u32[]{:S(2)}, u32[]{:S(2)}) collective-permute-start(bf16[2,24,1152]{2,1,0:T(8,128)(2,1)S(1)} %get-tuple-element.16), channel_id=1, source_target_pairs={{0,224},{8,232},{16,240},{24,248},{32,0},{40,8},{48,16},{56,24},{6... | collective-permute-start | bytes 331784 | tf_op jit(solution)/shard_map/ppermute | solution.py:38
  77.2 2.0 %collective-permute-start.5 = (bf16[1,24,1152]{2,1,0:T(8,128)(2,1)S(1)}, bf16[1,24,1152]{2,1,0:T(8,128)(2,1)S(1)}, u32[]{:S(2)}, u32[]{:S(2)}) collective-permute-start(bf16[1,24,1152]{2,1,0:T(8,128)(2,1)S(1)} %get-tuple-element.17), channel_id=1, source_target_pairs={{0,64},{8,72},{16,80},{24,88},{32,96},{40,104},{48,112},{56,120},{... | collective-permute-start | bytes 165896 | tf_op jit(solution)/shard_map/ppermute | solution.py:38
  80.8 1.2 copy-done
  82.0 4.0 %shard_map.178.refs_4_.refs_7_ = f32[8,2,128,128]{3,2,1,0:T(8,128)S(1)} custom-call(f32[48]{0:T(128)} %reshape.27.beta_ref, f32[48]{0:T(128)} %reshape.28.logdecay_ref, s32[8]{0:T(128)} %accepted_ref.1, bf16[8,3,2,128]{3,2,1,0:T(2,128)(2,1)S(1)} %copy-done.2, bf16[8,3,2,128]{3,2,1,0:T(2,128)(2,1)S(1)} %copy-done.3, f32[8,2,128,128]{3,2,1,0:T(8,128)S(1)} %copy-done), custom_call_target="tpu_custom_call" | custom-call | tf_op jit(solution)/shard_map/pallas_call | solution.py:28
  86.0 12.3 %collective-permute-done.5.refs_3_ = bf16[1,24,1152]{2,1,0:T(8,128)(2,1)S(1)} collective-permute-done((bf16[1,24,1152]{2,1,0:T(8,128)(2,1)S(1)}, bf16[1,24,1152]{2,1,0:T(8,128)(2,1)S(1)}, u32[]{:S(2)}, u32[]{:S(2)}) %collective-permute-start.5) | collective-permute-done | bytes 55328 | tf_op jit(solution)/shard_map/ppermute | solution.py:38
  98.5 1.9 %collective-permute-start.6 = (bf16[24,1152]{1,0:T(8,128)(2,1)S(1)}, bf16[24,1152]{1,0:T(8,128)(2,1)S(1)}, u32[]{:S(2)}, u32[]{:S(2)}) collective-permute-start(bf16[24,1152]{1,0:T(8,128)(2,1)S(1)} %get-tuple-element.18), channel_id=1, source_target_pairs={{0,64},{8,72},{16,80},{24,88},{32,96},{40,104},{48,112},{56,120},{... | collective-permute-start | bytes 165896 | tf_op jit(solution)/shard_map/ppermute | solution.py:38
  100.5 12.7 %collective-permute-start.7 = (bf16[24,1152]{1,0:T(8,128)(2,1)S(1)}, bf16[24,1152]{1,0:T(8,128)(2,1)S(1)}, u32[]{:S(2)}, u32[]{:S(2)}) collective-permute-start(bf16[24,1152]{1,0:T(8,128)(2,1)S(1)} %get-tuple-element.19), channel_id=1, source_target_pairs={{0,192},{8,200},{16,208},{24,216},{32,224},{40,232},{48,240},{56,2... | collective-permute-start | bytes 165896 | tf_op jit(solution)/shard_map/ppermute | solution.py:38
  113.2 2.5 %collective-permute-done.6.refs_5_ = bf16[24,1152]{1,0:T(8,128)(2,1)S(1)} collective-permute-done((bf16[24,1152]{1,0:T(8,128)(2,1)S(1)}, bf16[24,1152]{1,0:T(8,128)(2,1)S(1)}, u32[]{:S(2)}, u32[]{:S(2)}) %collective-permute-start.6) | collective-permute-done | bytes 55328 | tf_op jit(solution)/shard_map/ppermute | solution.py:38
  116.0 2.1 %shard_map.180.refs_2_ = bf16[24,256]{1,0:T(8,128)(2,1)S(1)} custom-call(f32[2]{0:T(128)} %refs_0_.4, bf16[1,128]{1,0:T(2,128)(2,1)S(1)} %bitcast.11, f32[3,24,1152]{2,1,0:T(8,128)S(1)} %get-tuple-element.14.refs_0_.refs_2_, bf16[2,24,1152]{2,1,0:T(8,128)(2,1)S(1)} %collective-permute-done.3.refs_1_.refs_3_, ...), custom_call_target="tpu_custom_call" | custom-call | tf_op jit(solution)/shard_map/pallas_call | solution.py:28
  118.1 2.0 %collective-permute-start.8 = (bf16[24,256]{1,0:T(8,128)(2,1)S(1)}, bf16[24,256]{1,0:T(8,128)(2,1)S(1)}, u32[]{:S(2)}, u32[]{:S(2)}) collective-permute-start(bf16[24,256]{1,0:T(8,128)(2,1)S(1)} %shard_map.180.refs_2_), channel_id=1, source_target_pairs={{0,64},{8,72},{16,80},{24,88},{32,96},{40,104},{48,112},{56,120},{... | collective-permute-start | bytes 36872 | tf_op jit(solution)/shard_map/ppermute | solution.py:38
  120.0 13.1 %collective-permute-start.10 = (bf16[24,256]{1,0:T(8,128)(2,1)S(1)}, bf16[24,256]{1,0:T(8,128)(2,1)S(1)}, u32[]{:S(2)}, u32[]{:S(2)}) collective-permute-start(bf16[24,256]{1,0:T(8,128)(2,1)S(1)} %shard_map.180.refs_2_), channel_id=1, source_target_pairs={{0,192},{8,200},{16,208},{24,216},{32,224},{40,232},{48,240},{56,2... | collective-permute-start | bytes 36872 | tf_op jit(solution)/shard_map/ppermute | solution.py:38
  133.1 3.4 %collective-permute-start.9 = (bf16[24,256]{1,0:T(8,128)(2,1)S(1)}, bf16[24,256]{1,0:T(8,128)(2,1)S(1)}, u32[]{:S(2)}, u32[]{:S(2)}) collective-permute-start(bf16[24,256]{1,0:T(8,128)(2,1)S(1)} %collective-permute-done.8.refs_1_), channel_id=1, source_target_pairs={{0,64},{8,72},{16,80},{24,88},{32,96},{40,104},{48,112},{56,120},{... | collective-permute-start | bytes 36872 | tf_op jit(solution)/shard_map/ppermute | solution.py:38
  136.6 10.9 %collective-permute-done.9.refs_0_ = bf16[24,256]{1,0:T(8,128)(2,1)S(1)} collective-permute-done((bf16[24,256]{1,0:T(8,128)(2,1)S(1)}, bf16[24,256]{1,0:T(8,128)(2,1)S(1)}, u32[]{:S(2)}, u32[]{:S(2)}) %collective-permute-start.9) | collective-permute-done | bytes 12320 | tf_op jit(solution)/shard_map/ppermute | solution.py:38
  147.5 1.9 %collective-permute-start.11 = (bf16[96,256]{1,0:T(8,128)(2,1)S(1)}, bf16[96,256]{1,0:T(8,128)(2,1)S(1)}, u32[]{:S(2)}, u32[]{:S(2)}) collective-permute-start(bf16[96,256]{1,0:T(8,128)(2,1)S(1)} %bitcast.8), channel_id=1, source_target_pairs={{0,8},{8,16},{16,24},{24,32},{32,40},{40,48},{48,56},{56,64},{64,7... | collective-permute-start | bytes 147464 | tf_op jit(solution)/shard_map/ppermute | solution.py:38
  149.4 5.2 %collective-permute-start.12 = (bf16[96,256]{1,0:T(8,128)(2,1)S(1)}, bf16[96,256]{1,0:T(8,128)(2,1)S(1)}, u32[]{:S(2)}, u32[]{:S(2)}) collective-permute-start(bf16[96,256]{1,0:T(8,128)(2,1)S(1)} %bitcast.9), channel_id=1, source_target_pairs={{0,248},{8,0},{16,8},{24,16},{32,24},{40,32},{48,40},{56,48},{64,5... | collective-permute-start | bytes 147464 | tf_op jit(solution)/shard_map/ppermute | solution.py:38
  154.7 1.6 collective-permute-done.12.refs_2_
  156.4 2.1 %collective-permute-start.13 = (bf16[3,96,256]{2,1,0:T(8,128)(2,1)S(1)}, bf16[3,96,256]{2,1,0:T(8,128)(2,1)S(1)}, u32[]{:S(2)}, u32[]{:S(2)}) collective-permute-start(bf16[3,96,256]{2,1,0:T(8,128)(2,1)S(1)} %shard_map.182.refs_2_), channel_id=1, source_target_pairs={{0,24},{8,32},{16,40},{24,48},{32,56},{40,64},{48,72},{56,80},{64,... | collective-permute-start | bytes 442376 | tf_op jit(solution)/shard_map/ppermute | solution.py:38
  158.5 7.0 %collective-permute-start.14 = (bf16[2,96,256]{2,1,0:T(8,128)(2,1)S(1)}, bf16[2,96,256]{2,1,0:T(8,128)(2,1)S(1)}, u32[]{:S(2)}, u32[]{:S(2)}) collective-permute-start(bf16[2,96,256]{2,1,0:T(8,128)(2,1)S(1)} %slice.9), channel_id=1, source_target_pairs={{0,232},{8,240},{16,248},{24,0},{32,8},{40,16},{48,24},{56,32},{64... | collective-permute-start | bytes 294920 | tf_op jit(solution)/shard_map/ppermute | solution.py:38
  165.4 3.7 %collective-permute-done.14.refs_3_ = bf16[2,96,256]{2,1,0:T(8,128)(2,1)S(1)} collective-permute-done((bf16[2,96,256]{2,1,0:T(8,128)(2,1)S(1)}, bf16[2,96,256]{2,1,0:T(8,128)(2,1)S(1)}, u32[]{:S(2)}, u32[]{:S(2)}) %collective-permute-start.14) | collective-permute-done | bytes 98336 | tf_op jit(solution)/shard_map/ppermute | solution.py:38
  169.4 11.2 %all_to_all.18.terms_ref = bf16[8,96,128]{2,1,0:T(8,128)(2,1)S(1)} all-to-all(bf16[8,96,128]{2,1,0:T(8,128)(2,1)S(1)} %bitcast.7), channel_id=1, replica_groups=mesh['grp'=2,'kv'=32,'tp'=8] {'tp'}, dimensions={0} | all-to-all | bytes 393216 | tf_op jit(solution)/shard_map/all_to_all | solution.py:445
  180.7 0.7 shard_map.184
  181.4 3.6 %all-to-all-start.1 = ((bf16[8,96,128]{2,1,0:T(8,128)(2,1)}), bf16[8,96,128]{2,1,0:T(8,128)(2,1)S(1)}, u32[]{:S(2)}, u32[]{:S(2)}) async-start(bf16[8,96,128]{2,1,0:T(8,128)(2,1)} %shard_map.184), calls=%async_computation.1 | async-start | bytes 393216 | tf_op jit(solution)/shard_map/all_to_all | solution.py:447
  185.0 1.0 copy.24
  186.0 5.6 %all-to-all-done.1 = bf16[8,96,128]{2,1,0:T(8,128)(2,1)S(1)} async-done(((bf16[8,96,128]{2,1,0:T(8,128)(2,1)}), bf16[8,96,128]{2,1,0:T(8,128)(2,1)S(1)}, u32[]{:S(2)}, u32[]{:S(2)}) %all-to-all-start.1) | async-done | bytes 196640 | tf_op jit(solution)/shard_map/all_to_all | solution.py:447
  (37 shorter events, 3.2 us)
Async XLA Ops:
  1.8 53.2 %collective-permute-start.1 = (bf16[720,256]{1,0:T(8,128)(2,1)S(1)}, bf16[720,256]{1,0:T(8,128)(2,1)S(1)}, u32[]{:S(2)}, u32[]{:S(2)}) collective-permute-start(bf16[720,256]{1,0:T(8,128)(2,1)S(1)} %get-tuple-element.13), channel_id=1, source_target_pairs={{0,248},{8,0},{16,8},{24,16},{32,24},{40,32},{48,40},{56,48},{64,5... | collective-permute-start | bytes 1105928 | tf_op jit(solution)/shard_map/ppermute | solution.py:38
  47.1 13.6 %copy-start.5 = (bf16[4096,16]{0,1:T(8,128)(2,1)S(1)}, bf16[4096,16]{0,1:T(8,128)(2,1)}, u32[]{:S(2)}) copy-start(bf16[4096,16]{0,1:T(8,128)(2,1)} %param.24) | copy-start | bytes 393220
  47.1 13.6 %copy-start.6 = (bf16[4096,16]{0,1:T(8,128)(2,1)S(1)}, bf16[4096,16]{0,1:T(8,128)(2,1)}, u32[]{:S(2)}) copy-start(bf16[4096,16]{0,1:T(8,128)(2,1)} %param.23) | copy-start | bytes 393220
  47.2 13.6 %collective-permute-start = (bf16[624,256]{1,0:T(8,128)(2,1)S(1)}, bf16[624,256]{1,0:T(8,128)(2,1)S(1)}, u32[]{:S(2)}, u32[]{:S(2)}) collective-permute-start(bf16[624,256]{1,0:T(8,128)(2,1)S(1)} %get-tuple-element.12.refs_2_), channel_id=1, source_target_pairs={{0,8},{8,16},{16,24},{24,32},{32,40},{40,48},{48,56},{56,64},{64,7... | collective-permute-start | bytes 958472 | tf_op jit(solution)/shard_map/ppermute | solution.py:38
  55.1 11.6 %collective-permute-start.2 = (bf16[624,256]{1,0:T(8,128)(2,1)S(1)}, bf16[624,256]{1,0:T(8,128)(2,1)S(1)}, u32[]{:S(2)}, u32[]{:S(2)}) collective-permute-start(bf16[624,256]{1,0:T(8,128)(2,1)S(1)} %slice.8), channel_id=1, source_target_pairs={{0,248},{8,0},{16,8},{24,16},{32,24},{40,32},{48,40},{56,48},{64,5... | collective-permute-start | bytes 958472 | tf_op jit(solution)/shard_map/ppermute | solution.py:38
  67.4 11.8 %copy-start.7 = (f32[8,3,2]{0,2,1:T(2,128)S(1)}, f32[8,3,2]{0,2,1:T(2,128)}, u32[]{:S(2)}) copy-start(f32[8,3,2]{0,2,1:T(2,128)} %param.31) | copy-start | bytes 580
  67.4 31.0 %collective-permute-start.3 = (bf16[2,24,1152]{2,1,0:T(8,128)(2,1)S(1)}, bf16[2,24,1152]{2,1,0:T(8,128)(2,1)S(1)}, u32[]{:S(2)}, u32[]{:S(2)}) collective-permute-start(bf16[2,24,1152]{2,1,0:T(8,128)(2,1)S(1)} %get-tuple-element.15), channel_id=1, source_target_pairs={{0,32},{8,40},{16,48},{24,56},{32,64},{40,72},{48,80},{56,88},{64,... | collective-permute-start | bytes 331784 | tf_op jit(solution)/shard_map/ppermute | solution.py:38
  69.3 29.0 %collective-permute-start.4 = (bf16[2,24,1152]{2,1,0:T(8,128)(2,1)S(1)}, bf16[2,24,1152]{2,1,0:T(8,128)(2,1)S(1)}, u32[]{:S(2)}, u32[]{:S(2)}) collective-permute-start(bf16[2,24,1152]{2,1,0:T(8,128)(2,1)S(1)} %get-tuple-element.16), channel_id=1, source_target_pairs={{0,224},{8,232},{16,240},{24,248},{32,0},{40,8},{48,16},{56,24},{6... | collective-permute-start | bytes 331784 | tf_op jit(solution)/shard_map/ppermute | solution.py:38
  77.2 21.2 %collective-permute-start.5 = (bf16[1,24,1152]{2,1,0:T(8,128)(2,1)S(1)}, bf16[1,24,1152]{2,1,0:T(8,128)(2,1)S(1)}, u32[]{:S(2)}, u32[]{:S(2)}) collective-permute-start(bf16[1,24,1152]{2,1,0:T(8,128)(2,1)S(1)} %get-tuple-element.17), channel_id=1, source_target_pairs={{0,64},{8,72},{16,80},{24,88},{32,96},{40,104},{48,112},{56,120},{... | collective-permute-start | bytes 165896 | tf_op jit(solution)/shard_map/ppermute | solution.py:38
  79.3 0.7 copy-start.8
  79.3 1.4 copy-start.3
  80.1 0.7 copy-start.2
  80.8 1.2 copy-start
  98.5 17.2 %collective-permute-start.6 = (bf16[24,1152]{1,0:T(8,128)(2,1)S(1)}, bf16[24,1152]{1,0:T(8,128)(2,1)S(1)}, u32[]{:S(2)}, u32[]{:S(2)}) collective-permute-start(bf16[24,1152]{1,0:T(8,128)(2,1)S(1)} %get-tuple-element.18), channel_id=1, source_target_pairs={{0,64},{8,72},{16,80},{24,88},{32,96},{40,104},{48,112},{56,120},{... | collective-permute-start | bytes 165896 | tf_op jit(solution)/shard_map/ppermute | solution.py:38
  100.5 15.5 %copy-start.4 = (bf16[128]{0:T(256)(128)(2,1)S(1)}, bf16[128]{0:T(256)(128)(2,1)}, u32[]{:S(2)}) copy-start(bf16[128]{0:T(256)(128)(2,1)} %param.26) | copy-start | bytes 772
  100.5 15.5 %collective-permute-start.7 = (bf16[24,1152]{1,0:T(8,128)(2,1)S(1)}, bf16[24,1152]{1,0:T(8,128)(2,1)S(1)}, u32[]{:S(2)}, u32[]{:S(2)}) collective-permute-start(bf16[24,1152]{1,0:T(8,128)(2,1)S(1)} %get-tuple-element.19), channel_id=1, source_target_pairs={{0,192},{8,200},{16,208},{24,216},{32,224},{40,232},{48,240},{56,2... | collective-permute-start | bytes 165896 | tf_op jit(solution)/shard_map/ppermute | solution.py:38
  118.1 15.1 %collective-permute-start.8 = (bf16[24,256]{1,0:T(8,128)(2,1)S(1)}, bf16[24,256]{1,0:T(8,128)(2,1)S(1)}, u32[]{:S(2)}, u32[]{:S(2)}) collective-permute-start(bf16[24,256]{1,0:T(8,128)(2,1)S(1)} %shard_map.180.refs_2_), channel_id=1, source_target_pairs={{0,64},{8,72},{16,80},{24,88},{32,96},{40,104},{48,112},{56,120},{... | collective-permute-start | bytes 36872 | tf_op jit(solution)/shard_map/ppermute | solution.py:38
  120.0 16.6 %collective-permute-start.10 = (bf16[24,256]{1,0:T(8,128)(2,1)S(1)}, bf16[24,256]{1,0:T(8,128)(2,1)S(1)}, u32[]{:S(2)}, u32[]{:S(2)}) collective-permute-start(bf16[24,256]{1,0:T(8,128)(2,1)S(1)} %shard_map.180.refs_2_), channel_id=1, source_target_pairs={{0,192},{8,200},{16,208},{24,216},{32,224},{40,232},{48,240},{56,2... | collective-permute-start | bytes 36872 | tf_op jit(solution)/shard_map/ppermute | solution.py:38
  133.1 14.3 %collective-permute-start.9 = (bf16[24,256]{1,0:T(8,128)(2,1)S(1)}, bf16[24,256]{1,0:T(8,128)(2,1)S(1)}, u32[]{:S(2)}, u32[]{:S(2)}) collective-permute-start(bf16[24,256]{1,0:T(8,128)(2,1)S(1)} %collective-permute-done.8.refs_1_), channel_id=1, source_target_pairs={{0,64},{8,72},{16,80},{24,88},{32,96},{40,104},{48,112},{56,120},{... | collective-permute-start | bytes 36872 | tf_op jit(solution)/shard_map/ppermute | solution.py:38
  147.5 7.2 %collective-permute-start.11 = (bf16[96,256]{1,0:T(8,128)(2,1)S(1)}, bf16[96,256]{1,0:T(8,128)(2,1)S(1)}, u32[]{:S(2)}, u32[]{:S(2)}) collective-permute-start(bf16[96,256]{1,0:T(8,128)(2,1)S(1)} %bitcast.8), channel_id=1, source_target_pairs={{0,8},{8,16},{16,24},{24,32},{32,40},{40,48},{48,56},{56,64},{64,7... | collective-permute-start | bytes 147464 | tf_op jit(solution)/shard_map/ppermute | solution.py:38
  149.4 6.9 %collective-permute-start.12 = (bf16[96,256]{1,0:T(8,128)(2,1)S(1)}, bf16[96,256]{1,0:T(8,128)(2,1)S(1)}, u32[]{:S(2)}, u32[]{:S(2)}) collective-permute-start(bf16[96,256]{1,0:T(8,128)(2,1)S(1)} %bitcast.9), channel_id=1, source_target_pairs={{0,248},{8,0},{16,8},{24,16},{32,24},{40,32},{48,40},{56,48},{64,5... | collective-permute-start | bytes 147464 | tf_op jit(solution)/shard_map/ppermute | solution.py:38
  156.3 12.8 %copy-start.1 = (bf16[256,128]{1,0:T(8,128)(2,1)S(1)}, bf16[256,128]{1,0:T(8,128)(2,1)}, u32[]{:S(2)}) copy-start(bf16[256,128]{1,0:T(8,128)(2,1)} %refs_0_.5) | copy-start | bytes 196612
  156.4 12.8 %collective-permute-start.13 = (bf16[3,96,256]{2,1,0:T(8,128)(2,1)S(1)}, bf16[3,96,256]{2,1,0:T(8,128)(2,1)S(1)}, u32[]{:S(2)}, u32[]{:S(2)}) collective-permute-start(bf16[3,96,256]{2,1,0:T(8,128)(2,1)S(1)} %shard_map.182.refs_2_), channel_id=1, source_target_pairs={{0,24},{8,32},{16,40},{24,48},{32,56},{40,64},{48,72},{56,80},{64,... | collective-permute-start | bytes 442376 | tf_op jit(solution)/shard_map/ppermute | solution.py:38
  158.5 10.7 %collective-permute-start.14 = (bf16[2,96,256]{2,1,0:T(8,128)(2,1)S(1)}, bf16[2,96,256]{2,1,0:T(8,128)(2,1)S(1)}, u32[]{:S(2)}, u32[]{:S(2)}) collective-permute-start(bf16[2,96,256]{2,1,0:T(8,128)(2,1)S(1)} %slice.9), channel_id=1, source_target_pairs={{0,232},{8,240},{16,248},{24,0},{32,8},{40,16},{48,24},{56,32},{64... | collective-permute-start | bytes 294920 | tf_op jit(solution)/shard_map/ppermute | solution.py:38
  181.4 10.2 %all-to-all-start.1 = ((bf16[8,96,128]{2,1,0:T(8,128)(2,1)}), bf16[8,96,128]{2,1,0:T(8,128)(2,1)S(1)}, u32[]{:S(2)}, u32[]{:S(2)}) async-start(bf16[8,96,128]{2,1,0:T(8,128)(2,1)} %shard_map.184), calls=%async_computation.1 | async-start | bytes 393216 | tf_op jit(solution)/shard_map/all_to_all | solution.py:447

commit v3 on v1

--- a/solution.py
+++ b/solution.py
@@ -252,12 +252,15 @@
     return kernel(body, [], [kept, up, down, across, carried], shapes)
 
 
-def deliver_body(rows_ref, weight_ref, out_ref):
-    out_ref[...] = jnp.dot(rows_ref[...], weight_ref[...], preferred_element_type=F32).astype(BF16)
-
-
-def deliver(rows, weight):
-    (partial,) = kernel(deliver_body, [], [rows, weight], [((rows.shape[0], weight.shape[1]), BF16)])
+def deliver_body(*refs):
+    *row_refs, weight_ref, out_ref = refs
+    rows = jnp.concatenate([ref[...].astype(F32) for ref in row_refs], axis=0).astype(BF16)
+    out_ref[...] = jnp.dot(rows, weight_ref[...], preferred_element_type=F32).astype(BF16)
+
+
+def deliver(pieces, weight):
+    shape = (sum(piece.shape[0] for piece in pieces), weight.shape[1])
+    (partial,) = kernel(deliver_body, [], [*pieces, weight], [(shape, BF16)])
     return partial
 
 
@@ -291,7 +294,7 @@
     shard_kv = lax.axis_index("kv")
     kv_size = blocks_ref.shape[0]
     for n in range(kv_size):
-        owner = (shard_kv + n % JUMP + JUMP - WINDOW[-1]) % JUMP + n // JUMP * JUMP
+        owner = (shard_kv + n + kv_size - WINDOW[-1] - kv_size // 2) % kv_size
         out_ref[owner] = blocks_ref[n]
 
 
@@ -442,10 +445,14 @@
     behind = shift(behind, kv_size, -2 * JUMP)
     terms = (kept, up, down, ahead, behind)
     members = kv_size // JUMP
-    hidden = propose(decay_rate, out_gain, terms, carried, span_size, total_heads, model_width, members)
-    groups = [list(range(first, kv_size, JUMP)) for first in range(JUMP)]
-    rows_all = lax.all_to_all(hidden, "kv", 0, 0, tiled=True, axis_index_groups=groups)
-    partial = deliver(rows_all, w_out_near)
+    hidden = propose(decay_rate, out_gain, terms, carried, span_size, total_heads, model_width, 1)
+    lower = [hidden]
+    upper = [hidden]
+    for step in range(members // 2):
+        lower.append(shift(lower[-1], kv_size, JUMP))
+        if step < members // 2 - 1:
+            upper.append(shift(upper[-1], kv_size, -JUMP))
+    partial = deliver([*lower[::-1], *upper[1:]], w_out_near)
     exchanged = lax.all_to_all(partial, "tp", 0, 0, tiled=True)
     finished = reduce_terms(exchanged.reshape(tp_size, own_rows, -1))
     landed = [

time: 199 us -> 196 us (0.985)
  blocking collectives: 49.9 us -> 11.2 us
  starting transfers between devices: 92.4 us -> 124 us
  waiting for transfers between devices: 40.3 us -> 44.5 us
    all_to_all x1 -> x0, blocking collectives: 37.2 us -> none  [shards(): lax.all_to_all(hidden, 'kv', 0, 0, tiled=True, axis_index_groups=groups)]
    ppermute x11 -> x18, starting transfers between devices: 88.8 us -> 120 us  [shift(): lax.ppermute(table, 'kv', [(i, (i + by) % axis_size) for i in range(axis_...]
    ppermute x11 -> x18, waiting for transfers between devices: 34.7 us -> 38.9 us  [shift(): lax.ppermute(table, 'kv', [(i, (i + by) % axis_size) for i in range(axis_...]
  transfers between devices with their start and end apart: 12 -> 19, of which waited for: 8 -> 8; matrix products, arithmetic and copies ran while one was open for 1% -> 1% of each run, Pallas kernels for 2% -> 2%
where the time goes in v3:
time: 196 us; the launch traced here: 195 us
  starting transfers between devices  124 us (63%)
  waiting for transfers between devices  44.5 us (23%)
  blocking collectives  11.2 us (6%)
  Pallas kernels  10.6 us (5%)
  local copies, waits for them, and re-layouts  3.84 us (2%)
    ppermute x18, starting transfers between devices, shift(): lax.ppermute(table, 'kv', [(i, (i + by) % axis_size) for i in range(axis_...  120 us
    ppermute x18, waiting for transfers between devices, shift(): lax.ppermute(table, 'kv', [(i, (i + by) % axis_size) for i in range(axis_...  38.9 us
    all_to_all x1, blocking collectives, shards(): exchanged = lax.all_to_all(partial, 'tp', 0, 0, tiled=True)  11.2 us
    pallas_call x9, Pallas kernels, kernel(): pl.pallas_call(body, in_specs=[smem] * len(scalars) + [vmem] * len(arrays...  10.6 us
    all_to_all x1, waiting for transfers between devices, shards(): mixed = lax.all_to_all(copies, 'tp', 0, 0, tiled=True)  5.61 us
  transfers between devices with their start and end apart: 19, of which 8 were waited for; matrix products, arithmetic and copies ran while one was open for 1% of the time, Pallas kernels for 2%

profile of v3, /device:TPU:40, one launch (start us, length us, event | category | flops | bytes accessed | tf_op | source)
XLA Modules:
  0.0 195.0 jit_solution(13397183862032127545)
XLA Ops:
  0.6 1.2 shard_map.176
  1.8 45.3 %collective-permute-start.1 = (bf16[848,256]{1,0:T(8,128)(2,1)S(1)}, bf16[848,256]{1,0:T(8,128)(2,1)S(1)}, u32[]{:S(2)}, u32[]{:S(2)}) collective-permute-start(bf16[848,256]{1,0:T(8,128)(2,1)S(1)} %get-tuple-element.18), channel_id=1, source_target_pairs={{0,248},{8,0},{16,8},{24,16},{32,24},{40,32},{48,40},{56,48},{64,5... | collective-permute-start | bytes 1302536 | tf_op jit(solution)/shard_map/ppermute | solution.py:37
  47.2 2.1 %collective-permute-start = (bf16[752,256]{1,0:T(8,128)(2,1)S(1)}, bf16[752,256]{1,0:T(8,128)(2,1)S(1)}, u32[]{:S(2)}, u32[]{:S(2)}) collective-permute-start(bf16[752,256]{1,0:T(8,128)(2,1)S(1)} %get-tuple-element.17.refs_2_), channel_id=1, source_target_pairs={{0,8},{8,16},{16,24},{24,32},{32,40},{40,48},{48,56},{56,64},{64,7... | collective-permute-start | bytes 1155080 | tf_op jit(solution)/shard_map/ppermute | solution.py:37
  49.3 7.2 %collective-permute-done.1.refs_4_ = bf16[848,256]{1,0:T(8,128)(2,1)S(1)} collective-permute-done((bf16[848,256]{1,0:T(8,128)(2,1)S(1)}, bf16[848,256]{1,0:T(8,128)(2,1)S(1)}, u32[]{:S(2)}, u32[]{:S(2)}) %collective-permute-start.1) | collective-permute-done | bytes 434208 | tf_op jit(solution)/shard_map/ppermute | solution.py:37
  56.5 5.6 %collective-permute-start.2 = (bf16[752,256]{1,0:T(8,128)(2,1)S(1)}, bf16[752,256]{1,0:T(8,128)(2,1)S(1)}, u32[]{:S(2)}, u32[]{:S(2)}) collective-permute-start(bf16[752,256]{1,0:T(8,128)(2,1)S(1)} %slice.4), channel_id=1, source_target_pairs={{0,248},{8,0},{16,8},{24,16},{32,24},{40,32},{48,40},{56,48},{64,5... | collective-permute-start | bytes 1155080 | tf_op jit(solution)/shard_map/ppermute | solution.py:37
  62.2 7.3 %collective-permute-done.2.refs_5_ = bf16[752,256]{1,0:T(8,128)(2,1)S(1)} collective-permute-done((bf16[752,256]{1,0:T(8,128)(2,1)S(1)}, bf16[752,256]{1,0:T(8,128)(2,1)S(1)}, u32[]{:S(2)}, u32[]{:S(2)}) %collective-permute-start.2) | collective-permute-done | bytes 385056 | tf_op jit(solution)/shard_map/ppermute | solution.py:37
  69.5 1.4 shard_map.177
  71.0 2.1 %collective-permute-start.3 = (bf16[2,24,1152]{2,1,0:T(8,128)(2,1)}, bf16[2,24,1152]{2,1,0:T(8,128)(2,1)S(1)}, u32[]{:S(2)}, u32[]{:S(2)}) collective-permute-start(bf16[2,24,1152]{2,1,0:T(8,128)(2,1)} %get-tuple-element.20), channel_id=1, source_target_pairs={{0,32},{8,40},{16,48},{24,56},{32,64},{40,72},{48,80},{56,88},{64,... | collective-permute-start | bytes 331784 | tf_op jit(solution)/shard_map/ppermute | solution.py:37
  73.0 7.9 %collective-permute-start.4 = (bf16[2,24,1152]{2,1,0:T(8,128)(2,1)}, bf16[2,24,1152]{2,1,0:T(8,128)(2,1)S(1)}, u32[]{:S(2)}, u32[]{:S(2)}) collective-permute-start(bf16[2,24,1152]{2,1,0:T(8,128)(2,1)} %get-tuple-element.21), channel_id=1, source_target_pairs={{0,224},{8,232},{16,240},{24,248},{32,0},{40,8},{48,16},{56,24},{6... | collective-permute-start | bytes 331784 | tf_op jit(solution)/shard_map/ppermute | solution.py:37
  80.9 2.0 %collective-permute-start.5 = (bf16[1,24,1152]{2,1,0:T(8,128)(2,1)}, bf16[1,24,1152]{2,1,0:T(8,128)(2,1)S(1)}, u32[]{:S(2)}, u32[]{:S(2)}) collective-permute-start(bf16[1,24,1152]{2,1,0:T(8,128)(2,1)} %get-tuple-element.22), channel_id=1, source_target_pairs={{0,64},{8,72},{16,80},{24,88},{32,96},{40,104},{48,112},{56,120},{... | collective-permute-start | bytes 165896 | tf_op jit(solution)/shard_map/ppermute | solution.py:37
  84.5 1.2 copy-done
  85.7 4.0 %shard_map.178.refs_4_.refs_7_ = f32[8,2,128,128]{3,2,1,0:T(8,128)S(1)} custom-call(f32[48]{0:T(128)} %reshape.29.beta_ref, f32[48]{0:T(128)} %reshape.30.logdecay_ref, s32[8]{0:T(128)} %accepted_ref.1, bf16[8,3,2,128]{3,2,1,0:T(2,128)(2,1)S(1)} %copy-done.1, bf16[8,3,2,128]{3,2,1,0:T(2,128)(2,1)S(1)} %copy-done.2, f32[8,2,128,128]{3,2,1,0:T(8,128)S(1)} %copy-done), custom_call_target="tpu_custom_call" | custom-call | tf_op jit(solution)/shard_map/pallas_call | solution.py:27
  89.7 12.5 %collective-permute-done.5.refs_3_ = bf16[1,24,1152]{2,1,0:T(8,128)(2,1)S(1)} collective-permute-done((bf16[1,24,1152]{2,1,0:T(8,128)(2,1)}, bf16[1,24,1152]{2,1,0:T(8,128)(2,1)S(1)}, u32[]{:S(2)}, u32[]{:S(2)}) %collective-permute-start.5) | collective-permute-done | bytes 55328 | tf_op jit(solution)/shard_map/ppermute | solution.py:37
  102.5 1.9 collective-permute-start.6
  104.4 12.7 %collective-permute-start.7 = (bf16[24,1152]{1,0:T(8,128)(2,1)S(1)}, bf16[24,1152]{1,0:T(8,128)(2,1)S(1)}, u32[]{:S(2)}, u32[]{:S(2)}) collective-permute-start(bf16[24,1152]{1,0:T(8,128)(2,1)S(1)} %get-tuple-element.24), channel_id=1, source_target_pairs={{0,192},{8,200},{16,208},{24,216},{32,224},{40,232},{48,240},{56,2... | collective-permute-start | bytes 165896 | tf_op jit(solution)/shard_map/ppermute | solution.py:37
  117.1 2.5 %collective-permute-done.6.refs_5_ = bf16[24,1152]{1,0:T(8,128)(2,1)S(1)} collective-permute-done((bf16[24,1152]{1,0:T(8,128)(2,1)S(1)}, bf16[24,1152]{1,0:T(8,128)(2,1)S(1)}, u32[]{:S(2)}, u32[]{:S(2)}) %collective-permute-start.6) | collective-permute-done | bytes 55328 | tf_op jit(solution)/shard_map/ppermute | solution.py:37
  119.9 2.1 %shard_map.180.refs_4_ = bf16[24,256]{1,0:T(8,128)(2,1)S(1)} custom-call(f32[2]{0:T(128)} %refs_0_.3, bf16[1,128]{1,0:T(2,128)(2,1)S(1)} %bitcast.10, f32[3,24,1152]{2,1,0:T(8,128)S(1)} %get-tuple-element.19.refs_0_.refs_2_, bf16[2,24,1152]{2,1,0:T(8,128)(2,1)S(1)} %collective-permute-done.3.refs_1_.refs_3_, ...), custom_call_target="tpu_custom_call" | custom-call | tf_op jit(solution)/shard_map/pallas_call | solution.py:27
  122.0 2.0 %collective-permute-start.8 = (bf16[24,256]{1,0:T(8,128)(2,1)S(1)}, bf16[24,256]{1,0:T(8,128)(2,1)S(1)}, u32[]{:S(2)}, u32[]{:S(2)}) collective-permute-start(bf16[24,256]{1,0:T(8,128)(2,1)S(1)} %shard_map.180.refs_4_), channel_id=1, source_target_pairs={{0,32},{8,40},{16,48},{24,56},{32,64},{40,72},{48,80},{56,88},{64,... | collective-permute-start | bytes 36872 | tf_op jit(solution)/shard_map/ppermute | solution.py:37
  124.0 7.9 %collective-permute-start.12 = (bf16[24,256]{1,0:T(8,128)(2,1)S(1)}, bf16[24,256]{1,0:T(8,128)(2,1)S(1)}, u32[]{:S(2)}, u32[]{:S(2)}) collective-permute-start(bf16[24,256]{1,0:T(8,128)(2,1)S(1)} %shard_map.180.refs_4_), channel_id=1, source_target_pairs={{0,224},{8,232},{16,240},{24,248},{32,0},{40,8},{48,16},{56,24},{6... | collective-permute-start | bytes 36872 | tf_op jit(solution)/shard_map/ppermute | solution.py:37
  131.8 2.0 %collective-permute-start.9 = (bf16[24,256]{1,0:T(8,128)(2,1)S(1)}, bf16[24,256]{1,0:T(8,128)(2,1)S(1)}, u32[]{:S(2)}, u32[]{:S(2)}) collective-permute-start(bf16[24,256]{1,0:T(8,128)(2,1)S(1)} %collective-permute-done.8.refs_3_), channel_id=1, source_target_pairs={{0,32},{8,40},{16,48},{24,56},{32,64},{40,72},{48,80},{56,88},{64,... | collective-permute-start | bytes 36872 | tf_op jit(solution)/shard_map/ppermute | solution.py:37
  133.8 7.9 %collective-permute-start.13 = (bf16[24,256]{1,0:T(8,128)(2,1)S(1)}, bf16[24,256]{1,0:T(8,128)(2,1)S(1)}, u32[]{:S(2)}, u32[]{:S(2)}) collective-permute-start(bf16[24,256]{1,0:T(8,128)(2,1)S(1)} %collective-permute-done.12.refs_5_), channel_id=1, source_target_pairs={{0,224},{8,232},{16,240},{24,248},{32,0},{40,8},{48,16},{56,24},{6... | collective-permute-start | bytes 36872 | tf_op jit(solution)/shard_map/ppermute | solution.py:37
  141.7 2.0 %collective-permute-start.10 = (bf16[24,256]{1,0:T(8,128)(2,1)S(1)}, bf16[24,256]{1,0:T(8,128)(2,1)S(1)}, u32[]{:S(2)}, u32[]{:S(2)}) collective-permute-start(bf16[24,256]{1,0:T(8,128)(2,1)S(1)} %collective-permute-done.9.refs_2_), channel_id=1, source_target_pairs={{0,32},{8,40},{16,48},{24,56},{32,64},{40,72},{48,80},{56,88},{64,... | collective-permute-start | bytes 36872 | tf_op jit(solution)/shard_map/ppermute | solution.py:37
  143.7 7.9 %collective-permute-start.14 = (bf16[24,256]{1,0:T(8,128)(2,1)S(1)}, bf16[24,256]{1,0:T(8,128)(2,1)S(1)}, u32[]{:S(2)}, u32[]{:S(2)}) collective-permute-start(bf16[24,256]{1,0:T(8,128)(2,1)S(1)} %collective-permute-done.13.refs_6_), channel_id=1, source_target_pairs={{0,224},{8,232},{16,240},{24,248},{32,0},{40,8},{48,16},{56,24},{6... | collective-permute-start | bytes 36872 | tf_op jit(solution)/shard_map/ppermute | solution.py:37
  151.5 2.0 %collective-permute-start.11 = (bf16[24,256]{1,0:T(8,128)(2,1)S(1)}, bf16[24,256]{1,0:T(8,128)(2,1)S(1)}, u32[]{:S(2)}, u32[]{:S(2)}) collective-permute-start(bf16[24,256]{1,0:T(8,128)(2,1)S(1)} %collective-permute-done.10.refs_1_), channel_id=1, source_target_pairs={{0,32},{8,40},{16,48},{24,56},{32,64},{40,72},{48,80},{56,88},{64,... | collective-permute-start | bytes 36872 | tf_op jit(solution)/shard_map/ppermute | solution.py:37
  153.5 7.6 %collective-permute-done.11.refs_0_ = bf16[24,256]{1,0:T(8,128)(2,1)S(1)} collective-permute-done((bf16[24,256]{1,0:T(8,128)(2,1)S(1)}, bf16[24,256]{1,0:T(8,128)(2,1)S(1)}, u32[]{:S(2)}, u32[]{:S(2)}) %collective-permute-start.11) | collective-permute-done | bytes 12320 | tf_op jit(solution)/shard_map/ppermute | solution.py:37
  161.3 11.2 %all_to_all.18.terms_ref = bf16[8,24,512]{2,1,0:T(8,128)(2,1)S(1)} all-to-all(bf16[8,24,512]{2,1,0:T(8,128)(2,1)S(1)} %bitcast.9), channel_id=1, replica_groups=mesh['grp'=2,'kv'=32,'tp'=8] {'tp'}, dimensions={0} | all-to-all | bytes 393216 | tf_op jit(solution)/shard_map/all_to_all | solution.py:456
  172.5 2.0 %collective-permute-start.15 = (bf16[24,128]{1,0:T(8,128)(2,1)S(1)}, bf16[24,128]{1,0:T(8,128)(2,1)S(1)}, u32[]{:S(2)}, u32[]{:S(2)}) collective-permute-start(bf16[24,128]{1,0:T(8,128)(2,1)S(1)} %get-tuple-element.26), channel_id=1, source_target_pairs={{0,16},{8,24},{16,32},{24,40},{32,48},{40,56},{48,64},{56,72},{64,... | collective-permute-start | bytes 18440 | tf_op jit(solution)/shard_map/ppermute | solution.py:37
  174.5 3.3 %collective-permute-start.16 = (bf16[24,128]{1,0:T(8,128)(2,1)S(1)}, bf16[24,128]{1,0:T(8,128)(2,1)S(1)}, u32[]{:S(2)}, u32[]{:S(2)}) collective-permute-start(bf16[24,128]{1,0:T(8,128)(2,1)S(1)} %get-tuple-element.27), channel_id=1, source_target_pairs={{0,8},{8,16},{16,24},{24,32},{32,40},{40,48},{48,56},{56,64},{64,7... | collective-permute-start | bytes 18440 | tf_op jit(solution)/shard_map/ppermute | solution.py:37
  177.8 4.1 %collective-permute-start.17 = (bf16[24,128]{1,0:T(8,128)(2,1)S(1)}, bf16[24,128]{1,0:T(8,128)(2,1)S(1)}, u32[]{:S(2)}, u32[]{:S(2)}) collective-permute-start(bf16[24,128]{1,0:T(8,128)(2,1)S(1)} %get-tuple-element.29), channel_id=1, source_target_pairs={{0,248},{8,0},{16,8},{24,16},{32,24},{40,32},{48,40},{56,48},{64,5... | collective-permute-start | bytes 18440 | tf_op jit(solution)/shard_map/ppermute | solution.py:37
  181.8 1.5 collective-permute-done.17.refs_3_
  184.0 3.6 %all-to-all-start.1 = ((bf16[8,96,128]{2,1,0:T(8,128)(2,1)}), bf16[8,96,128]{2,1,0:T(8,128)(2,1)S(1)}, u32[]{:S(2)}, u32[]{:S(2)}) async-start(bf16[8,96,128]{2,1,0:T(8,128)(2,1)} %bitcast.5), calls=%async_computation.1 | async-start | bytes 393216 | tf_op jit(solution)/shard_map/all_to_all | solution.py:462
  188.6 5.6 %all-to-all-done.1 = bf16[8,96,128]{2,1,0:T(8,128)(2,1)S(1)} async-done(((bf16[8,96,128]{2,1,0:T(8,128)(2,1)}), bf16[8,96,128]{2,1,0:T(8,128)(2,1)S(1)}, u32[]{:S(2)}, u32[]{:S(2)}) %all-to-all-start.1) | async-done | bytes 196640 | tf_op jit(solution)/shard_map/all_to_all | solution.py:462
  (39 shorter events, 4.9 us)
Async XLA Ops:
  1.8 54.6 %collective-permute-start.1 = (bf16[848,256]{1,0:T(8,128)(2,1)S(1)}, bf16[848,256]{1,0:T(8,128)(2,1)S(1)}, u32[]{:S(2)}, u32[]{:S(2)}) collective-permute-start(bf16[848,256]{1,0:T(8,128)(2,1)S(1)} %get-tuple-element.18), channel_id=1, source_target_pairs={{0,248},{8,0},{16,8},{24,16},{32,24},{40,32},{48,40},{56,48},{64,5... | collective-permute-start | bytes 1302536 | tf_op jit(solution)/shard_map/ppermute | solution.py:37
  47.2 15.0 %copy-start.4 = (bf16[4096,16]{0,1:T(8,128)(2,1)S(1)}, bf16[4096,16]{0,1:T(8,128)(2,1)}, u32[]{:S(2)}) copy-start(bf16[4096,16]{0,1:T(8,128)(2,1)} %param.24) | copy-start | bytes 393220
  47.2 15.0 %copy-start.5 = (bf16[4096,16]{0,1:T(8,128)(2,1)S(1)}, bf16[4096,16]{0,1:T(8,128)(2,1)}, u32[]{:S(2)}) copy-start(bf16[4096,16]{0,1:T(8,128)(2,1)} %param.23) | copy-start | bytes 393220
  47.2 15.0 %collective-permute-start = (bf16[752,256]{1,0:T(8,128)(2,1)S(1)}, bf16[752,256]{1,0:T(8,128)(2,1)S(1)}, u32[]{:S(2)}, u32[]{:S(2)}) collective-permute-start(bf16[752,256]{1,0:T(8,128)(2,1)S(1)} %get-tuple-element.17.refs_2_), channel_id=1, source_target_pairs={{0,8},{8,16},{16,24},{24,32},{32,40},{40,48},{48,56},{56,64},{64,7... | collective-permute-start | bytes 1155080 | tf_op jit(solution)/shard_map/ppermute | solution.py:37
  56.5 13.0 %collective-permute-start.2 = (bf16[752,256]{1,0:T(8,128)(2,1)S(1)}, bf16[752,256]{1,0:T(8,128)(2,1)S(1)}, u32[]{:S(2)}, u32[]{:S(2)}) collective-permute-start(bf16[752,256]{1,0:T(8,128)(2,1)S(1)} %slice.4), channel_id=1, source_target_pairs={{0,248},{8,0},{16,8},{24,16},{32,24},{40,32},{48,40},{56,48},{64,5... | collective-permute-start | bytes 1155080 | tf_op jit(solution)/shard_map/ppermute | solution.py:37
  71.0 11.9 %copy-start.6 = (f32[8,3,2]{0,2,1:T(2,128)S(1)}, f32[8,3,2]{0,2,1:T(2,128)}, u32[]{:S(2)}) copy-start(f32[8,3,2]{0,2,1:T(2,128)} %param.31) | copy-start | bytes 580
  71.0 31.3 %collective-permute-start.3 = (bf16[2,24,1152]{2,1,0:T(8,128)(2,1)}, bf16[2,24,1152]{2,1,0:T(8,128)(2,1)S(1)}, u32[]{:S(2)}, u32[]{:S(2)}) collective-permute-start(bf16[2,24,1152]{2,1,0:T(8,128)(2,1)} %get-tuple-element.20), channel_id=1, source_target_pairs={{0,32},{8,40},{16,48},{24,56},{32,64},{40,72},{48,80},{56,88},{64,... | collective-permute-start | bytes 331784 | tf_op jit(solution)/shard_map/ppermute | solution.py:37
  73.0 29.3 %collective-permute-start.4 = (bf16[2,24,1152]{2,1,0:T(8,128)(2,1)}, bf16[2,24,1152]{2,1,0:T(8,128)(2,1)S(1)}, u32[]{:S(2)}, u32[]{:S(2)}) collective-permute-start(bf16[2,24,1152]{2,1,0:T(8,128)(2,1)} %get-tuple-element.21), channel_id=1, source_target_pairs={{0,224},{8,232},{16,240},{24,248},{32,0},{40,8},{48,16},{56,24},{6... | collective-permute-start | bytes 331784 | tf_op jit(solution)/shard_map/ppermute | solution.py:37
  80.9 21.4 %collective-permute-start.5 = (bf16[1,24,1152]{2,1,0:T(8,128)(2,1)}, bf16[1,24,1152]{2,1,0:T(8,128)(2,1)S(1)}, u32[]{:S(2)}, u32[]{:S(2)}) collective-permute-start(bf16[1,24,1152]{2,1,0:T(8,128)(2,1)} %get-tuple-element.22), channel_id=1, source_target_pairs={{0,64},{8,72},{16,80},{24,88},{32,96},{40,104},{48,112},{56,120},{... | collective-permute-start | bytes 165896 | tf_op jit(solution)/shard_map/ppermute | solution.py:37
  82.9 1.6 copy-start.2
  83.0 0.7 copy-start.7
  83.8 0.7 copy-start.1
  84.5 1.2 copy-start
  102.5 17.1 %collective-permute-start.6 = (bf16[24,1152]{1,0:T(8,128)(2,1)S(1)}, bf16[24,1152]{1,0:T(8,128)(2,1)S(1)}, u32[]{:S(2)}, u32[]{:S(2)}) collective-permute-start(bf16[24,1152]{1,0:T(8,128)(2,1)S(1)} %get-tuple-element.23), channel_id=1, source_target_pairs={{0,64},{8,72},{16,80},{24,88},{32,96},{40,104},{48,112},{56,120},{... | collective-permute-start | bytes 165896 | tf_op jit(solution)/shard_map/ppermute | solution.py:37
  104.4 15.5 %copy-start.3 = (bf16[128]{0:T(256)(128)(2,1)S(1)}, bf16[128]{0:T(256)(128)(2,1)}, u32[]{:S(2)}) copy-start(bf16[128]{0:T(256)(128)(2,1)} %param.26) | copy-start | bytes 772
  104.4 15.5 %collective-permute-start.7 = (bf16[24,1152]{1,0:T(8,128)(2,1)S(1)}, bf16[24,1152]{1,0:T(8,128)(2,1)S(1)}, u32[]{:S(2)}, u32[]{:S(2)}) collective-permute-start(bf16[24,1152]{1,0:T(8,128)(2,1)S(1)} %get-tuple-element.24), channel_id=1, source_target_pairs={{0,192},{8,200},{16,208},{24,216},{32,224},{40,232},{48,240},{56,2... | collective-permute-start | bytes 165896 | tf_op jit(solution)/shard_map/ppermute | solution.py:37
  122.0 9.8 %collective-permute-start.8 = (bf16[24,256]{1,0:T(8,128)(2,1)S(1)}, bf16[24,256]{1,0:T(8,128)(2,1)S(1)}, u32[]{:S(2)}, u32[]{:S(2)}) collective-permute-start(bf16[24,256]{1,0:T(8,128)(2,1)S(1)} %shard_map.180.refs_4_), channel_id=1, source_target_pairs={{0,32},{8,40},{16,48},{24,56},{32,64},{40,72},{48,80},{56,88},{64,... | collective-permute-start | bytes 36872 | tf_op jit(solution)/shard_map/ppermute | solution.py:37
  124.0 9.8 %collective-permute-start.12 = (bf16[24,256]{1,0:T(8,128)(2,1)S(1)}, bf16[24,256]{1,0:T(8,128)(2,1)S(1)}, u32[]{:S(2)}, u32[]{:S(2)}) collective-permute-start(bf16[24,256]{1,0:T(8,128)(2,1)S(1)} %shard_map.180.refs_4_), channel_id=1, source_target_pairs={{0,224},{8,232},{16,240},{24,248},{32,0},{40,8},{48,16},{56,24},{6... | collective-permute-start | bytes 36872 | tf_op jit(solution)/shard_map/ppermute | solution.py:37
  131.8 9.8 %collective-permute-start.9 = (bf16[24,256]{1,0:T(8,128)(2,1)S(1)}, bf16[24,256]{1,0:T(8,128)(2,1)S(1)}, u32[]{:S(2)}, u32[]{:S(2)}) collective-permute-start(bf16[24,256]{1,0:T(8,128)(2,1)S(1)} %collective-permute-done.8.refs_3_), channel_id=1, source_target_pairs={{0,32},{8,40},{16,48},{24,56},{32,64},{40,72},{48,80},{56,88},{64,... | collective-permute-start | bytes 36872 | tf_op jit(solution)/shard_map/ppermute | solution.py:37
  133.8 9.8 %collective-permute-start.13 = (bf16[24,256]{1,0:T(8,128)(2,1)S(1)}, bf16[24,256]{1,0:T(8,128)(2,1)S(1)}, u32[]{:S(2)}, u32[]{:S(2)}) collective-permute-start(bf16[24,256]{1,0:T(8,128)(2,1)S(1)} %collective-permute-done.12.refs_5_), channel_id=1, source_target_pairs={{0,224},{8,232},{16,240},{24,248},{32,0},{40,8},{48,16},{56,24},{6... | collective-permute-start | bytes 36872 | tf_op jit(solution)/shard_map/ppermute | solution.py:37
  141.7 9.8 %collective-permute-start.10 = (bf16[24,256]{1,0:T(8,128)(2,1)S(1)}, bf16[24,256]{1,0:T(8,128)(2,1)S(1)}, u32[]{:S(2)}, u32[]{:S(2)}) collective-permute-start(bf16[24,256]{1,0:T(8,128)(2,1)S(1)} %collective-permute-done.9.refs_2_), channel_id=1, source_target_pairs={{0,32},{8,40},{16,48},{24,56},{32,64},{40,72},{48,80},{56,88},{64,... | collective-permute-start | bytes 36872 | tf_op jit(solution)/shard_map/ppermute | solution.py:37
  143.7 9.8 %collective-permute-start.14 = (bf16[24,256]{1,0:T(8,128)(2,1)S(1)}, bf16[24,256]{1,0:T(8,128)(2,1)S(1)}, u32[]{:S(2)}, u32[]{:S(2)}) collective-permute-start(bf16[24,256]{1,0:T(8,128)(2,1)S(1)} %collective-permute-done.13.refs_6_), channel_id=1, source_target_pairs={{0,224},{8,232},{16,240},{24,248},{32,0},{40,8},{48,16},{56,24},{6... | collective-permute-start | bytes 36872 | tf_op jit(solution)/shard_map/ppermute | solution.py:37
  151.5 9.5 %collective-permute-start.11 = (bf16[24,256]{1,0:T(8,128)(2,1)S(1)}, bf16[24,256]{1,0:T(8,128)(2,1)S(1)}, u32[]{:S(2)}, u32[]{:S(2)}) collective-permute-start(bf16[24,256]{1,0:T(8,128)(2,1)S(1)} %collective-permute-done.10.refs_1_), channel_id=1, source_target_pairs={{0,32},{8,40},{16,48},{24,56},{32,64},{40,72},{48,80},{56,88},{64,... | collective-permute-start | bytes 36872 | tf_op jit(solution)/shard_map/ppermute | solution.py:37
  172.5 9.3 %collective-permute-start.15 = (bf16[24,128]{1,0:T(8,128)(2,1)S(1)}, bf16[24,128]{1,0:T(8,128)(2,1)S(1)}, u32[]{:S(2)}, u32[]{:S(2)}) collective-permute-start(bf16[24,128]{1,0:T(8,128)(2,1)S(1)} %get-tuple-element.26), channel_id=1, source_target_pairs={{0,16},{8,24},{16,32},{24,40},{32,48},{40,56},{48,64},{56,72},{64,... | collective-permute-start | bytes 18440 | tf_op jit(solution)/shard_map/ppermute | solution.py:37
  174.5 7.4 %collective-permute-start.16 = (bf16[24,128]{1,0:T(8,128)(2,1)S(1)}, bf16[24,128]{1,0:T(8,128)(2,1)S(1)}, u32[]{:S(2)}, u32[]{:S(2)}) collective-permute-start(bf16[24,128]{1,0:T(8,128)(2,1)S(1)} %get-tuple-element.27), channel_id=1, source_target_pairs={{0,8},{8,16},{16,24},{24,32},{32,40},{40,48},{48,56},{56,64},{64,7... | collective-permute-start | bytes 18440 | tf_op jit(solution)/shard_map/ppermute | solution.py:37
  177.8 5.6 %collective-permute-start.17 = (bf16[24,128]{1,0:T(8,128)(2,1)S(1)}, bf16[24,128]{1,0:T(8,128)(2,1)S(1)}, u32[]{:S(2)}, u32[]{:S(2)}) collective-permute-start(bf16[24,128]{1,0:T(8,128)(2,1)S(1)} %get-tuple-element.29), channel_id=1, source_target_pairs={{0,248},{8,0},{16,8},{24,16},{32,24},{40,32},{48,40},{56,48},{64,5... | collective-permute-start | bytes 18440 | tf_op jit(solution)/shard_map/ppermute | solution.py:37
  184.0 10.2 %all-to-all-start.1 = ((bf16[8,96,128]{2,1,0:T(8,128)(2,1)}), bf16[8,96,128]{2,1,0:T(8,128)(2,1)S(1)}, u32[]{:S(2)}, u32[]{:S(2)}) async-start(bf16[8,96,128]{2,1,0:T(8,128)(2,1)} %bitcast.5), calls=%async_computation.1 | async-start | bytes 393216 | tf_op jit(solution)/shard_map/all_to_all | solution.py:462

commit v4 on v2

--- a/solution.py
+++ b/solution.py
@@ -9,7 +9,6 @@
 EPS = 1e-06
 WINDOW = (-1, 0, 1, 2)
 JUMP = len(WINDOW)
-NEAR_OUT = 8
 AHEAD = (0, JUMP, -JUMP, 2 * JUMP, -2 * JUMP, 3 * JUMP, -3 * JUMP, 4 * JUMP)
 LANES = 128
 HALF = LANES // 2
@@ -245,24 +244,12 @@
     return kernel(body, [], [kept, up, down, across, carried], shapes)
 
 
-def deliver_near_body(kv_size, weight_ref, left_ref, three_ref, right_ref, out_ref):
-    shard_kv = lax.axis_index("kv")
-    own_rows = out_ref.shape[1]
-    far_members = kv_size // NEAR_OUT
-    pieces = [left_ref[0], left_ref[1], left_ref[2], three_ref[0], three_ref[1], three_ref[2], right_ref[0], right_ref[1]]
-    for n, piece in enumerate(pieces):
-        product = jnp.dot(piece, weight_ref[...], preferred_element_type=F32)
-        for j in range(far_members):
-            owner = (shard_kv + n - 4 + NEAR_OUT * (j - 2) + kv_size) % kv_size
-            out_ref[owner] = product[j * own_rows : (j + 1) * own_rows].astype(BF16)
-
-
-def deliver_near(w_out, left, three, right, kv_size, own_rows):
-    def body(*refs):
-        deliver_near_body(kv_size, *refs)
-
-    shape = (kv_size, own_rows, w_out.shape[1])
-    (partial,) = kernel(body, [], [w_out, left, three, right], [(shape, BF16)])
+def deliver_body(rows_ref, weight_ref, out_ref):
+    out_ref[...] = jnp.dot(rows_ref[...], weight_ref[...], preferred_element_type=F32).astype(BF16)
+
+
+def deliver(rows, weight):
+    (partial,) = kernel(deliver_body, [], [rows, weight], [((rows.shape[0], weight.shape[1]), BF16)])
     return partial
 
 
@@ -277,17 +264,6 @@
 def reduce_all(terms):
     (copies,) = kernel(reduce_all_body, [], [terms], [(terms.shape, BF16)])
     return copies
-
-
-def stack_body(*refs):
-    out_ref = refs[-1]
-    for at, ref in enumerate(refs[:-1]):
-        out_ref[at] = ref[...]
-
-
-def stacked(pieces):
-    (out,) = kernel(stack_body, [], pieces, [((len(pieces), *pieces[0].shape), BF16)])
-    return out
 
 
 def propose_body(
@@ -431,17 +407,7 @@
     behind = shift(behind, kv_size, -2 * JUMP)
     terms = (kept, up, down, ahead, behind)
     hidden = propose(decay_rate, out_gain, terms, carried, span_size, total_heads, model_width)
-    below = shift(hidden, kv_size, NEAR_OUT)
-    above = shift(hidden, kv_size, -NEAR_OUT)
-    opposite = shift(below, kv_size, NEAR_OUT)
-    block = stacked([opposite, below, hidden, above]).reshape(4 * own_rows, -1)
-    left = shift(block, kv_size, 1)
-    right = shift(block, kv_size, -1)
-    three = stacked([left, block, right])
-    near_left = shift(three, kv_size, 3)
-    near_right = shift(three[:2], kv_size, -3)
-    partial = deliver_near(w_out, near_left, three, near_right, kv_size, own_rows)
-    partial = partial.reshape(kv_size * own_rows, -1)
+    partial = deliver(lax.all_gather(hidden, "kv", axis=0, tiled=True), w_out)
     exchanged = lax.all_to_all(partial, "tp", 0, 0, tiled=True)
     copies = reduce_all(exchanged.reshape(tp_size, -1, exchanged.shape[1]))
     mixed = lax.all_to_all(copies.reshape(exchanged.shape), "tp", 0, 0, tiled=True)

time: 194 us -> 199 us (1.026)
  blocking collectives: 11.2 us -> 68.5 us
  starting transfers between devices: 118 us -> 83 us
  waiting for transfers between devices: 48.8 us -> 32.2 us
    all_gather x0 -> x1, blocking collectives: none -> 57.3 us  [shards(): partial = deliver(lax.all_gather(hidden, 'kv', axis=0, tiled=True), w_out)]
    ppermute x15 -> x8, starting transfers between devices: 114 us -> 79.4 us  [shift(): lax.ppermute(table, 'kv', [(i, (i + by) % axis_size) for i in range(axis_...]
    ppermute x15 -> x8, waiting for transfers between devices: 43.2 us -> 26.6 us  [shift(): lax.ppermute(table, 'kv', [(i, (i + by) % axis_size) for i in range(axis_...]
    pallas_call x9 -> x7, Pallas kernels: 9.08 us -> 9.07 us  [kernel(): pl.pallas_call(body, in_specs=[smem] * len(scalars) + [vmem] * len(arrays...]
  transfers between devices with their start and end apart: 16 -> 9, of which waited for: 10 -> 5; matrix products, arithmetic and copies ran while one was open for 1% -> 1% of each run, Pallas kernels for 2% -> 2%
where the time goes in v4:
time: 199 us; the launch traced here: 198 us
  starting transfers between devices  83 us (42%)
  blocking collectives  68.5 us (34%)
  waiting for transfers between devices  32.2 us (16%)
  Pallas kernels  9.07 us (5%)
  local copies, waits for them, and re-layouts  4.52 us (2%)
    ppermute x8, starting transfers between devices, shift(): lax.ppermute(table, 'kv', [(i, (i + by) % axis_size) for i in range(axis_...  79.4 us
    all_gather x1, blocking collectives, shards(): partial = deliver(lax.all_gather(hidden, 'kv', axis=0, tiled=True), w_out)  57.3 us
    ppermute x8, waiting for transfers between devices, shift(): lax.ppermute(table, 'kv', [(i, (i + by) % axis_size) for i in range(axis_...  26.6 us
    all_to_all x1, blocking collectives, shards(): exchanged = lax.all_to_all(partial, 'tp', 0, 0, tiled=True)  11.2 us
    pallas_call x7, Pallas kernels, kernel(): pl.pallas_call(body, in_specs=[smem] * len(scalars) + [vmem] * len(arrays...  9.07 us
    all_to_all x1, waiting for transfers between devices, shards(): lax.all_to_all(copies.reshape(exchanged.shape), 'tp', 0, 0, tiled=True)  5.61 us
  transfers between devices with their start and end apart: 9, of which 5 were waited for; matrix products, arithmetic and copies ran while one was open for 1% of the time, Pallas kernels for 2%

profile of v4, /device:TPU:40, one launch (start us, length us, event | category | flops | bytes accessed | tf_op | source)
XLA Modules:
  0.0 198.2 jit_solution(5449248947635422970)
XLA Ops:
  0.6 1.2 shard_map.176
  1.8 45.3 %collective-permute-start.1 = (bf16[720,256]{1,0:T(8,128)(2,1)S(1)}, bf16[720,256]{1,0:T(8,128)(2,1)S(1)}, u32[]{:S(2)}, u32[]{:S(2)}) collective-permute-start(bf16[720,256]{1,0:T(8,128)(2,1)S(1)} %get-tuple-element.13), channel_id=1, source_target_pairs={{0,248},{8,0},{16,8},{24,16},{32,24},{40,32},{48,40},{56,48},{64,5... | collective-permute-start | bytes 1105928 | tf_op jit(solution)/shard_map/ppermute | solution.py:37
  47.2 2.1 %collective-permute-start = (bf16[624,256]{1,0:T(8,128)(2,1)S(1)}, bf16[624,256]{1,0:T(8,128)(2,1)S(1)}, u32[]{:S(2)}, u32[]{:S(2)}) collective-permute-start(bf16[624,256]{1,0:T(8,128)(2,1)S(1)} %get-tuple-element.12.refs_2_), channel_id=1, source_target_pairs={{0,8},{8,16},{16,24},{24,32},{32,40},{40,48},{48,56},{56,64},{64,7... | collective-permute-start | bytes 958472 | tf_op jit(solution)/shard_map/ppermute | solution.py:37
  49.2 5.8 %collective-permute-done.1.refs_4_ = bf16[720,256]{1,0:T(8,128)(2,1)S(1)} collective-permute-done((bf16[720,256]{1,0:T(8,128)(2,1)S(1)}, bf16[720,256]{1,0:T(8,128)(2,1)S(1)}, u32[]{:S(2)}, u32[]{:S(2)}) %collective-permute-start.1) | collective-permute-done | bytes 368672 | tf_op jit(solution)/shard_map/ppermute | solution.py:37
  55.1 5.6 %collective-permute-start.2 = (bf16[624,256]{1,0:T(8,128)(2,1)S(1)}, bf16[624,256]{1,0:T(8,128)(2,1)S(1)}, u32[]{:S(2)}, u32[]{:S(2)}) collective-permute-start(bf16[624,256]{1,0:T(8,128)(2,1)S(1)} %slice.4), channel_id=1, source_target_pairs={{0,248},{8,0},{16,8},{24,16},{32,24},{40,32},{48,40},{56,48},{64,5... | collective-permute-start | bytes 958472 | tf_op jit(solution)/shard_map/ppermute | solution.py:37
  60.7 5.9 %collective-permute-done.2.refs_5_ = bf16[624,256]{1,0:T(8,128)(2,1)S(1)} collective-permute-done((bf16[624,256]{1,0:T(8,128)(2,1)S(1)}, bf16[624,256]{1,0:T(8,128)(2,1)S(1)}, u32[]{:S(2)}, u32[]{:S(2)}) %collective-permute-start.2) | collective-permute-done | bytes 319520 | tf_op jit(solution)/shard_map/ppermute | solution.py:37
  66.7 0.7 shard_map.177
  67.4 2.0 collective-permute-start.3
  69.3 7.9 %collective-permute-start.4 = (bf16[2,24,1152]{2,1,0:T(8,128)(2,1)S(1)}, bf16[2,24,1152]{2,1,0:T(8,128)(2,1)S(1)}, u32[]{:S(2)}, u32[]{:S(2)}) collective-permute-start(bf16[2,24,1152]{2,1,0:T(8,128)(2,1)S(1)} %get-tuple-element.16), channel_id=1, source_target_pairs={{0,224},{8,232},{16,240},{24,248},{32,0},{40,8},{48,16},{56,24},{6... | collective-permute-start | bytes 331784 | tf_op jit(solution)/shard_map/ppermute | solution.py:37
  77.2 2.0 collective-permute-start.5
  79.2 0.1 copy.21
  79.3 0.6 reshape.22.beta_ref
  79.9 0.1 copy-done.8
  80.0 0.1 copy.22
  80.1 0.6 reshape.23.logdecay_ref
  80.7 0.1 copy-done.2
  80.8 1.2 copy-done
  82.0 4.0 %shard_map.178.refs_4_.refs_7_ = f32[8,2,128,128]{3,2,1,0:T(8,128)S(1)} custom-call(f32[48]{0:T(128)} %reshape.22.beta_ref, f32[48]{0:T(128)} %reshape.23.logdecay_ref, s32[8]{0:T(128)} %accepted_ref.1, bf16[8,3,2,128]{3,2,1,0:T(2,128)(2,1)S(1)} %copy-done.2, bf16[8,3,2,128]{3,2,1,0:T(2,128)(2,1)S(1)} %copy-done.3, f32[8,2,128,128]{3,2,1,0:T(8,128)S(1)} %copy-done), custom_call_target="tpu_custom_call" | custom-call | tf_op jit(solution)/shard_map/pallas_call | solution.py:27
  86.0 12.3 %collective-permute-done.5.refs_3_ = bf16[1,24,1152]{2,1,0:T(8,128)(2,1)S(1)} collective-permute-done((bf16[1,24,1152]{2,1,0:T(8,128)(2,1)S(1)}, bf16[1,24,1152]{2,1,0:T(8,128)(2,1)S(1)}, u32[]{:S(2)}, u32[]{:S(2)}) %collective-permute-start.5) | collective-permute-done | bytes 55328 | tf_op jit(solution)/shard_map/ppermute | solution.py:37
  98.4 0.2 shard_map.179
  98.5 1.9 collective-permute-start.6
  100.5 12.7 %collective-permute-start.7 = (bf16[24,1152]{1,0:T(8,128)(2,1)S(1)}, bf16[24,1152]{1,0:T(8,128)(2,1)S(1)}, u32[]{:S(2)}, u32[]{:S(2)}) collective-permute-start(bf16[24,1152]{1,0:T(8,128)(2,1)S(1)} %get-tuple-element.19), channel_id=1, source_target_pairs={{0,192},{8,200},{16,208},{24,216},{32,224},{40,232},{48,240},{56,2... | collective-permute-start | bytes 165896 | tf_op jit(solution)/shard_map/ppermute | solution.py:37
  113.2 2.5 %collective-permute-done.6.refs_5_ = bf16[24,1152]{1,0:T(8,128)(2,1)S(1)} collective-permute-done((bf16[24,1152]{1,0:T(8,128)(2,1)S(1)}, bf16[24,1152]{1,0:T(8,128)(2,1)S(1)}, u32[]{:S(2)}, u32[]{:S(2)}) %collective-permute-start.6) | collective-permute-done | bytes 55328 | tf_op jit(solution)/shard_map/ppermute | solution.py:37
  115.7 2.1 %shard_map.180 = bf16[24,256]{1,0:T(8,128)(2,1)S(1)} custom-call(f32[2]{0:T(128)} %refs_0_.3, bf16[1,128]{1,0:T(2,128)(2,1)S(1)} %bitcast.7, f32[3,24,1152]{2,1,0:T(8,128)S(1)} %get-tuple-element.14.refs_0_.refs_2_, bf16[2,24,1152]{2,1,0:T(8,128)(2,1)S(1)} %collective-permute-done.3.refs_1_.refs_3_, ...), custom_call_target="tpu_custom_call" | custom-call | tf_op jit(solution)/shard_map/pallas_call | solution.py:27
  117.8 57.3 %all_gather.3.rows_ref = bf16[768,256]{1,0:T(8,128)(2,1)S(1)} all-gather(bf16[24,256]{1,0:T(8,128)(2,1)S(1)} %shard_map.180), channel_id=1, replica_groups=mesh['grp'=2,'kv'=32,'tp'=8] {'kv'}, dimensions={0}, use_global_device_ids=true | all-gather | bytes 405504 | tf_op jit(solution)/shard_map/all_gather | solution.py:410
  175.1 0.3 shard_map.181
  175.4 11.2 %all_to_all.18.terms_ref = bf16[8,96,128]{2,1,0:T(8,128)(2,1)S(1)} all-to-all(bf16[8,96,128]{2,1,0:T(8,128)(2,1)S(1)} %bitcast.6), channel_id=1, replica_groups=mesh['grp'=2,'kv'=32,'tp'=8] {'tp'}, dimensions={0} | all-to-all | bytes 393216 | tf_op jit(solution)/shard_map/all_to_all | solution.py:411
  186.6 0.7 shard_map.182
  187.3 3.6 %all-to-all-start.1 = ((bf16[8,96,128]{2,1,0:T(8,128)(2,1)}), bf16[8,96,128]{2,1,0:T(8,128)(2,1)S(1)}, u32[]{:S(2)}, u32[]{:S(2)}) async-start(bf16[8,96,128]{2,1,0:T(8,128)(2,1)} %shard_map.182), calls=%async_computation.1 | async-start | bytes 393216 | tf_op jit(solution)/shard_map/all_to_all | solution.py:413
  190.9 1.0 copy.24
  191.9 5.6 %all-to-all-done.1 = bf16[8,96,128]{2,1,0:T(8,128)(2,1)S(1)} async-done(((bf16[8,96,128]{2,1,0:T(8,128)(2,1)}), bf16[8,96,128]{2,1,0:T(8,128)(2,1)S(1)}, u32[]{:S(2)}, u32[]{:S(2)}) %all-to-all-start.1) | async-done | bytes 196640 | tf_op jit(solution)/shard_map/all_to_all | solution.py:413
  197.5 0.7 copy.25
  (21 shorter events, 0.1 us)
Async XLA Ops:
  1.8 53.2 %collective-permute-start.1 = (bf16[720,256]{1,0:T(8,128)(2,1)S(1)}, bf16[720,256]{1,0:T(8,128)(2,1)S(1)}, u32[]{:S(2)}, u32[]{:S(2)}) collective-permute-start(bf16[720,256]{1,0:T(8,128)(2,1)S(1)} %get-tuple-element.13), channel_id=1, source_target_pairs={{0,248},{8,0},{16,8},{24,16},{32,24},{40,32},{48,40},{56,48},{64,5... | collective-permute-start | bytes 1105928 | tf_op jit(solution)/shard_map/ppermute | solution.py:37
  47.1 13.6 %copy-start.5 = (bf16[4096,16]{0,1:T(8,128)(2,1)S(1)}, bf16[4096,16]{0,1:T(8,128)(2,1)}, u32[]{:S(2)}) copy-start(bf16[4096,16]{0,1:T(8,128)(2,1)} %param.24) | copy-start | bytes 393220
  47.1 13.6 %copy-start.6 = (bf16[4096,16]{0,1:T(8,128)(2,1)S(1)}, bf16[4096,16]{0,1:T(8,128)(2,1)}, u32[]{:S(2)}) copy-start(bf16[4096,16]{0,1:T(8,128)(2,1)} %param.23) | copy-start | bytes 393220
  47.2 13.6 %collective-permute-start = (bf16[624,256]{1,0:T(8,128)(2,1)S(1)}, bf16[624,256]{1,0:T(8,128)(2,1)S(1)}, u32[]{:S(2)}, u32[]{:S(2)}) collective-permute-start(bf16[624,256]{1,0:T(8,128)(2,1)S(1)} %get-tuple-element.12.refs_2_), channel_id=1, source_target_pairs={{0,8},{8,16},{16,24},{24,32},{32,40},{40,48},{48,56},{56,64},{64,7... | collective-permute-start | bytes 958472 | tf_op jit(solution)/shard_map/ppermute | solution.py:37
  55.1 11.6 %collective-permute-start.2 = (bf16[624,256]{1,0:T(8,128)(2,1)S(1)}, bf16[624,256]{1,0:T(8,128)(2,1)S(1)}, u32[]{:S(2)}, u32[]{:S(2)}) collective-permute-start(bf16[624,256]{1,0:T(8,128)(2,1)S(1)} %slice.4), channel_id=1, source_target_pairs={{0,248},{8,0},{16,8},{24,16},{32,24},{40,32},{48,40},{56,48},{64,5... | collective-permute-start | bytes 958472 | tf_op jit(solution)/shard_map/ppermute | solution.py:37
  67.4 11.8 %copy-start.7 = (f32[8,3,2]{0,2,1:T(2,128)S(1)}, f32[8,3,2]{0,2,1:T(2,128)}, u32[]{:S(2)}) copy-start(f32[8,3,2]{0,2,1:T(2,128)} %param.31) | copy-start | bytes 580
  67.4 31.0 %collective-permute-start.3 = (bf16[2,24,1152]{2,1,0:T(8,128)(2,1)S(1)}, bf16[2,24,1152]{2,1,0:T(8,128)(2,1)S(1)}, u32[]{:S(2)}, u32[]{:S(2)}) collective-permute-start(bf16[2,24,1152]{2,1,0:T(8,128)(2,1)S(1)} %get-tuple-element.15), channel_id=1, source_target_pairs={{0,32},{8,40},{16,48},{24,56},{32,64},{40,72},{48,80},{56,88},{64,... | collective-permute-start | bytes 331784 | tf_op jit(solution)/shard_map/ppermute | solution.py:37
  69.3 29.0 %collective-permute-start.4 = (bf16[2,24,1152]{2,1,0:T(8,128)(2,1)S(1)}, bf16[2,24,1152]{2,1,0:T(8,128)(2,1)S(1)}, u32[]{:S(2)}, u32[]{:S(2)}) collective-permute-start(bf16[2,24,1152]{2,1,0:T(8,128)(2,1)S(1)} %get-tuple-element.16), channel_id=1, source_target_pairs={{0,224},{8,232},{16,240},{24,248},{32,0},{40,8},{48,16},{56,24},{6... | collective-permute-start | bytes 331784 | tf_op jit(solution)/shard_map/ppermute | solution.py:37
  77.2 21.2 %collective-permute-start.5 = (bf16[1,24,1152]{2,1,0:T(8,128)(2,1)S(1)}, bf16[1,24,1152]{2,1,0:T(8,128)(2,1)S(1)}, u32[]{:S(2)}, u32[]{:S(2)}) collective-permute-start(bf16[1,24,1152]{2,1,0:T(8,128)(2,1)S(1)} %get-tuple-element.17), channel_id=1, source_target_pairs={{0,64},{8,72},{16,80},{24,88},{32,96},{40,104},{48,112},{56,120},{... | collective-permute-start | bytes 165896 | tf_op jit(solution)/shard_map/ppermute | solution.py:37
  79.3 0.7 copy-start.8
  79.3 1.4 copy-start.3
  80.1 0.7 copy-start.2
  80.8 1.2 copy-start
  98.5 17.2 %collective-permute-start.6 = (bf16[24,1152]{1,0:T(8,128)(2,1)S(1)}, bf16[24,1152]{1,0:T(8,128)(2,1)S(1)}, u32[]{:S(2)}, u32[]{:S(2)}) collective-permute-start(bf16[24,1152]{1,0:T(8,128)(2,1)S(1)} %get-tuple-element.18), channel_id=1, source_target_pairs={{0,64},{8,72},{16,80},{24,88},{32,96},{40,104},{48,112},{56,120},{... | collective-permute-start | bytes 165896 | tf_op jit(solution)/shard_map/ppermute | solution.py:37
  100.5 15.2 %copy-start.4 = (bf16[128]{0:T(256)(128)(2,1)S(1)}, bf16[128]{0:T(256)(128)(2,1)}, u32[]{:S(2)}) copy-start(bf16[128]{0:T(256)(128)(2,1)} %param.26) | copy-start | bytes 772
  100.5 15.2 %collective-permute-start.7 = (bf16[24,1152]{1,0:T(8,128)(2,1)S(1)}, bf16[24,1152]{1,0:T(8,128)(2,1)S(1)}, u32[]{:S(2)}, u32[]{:S(2)}) collective-permute-start(bf16[24,1152]{1,0:T(8,128)(2,1)S(1)} %get-tuple-element.19), channel_id=1, source_target_pairs={{0,192},{8,200},{16,208},{24,216},{32,224},{40,232},{48,240},{56,2... | collective-permute-start | bytes 165896 | tf_op jit(solution)/shard_map/ppermute | solution.py:37
  117.8 57.3 %copy-start.1 = (bf16[256,128]{1,0:T(8,128)(2,1)S(1)}, bf16[256,128]{1,0:T(8,128)(2,1)}, u32[]{:S(2)}) copy-start(bf16[256,128]{1,0:T(8,128)(2,1)} %weight_ref.1) | copy-start | bytes 196612
  187.3 10.2 %all-to-all-start.1 = ((bf16[8,96,128]{2,1,0:T(8,128)(2,1)}), bf16[8,96,128]{2,1,0:T(8,128)(2,1)S(1)}, u32[]{:S(2)}, u32[]{:S(2)}) async-start(bf16[8,96,128]{2,1,0:T(8,128)(2,1)} %shard_map.182), calls=%async_computation.1 | async-start | bytes 393216 | tf_op jit(solution)/shard_map/all_to_all | solution.py:413

commit v5 on v2

--- a/solution.py
+++ b/solution.py
@@ -24,12 +24,13 @@
 def kernel(body, scalars, arrays, shapes, scratch=(), in_near=True, out_near=True):
     smem = pl.BlockSpec(memory_space=pltpu.SMEM)
     vmem = pl.BlockSpec(memory_space=pltpu.VMEM)
-    kind = pltpu.VMEM if out_near else jax.ShapeDtypeStruct
+    placed = out_near if isinstance(out_near, tuple) else (out_near,) * len(shapes)
+    kinds = [pltpu.VMEM if one else jax.ShapeDtypeStruct for one in placed]
     return pl.pallas_call(
         body,
         in_specs=[smem] * len(scalars) + [vmem] * len(arrays),
         out_specs=[vmem] * len(shapes),
-        out_shape=[kind(shape, dtype) for shape, dtype in shapes],
+        out_shape=[kind(shape, dtype) for kind, (shape, dtype) in zip(kinds, shapes)],
         scratch_shapes=list(scratch),
     )(*scalars, *[near_memory(array) if in_near else array for array in arrays])
 
@@ -38,7 +39,9 @@
     return lax.ppermute(table, "kv", [(i, (i + by) % axis_size) for i in range(axis_size)])
 
 
-def replay_body(beta_ref, logdecay_ref, accepted_ref, keys_ref, values_ref, state_ref, out_ref, rows_ref):
+def replay_body(
+    beta_ref, logdecay_ref, accepted_ref, keys_ref, values_ref, state_ref, near_ref, out_ref, rows_ref
+):
     seq_count, span_size, heads_here, depth = keys_ref.shape
     rows_ref[...] = jnp.zeros(rows_ref.shape, F32)
 
@@ -62,6 +65,7 @@
                 predicted = jnp.sum(column * state, axis=0, keepdims=True)
                 value = values_ref[seq, position].astype(F32)[head : head + 1]
                 state = state + column * (strength * (value - predicted))
+            near_ref[seq, head] = state
             out_ref[seq, head] = state
         return carry
 
@@ -72,8 +76,8 @@
     rows = -(-prev_keys.shape[1] * prev_keys.shape[2] // 8) * 8
     scratch = [pltpu.VMEM((rows, state.shape[-1]), F32)]
     scalars = [beta, logdecay, accepted]
-    (carried,) = kernel(replay_body, scalars, [prev_keys, prev_values, state], [(state.shape, F32)], scratch)
-    return carried
+    shapes = [(state.shape, F32)] * 2
+    return kernel(replay_body, scalars, [prev_keys, prev_values, state], shapes, scratch, out_near=(True, False))
 
 
 def rows_for(wide_ref, device, kv_size, own_rows):
@@ -419,7 +423,7 @@
 
     beta = prev_beta.reshape(-1)
     logdecay = prev_logdecay.reshape(-1)
-    carried = replay(state, prev_keys, prev_values, beta, logdecay, accepted)
+    carried, new_state = replay(state, prev_keys, prev_values, beta, logdecay, accepted)
     small_weights = jnp.concatenate([w_beta.T, w_decay.T], axis=0)
     packets = (to_next, before, after, after2)
     up, down, across, kept = project(own_rows_wide, small_weights, packets, kv_size, own_rows)
@@ -445,7 +449,7 @@
     exchanged = lax.all_to_all(partial, "tp", 0, 0, tiled=True)
     copies = reduce_all(exchanged.reshape(tp_size, -1, exchanged.shape[1]))
     mixed = lax.all_to_all(copies.reshape(exchanged.shape), "tp", 0, 0, tiled=True)
-    return (mixed, carried)
+    return (mixed, new_state)
 
 
 def solution(mesh):

time: 194 us -> 195 us (level)
  blocking collectives: 11.2 us -> 20.3 us
  waiting for transfers between devices: 48.8 us -> 44.6 us
  starting transfers between devices: 118 us -> 115 us
    all_to_all x0 -> x1, blocking collectives: none -> 9.28 us  [shards(): lax.all_to_all(copies.reshape(exchanged.shape), 'tp', 0, 0, tiled=True)]
    all_to_all x1 -> x0, waiting for transfers between devices: 5.61 us -> none  [shards(): lax.all_to_all(copies.reshape(exchanged.shape), 'tp', 0, 0, tiled=True)]
    all_to_all x1 -> x0, starting transfers between devices: 3.6 us -> none  [shards(): lax.all_to_all(copies.reshape(exchanged.shape), 'tp', 0, 0, tiled=True)]
  transfers between devices with their start and end apart: 16 -> 15, of which waited for: 10 -> 7; matrix products, arithmetic and copies ran while one was open for 1% -> 1% of each run, Pallas kernels for 2% -> 3%
where the time goes in v5:
time: 195 us; the launch traced here: 194 us
  starting transfers between devices  115 us (59%)
  waiting for transfers between devices  44.6 us (23%)
  blocking collectives  20.3 us (10%)
  Pallas kernels  9.44 us (5%)
  local copies, waits for them, and re-layouts  3.55 us (2%)
    ppermute x15, starting transfers between devices, shift(): lax.ppermute(table, 'kv', [(i, (i + by) % axis_size) for i in range(axis_...  115 us
    ppermute x15, waiting for transfers between devices, shift(): lax.ppermute(table, 'kv', [(i, (i + by) % axis_size) for i in range(axis_...  44.6 us
    all_to_all x1, blocking collectives, shards(): exchanged = lax.all_to_all(partial, 'tp', 0, 0, tiled=True)  11.1 us
    pallas_call x9, Pallas kernels, kernel(): pl.pallas_call(body, in_specs=[smem] * len(scalars) + [vmem] * len(arrays...  9.44 us
    all_to_all x1, blocking collectives, shards(): lax.all_to_all(copies.reshape(exchanged.shape), 'tp', 0, 0, tiled=True)  9.28 us
  transfers between devices with their start and end apart: 15, of which 7 were waited for; matrix products, arithmetic and copies ran while one was open for 1% of the time, Pallas kernels for 3%

profile of v5, /device:TPU:40, one launch (start us, length us, event | category | flops | bytes accessed | tf_op | source)
XLA Modules:
  0.0 194.4 jit_solution(6231786579059318974)
XLA Ops:
  0.6 1.2 shard_map.176
  1.8 45.3 %collective-permute-start.1 = (bf16[720,256]{1,0:T(8,128)(2,1)S(1)}, bf16[720,256]{1,0:T(8,128)(2,1)S(1)}, u32[]{:S(2)}, u32[]{:S(2)}) collective-permute-start(bf16[720,256]{1,0:T(8,128)(2,1)S(1)} %get-tuple-element.15), channel_id=1, source_target_pairs={{0,248},{8,0},{16,8},{24,16},{32,24},{40,32},{48,40},{56,48},{64,5... | collective-permute-start | bytes 1105928 | tf_op jit(solution)/shard_map/ppermute | solution.py:39
  47.2 2.1 %collective-permute-start = (bf16[624,256]{1,0:T(8,128)(2,1)S(1)}, bf16[624,256]{1,0:T(8,128)(2,1)S(1)}, u32[]{:S(2)}, u32[]{:S(2)}) collective-permute-start(bf16[624,256]{1,0:T(8,128)(2,1)S(1)} %get-tuple-element.14.refs_2_), channel_id=1, source_target_pairs={{0,8},{8,16},{16,24},{24,32},{32,40},{40,48},{48,56},{56,64},{64,7... | collective-permute-start | bytes 958472 | tf_op jit(solution)/shard_map/ppermute | solution.py:39
  49.2 5.8 %collective-permute-done.1.refs_4_ = bf16[720,256]{1,0:T(8,128)(2,1)S(1)} collective-permute-done((bf16[720,256]{1,0:T(8,128)(2,1)S(1)}, bf16[720,256]{1,0:T(8,128)(2,1)S(1)}, u32[]{:S(2)}, u32[]{:S(2)}) %collective-permute-start.1) | collective-permute-done | bytes 368672 | tf_op jit(solution)/shard_map/ppermute | solution.py:39
  55.1 5.6 %collective-permute-start.2 = (bf16[624,256]{1,0:T(8,128)(2,1)S(1)}, bf16[624,256]{1,0:T(8,128)(2,1)S(1)}, u32[]{:S(2)}, u32[]{:S(2)}) collective-permute-start(bf16[624,256]{1,0:T(8,128)(2,1)S(1)} %slice.8), channel_id=1, source_target_pairs={{0,248},{8,0},{16,8},{24,16},{32,24},{40,32},{48,40},{56,48},{64,5... | collective-permute-start | bytes 958472 | tf_op jit(solution)/shard_map/ppermute | solution.py:39
  60.7 5.9 %collective-permute-done.2.refs_5_ = bf16[624,256]{1,0:T(8,128)(2,1)S(1)} collective-permute-done((bf16[624,256]{1,0:T(8,128)(2,1)S(1)}, bf16[624,256]{1,0:T(8,128)(2,1)S(1)}, u32[]{:S(2)}, u32[]{:S(2)}) %collective-permute-start.2) | collective-permute-done | bytes 319520 | tf_op jit(solution)/shard_map/ppermute | solution.py:39
  66.7 0.7 shard_map.177
  67.4 2.0 %collective-permute-start.3 = (bf16[2,24,1152]{2,1,0:T(8,128)(2,1)S(1)}, bf16[2,24,1152]{2,1,0:T(8,128)(2,1)S(1)}, u32[]{:S(2)}, u32[]{:S(2)}) collective-permute-start(bf16[2,24,1152]{2,1,0:T(8,128)(2,1)S(1)} %get-tuple-element.17), channel_id=1, source_target_pairs={{0,32},{8,40},{16,48},{24,56},{32,64},{40,72},{48,80},{56,88},{64,... | collective-permute-start | bytes 331784 | tf_op jit(solution)/shard_map/ppermute | solution.py:39
  69.3 7.9 %collective-permute-start.4 = (bf16[2,24,1152]{2,1,0:T(8,128)(2,1)S(1)}, bf16[2,24,1152]{2,1,0:T(8,128)(2,1)S(1)}, u32[]{:S(2)}, u32[]{:S(2)}) collective-permute-start(bf16[2,24,1152]{2,1,0:T(8,128)(2,1)S(1)} %get-tuple-element.18), channel_id=1, source_target_pairs={{0,224},{8,232},{16,240},{24,248},{32,0},{40,8},{48,16},{56,24},{6... | collective-permute-start | bytes 331784 | tf_op jit(solution)/shard_map/ppermute | solution.py:39
  77.2 2.0 %collective-permute-start.5 = (bf16[1,24,1152]{2,1,0:T(8,128)(2,1)S(1)}, bf16[1,24,1152]{2,1,0:T(8,128)(2,1)S(1)}, u32[]{:S(2)}, u32[]{:S(2)}) collective-permute-start(bf16[1,24,1152]{2,1,0:T(8,128)(2,1)S(1)} %get-tuple-element.19), channel_id=1, source_target_pairs={{0,64},{8,72},{16,80},{24,88},{32,96},{40,104},{48,112},{56,120},{... | collective-permute-start | bytes 165896 | tf_op jit(solution)/shard_map/ppermute | solution.py:39
  79.3 0.6 reshape.27.beta_ref
  80.1 0.7 reshape.28.logdecay_ref
  80.8 1.2 copy-done
  82.0 5.1 %shard_map.178 = (f32[8,2,128,128]{3,2,1,0:T(8,128)S(1)}, f32[8,2,128,128]{3,2,1,0:T(8,128)}) custom-call(f32[48]{0:T(128)} %reshape.27.beta_ref, f32[48]{0:T(128)} %reshape.28.logdecay_ref, s32[8]{0:T(128)} %accepted_ref.1, bf16[8,3,2,128]{3,2,1,0:T(2,128)(2,1)S(1)} %copy-done.2, bf16[8,3,2,128]{3,2,1,0:T(2,128)(2,1)S(1)} %copy-done.3, ...), custom_call_target="tpu_custom_call" | custom-call | tf_op jit(solution)/shard_map/pallas_call | solution.py:29
  87.1 11.3 %collective-permute-done.5.refs_3_ = bf16[1,24,1152]{2,1,0:T(8,128)(2,1)S(1)} collective-permute-done((bf16[1,24,1152]{2,1,0:T(8,128)(2,1)S(1)}, bf16[1,24,1152]{2,1,0:T(8,128)(2,1)S(1)}, u32[]{:S(2)}, u32[]{:S(2)}) %collective-permute-start.5) | collective-permute-done | bytes 55328 | tf_op jit(solution)/shard_map/ppermute | solution.py:39
  98.5 1.9 collective-permute-start.6
  100.5 12.7 %collective-permute-start.7 = (bf16[24,1152]{1,0:T(8,128)(2,1)S(1)}, bf16[24,1152]{1,0:T(8,128)(2,1)S(1)}, u32[]{:S(2)}, u32[]{:S(2)}) collective-permute-start(bf16[24,1152]{1,0:T(8,128)(2,1)S(1)} %get-tuple-element.22), channel_id=1, source_target_pairs={{0,192},{8,200},{16,208},{24,216},{32,224},{40,232},{48,240},{56,2... | collective-permute-start | bytes 165896 | tf_op jit(solution)/shard_map/ppermute | solution.py:39
  113.2 2.6 %collective-permute-done.6.refs_5_ = bf16[24,1152]{1,0:T(8,128)(2,1)S(1)} collective-permute-done((bf16[24,1152]{1,0:T(8,128)(2,1)S(1)}, bf16[24,1152]{1,0:T(8,128)(2,1)S(1)}, u32[]{:S(2)}, u32[]{:S(2)}) %collective-permute-start.6) | collective-permute-done | bytes 55328 | tf_op jit(solution)/shard_map/ppermute | solution.py:39
  115.7 2.1 %shard_map.180.refs_2_ = bf16[24,256]{1,0:T(8,128)(2,1)S(1)} custom-call(f32[2]{0:T(128)} %refs_0_.4, bf16[1,128]{1,0:T(2,128)(2,1)S(1)} %bitcast.11, f32[3,24,1152]{2,1,0:T(8,128)S(1)} %get-tuple-element.16.refs_0_.refs_2_, bf16[2,24,1152]{2,1,0:T(8,128)(2,1)S(1)} %collective-permute-done.3.refs_1_.refs_3_, ...), custom_call_target="tpu_custom_call" | custom-call | tf_op jit(solution)/shard_map/pallas_call | solution.py:29
  117.8 2.0 %collective-permute-start.8 = (bf16[24,256]{1,0:T(8,128)(2,1)S(1)}, bf16[24,256]{1,0:T(8,128)(2,1)S(1)}, u32[]{:S(2)}, u32[]{:S(2)}) collective-permute-start(bf16[24,256]{1,0:T(8,128)(2,1)S(1)} %shard_map.180.refs_2_), channel_id=1, source_target_pairs={{0,64},{8,72},{16,80},{24,88},{32,96},{40,104},{48,112},{56,120},{... | collective-permute-start | bytes 36872 | tf_op jit(solution)/shard_map/ppermute | solution.py:39
  119.8 12.7 %collective-permute-start.10 = (bf16[24,256]{1,0:T(8,128)(2,1)S(1)}, bf16[24,256]{1,0:T(8,128)(2,1)S(1)}, u32[]{:S(2)}, u32[]{:S(2)}) collective-permute-start(bf16[24,256]{1,0:T(8,128)(2,1)S(1)} %shard_map.180.refs_2_), channel_id=1, source_target_pairs={{0,192},{8,200},{16,208},{24,216},{32,224},{40,232},{48,240},{56,2... | collective-permute-start | bytes 36872 | tf_op jit(solution)/shard_map/ppermute | solution.py:39
  132.5 4.8 %collective-permute-start.9 = (bf16[24,256]{1,0:T(8,128)(2,1)S(1)}, bf16[24,256]{1,0:T(8,128)(2,1)S(1)}, u32[]{:S(2)}, u32[]{:S(2)}) collective-permute-start(bf16[24,256]{1,0:T(8,128)(2,1)S(1)} %collective-permute-done.8.refs_1_), channel_id=1, source_target_pairs={{0,64},{8,72},{16,80},{24,88},{32,96},{40,104},{48,112},{56,120},{... | collective-permute-start | bytes 36872 | tf_op jit(solution)/shard_map/ppermute | solution.py:39
  137.3 9.5 %collective-permute-done.9.refs_0_ = bf16[24,256]{1,0:T(8,128)(2,1)S(1)} collective-permute-done((bf16[24,256]{1,0:T(8,128)(2,1)S(1)}, bf16[24,256]{1,0:T(8,128)(2,1)S(1)}, u32[]{:S(2)}, u32[]{:S(2)}) %collective-permute-start.9) | collective-permute-done | bytes 12320 | tf_op jit(solution)/shard_map/ppermute | solution.py:39
  146.8 5.7 %collective-permute-start.12 = (bf16[96,256]{1,0:T(8,128)(2,1)S(1)}, bf16[96,256]{1,0:T(8,128)(2,1)S(1)}, u32[]{:S(2)}, u32[]{:S(2)}) collective-permute-start(bf16[96,256]{1,0:T(8,128)(2,1)S(1)} %bitcast.8), channel_id=1, source_target_pairs={{0,248},{8,0},{16,8},{24,16},{32,24},{40,32},{48,40},{56,48},{64,5... | collective-permute-start | bytes 147464 | tf_op jit(solution)/shard_map/ppermute | solution.py:39
  152.5 2.0 %collective-permute-start.11 = (bf16[96,256]{1,0:T(8,128)(2,1)S(1)}, bf16[96,256]{1,0:T(8,128)(2,1)S(1)}, u32[]{:S(2)}, u32[]{:S(2)}) collective-permute-start(bf16[96,256]{1,0:T(8,128)(2,1)S(1)} %bitcast.9), channel_id=1, source_target_pairs={{0,8},{8,16},{16,24},{24,32},{32,40},{40,48},{48,56},{56,64},{64,7... | collective-permute-start | bytes 147464 | tf_op jit(solution)/shard_map/ppermute | solution.py:39
  154.4 5.3 %collective-permute-done.11.refs_0_ = bf16[96,256]{1,0:T(8,128)(2,1)S(1)} collective-permute-done((bf16[96,256]{1,0:T(8,128)(2,1)S(1)}, bf16[96,256]{1,0:T(8,128)(2,1)S(1)}, u32[]{:S(2)}, u32[]{:S(2)}) %collective-permute-start.11) | collective-permute-done | bytes 49184 | tf_op jit(solution)/shard_map/ppermute | solution.py:39
  159.7 2.1 %collective-permute-start.13 = (bf16[3,96,256]{2,1,0:T(8,128)(2,1)S(1)}, bf16[3,96,256]{2,1,0:T(8,128)(2,1)S(1)}, u32[]{:S(2)}, u32[]{:S(2)}) collective-permute-start(bf16[3,96,256]{2,1,0:T(8,128)(2,1)S(1)} %shard_map.182.refs_2_), channel_id=1, source_target_pairs={{0,24},{8,32},{16,40},{24,48},{32,56},{40,64},{48,72},{56,80},{64,... | collective-permute-start | bytes 442376 | tf_op jit(solution)/shard_map/ppermute | solution.py:39
  161.8 7.0 %collective-permute-start.14 = (bf16[2,96,256]{2,1,0:T(8,128)(2,1)S(1)}, bf16[2,96,256]{2,1,0:T(8,128)(2,1)S(1)}, u32[]{:S(2)}, u32[]{:S(2)}) collective-permute-start(bf16[2,96,256]{2,1,0:T(8,128)(2,1)S(1)} %slice.9), channel_id=1, source_target_pairs={{0,232},{8,240},{16,248},{24,0},{32,8},{40,16},{48,24},{56,32},{64... | collective-permute-start | bytes 294920 | tf_op jit(solution)/shard_map/ppermute | solution.py:39
  168.8 4.3 %collective-permute-done.14.refs_3_ = bf16[2,96,256]{2,1,0:T(8,128)(2,1)S(1)} collective-permute-done((bf16[2,96,256]{2,1,0:T(8,128)(2,1)S(1)}, bf16[2,96,256]{2,1,0:T(8,128)(2,1)S(1)}, u32[]{:S(2)}, u32[]{:S(2)}) %collective-permute-start.14) | collective-permute-done | bytes 98336 | tf_op jit(solution)/shard_map/ppermute | solution.py:39
  173.3 11.1 %all_to_all.18.terms_ref = bf16[8,96,128]{2,1,0:T(8,128)(2,1)S(1)} all-to-all(bf16[8,96,128]{2,1,0:T(8,128)(2,1)S(1)} %bitcast.7), channel_id=1, replica_groups=mesh['grp'=2,'kv'=32,'tp'=8] {'tp'}, dimensions={0} | all-to-all | bytes 393216 | tf_op jit(solution)/shard_map/all_to_all | solution.py:449
  184.4 9.3 %all_to_all.19 = bf16[8,96,128]{2,1,0:T(8,128)(2,1)S(1)} all-to-all(bf16[8,96,128]{2,1,0:T(8,128)(2,1)S(1)} %shard_map.184), channel_id=1, replica_groups=mesh['grp'=2,'kv'=32,'tp'=8] {'tp'}, dimensions={0} | all-to-all | bytes 393216 | tf_op jit(solution)/shard_map/all_to_all | solution.py:451
  193.7 0.7 copy.24
  (35 shorter events, 0.9 us)
Async XLA Ops:
  1.8 53.2 %collective-permute-start.1 = (bf16[720,256]{1,0:T(8,128)(2,1)S(1)}, bf16[720,256]{1,0:T(8,128)(2,1)S(1)}, u32[]{:S(2)}, u32[]{:S(2)}) collective-permute-start(bf16[720,256]{1,0:T(8,128)(2,1)S(1)} %get-tuple-element.15), channel_id=1, source_target_pairs={{0,248},{8,0},{16,8},{24,16},{32,24},{40,32},{48,40},{56,48},{64,5... | collective-permute-start | bytes 1105928 | tf_op jit(solution)/shard_map/ppermute | solution.py:39
  47.1 13.6 %copy-start.5 = (bf16[4096,16]{0,1:T(8,128)(2,1)S(1)}, bf16[4096,16]{0,1:T(8,128)(2,1)}, u32[]{:S(2)}) copy-start(bf16[4096,16]{0,1:T(8,128)(2,1)} %param.24) | copy-start | bytes 393220
  47.1 13.6 %copy-start.6 = (bf16[4096,16]{0,1:T(8,128)(2,1)S(1)}, bf16[4096,16]{0,1:T(8,128)(2,1)}, u32[]{:S(2)}) copy-start(bf16[4096,16]{0,1:T(8,128)(2,1)} %param.23) | copy-start | bytes 393220
  47.2 13.6 %collective-permute-start = (bf16[624,256]{1,0:T(8,128)(2,1)S(1)}, bf16[624,256]{1,0:T(8,128)(2,1)S(1)}, u32[]{:S(2)}, u32[]{:S(2)}) collective-permute-start(bf16[624,256]{1,0:T(8,128)(2,1)S(1)} %get-tuple-element.14.refs_2_), channel_id=1, source_target_pairs={{0,8},{8,16},{16,24},{24,32},{32,40},{40,48},{48,56},{56,64},{64,7... | collective-permute-start | bytes 958472 | tf_op jit(solution)/shard_map/ppermute | solution.py:39
  55.1 11.6 %collective-permute-start.2 = (bf16[624,256]{1,0:T(8,128)(2,1)S(1)}, bf16[624,256]{1,0:T(8,128)(2,1)S(1)}, u32[]{:S(2)}, u32[]{:S(2)}) collective-permute-start(bf16[624,256]{1,0:T(8,128)(2,1)S(1)} %slice.8), channel_id=1, source_target_pairs={{0,248},{8,0},{16,8},{24,16},{32,24},{40,32},{48,40},{56,48},{64,5... | collective-permute-start | bytes 958472 | tf_op jit(solution)/shard_map/ppermute | solution.py:39
  67.4 11.8 %copy-start.7 = (f32[8,3,2]{0,2,1:T(2,128)S(1)}, f32[8,3,2]{0,2,1:T(2,128)}, u32[]{:S(2)}) copy-start(f32[8,3,2]{0,2,1:T(2,128)} %param.31) | copy-start | bytes 580
  67.4 31.0 %collective-permute-start.3 = (bf16[2,24,1152]{2,1,0:T(8,128)(2,1)S(1)}, bf16[2,24,1152]{2,1,0:T(8,128)(2,1)S(1)}, u32[]{:S(2)}, u32[]{:S(2)}) collective-permute-start(bf16[2,24,1152]{2,1,0:T(8,128)(2,1)S(1)} %get-tuple-element.17), channel_id=1, source_target_pairs={{0,32},{8,40},{16,48},{24,56},{32,64},{40,72},{48,80},{56,88},{64,... | collective-permute-start | bytes 331784 | tf_op jit(solution)/shard_map/ppermute | solution.py:39
  69.3 29.0 %collective-permute-start.4 = (bf16[2,24,1152]{2,1,0:T(8,128)(2,1)S(1)}, bf16[2,24,1152]{2,1,0:T(8,128)(2,1)S(1)}, u32[]{:S(2)}, u32[]{:S(2)}) collective-permute-start(bf16[2,24,1152]{2,1,0:T(8,128)(2,1)S(1)} %get-tuple-element.18), channel_id=1, source_target_pairs={{0,224},{8,232},{16,240},{24,248},{32,0},{40,8},{48,16},{56,24},{6... | collective-permute-start | bytes 331784 | tf_op jit(solution)/shard_map/ppermute | solution.py:39
  77.2 21.2 %collective-permute-start.5 = (bf16[1,24,1152]{2,1,0:T(8,128)(2,1)S(1)}, bf16[1,24,1152]{2,1,0:T(8,128)(2,1)S(1)}, u32[]{:S(2)}, u32[]{:S(2)}) collective-permute-start(bf16[1,24,1152]{2,1,0:T(8,128)(2,1)S(1)} %get-tuple-element.19), channel_id=1, source_target_pairs={{0,64},{8,72},{16,80},{24,88},{32,96},{40,104},{48,112},{56,120},{... | collective-permute-start | bytes 165896 | tf_op jit(solution)/shard_map/ppermute | solution.py:39
  79.3 0.7 copy-start.8
  79.3 1.5 copy-start.3
  80.1 0.7 copy-start.2
  80.8 1.2 copy-start
  98.5 17.2 %collective-permute-start.6 = (bf16[24,1152]{1,0:T(8,128)(2,1)S(1)}, bf16[24,1152]{1,0:T(8,128)(2,1)S(1)}, u32[]{:S(2)}, u32[]{:S(2)}) collective-permute-start(bf16[24,1152]{1,0:T(8,128)(2,1)S(1)} %get-tuple-element.21), channel_id=1, source_target_pairs={{0,64},{8,72},{16,80},{24,88},{32,96},{40,104},{48,112},{56,120},{... | collective-permute-start | bytes 165896 | tf_op jit(solution)/shard_map/ppermute | solution.py:39
  100.5 15.2 %copy-start.4 = (bf16[128]{0:T(256)(128)(2,1)S(1)}, bf16[128]{0:T(256)(128)(2,1)}, u32[]{:S(2)}) copy-start(bf16[128]{0:T(256)(128)(2,1)} %param.26) | copy-start | bytes 772
  100.5 15.2 %collective-permute-start.7 = (bf16[24,1152]{1,0:T(8,128)(2,1)S(1)}, bf16[24,1152]{1,0:T(8,128)(2,1)S(1)}, u32[]{:S(2)}, u32[]{:S(2)}) collective-permute-start(bf16[24,1152]{1,0:T(8,128)(2,1)S(1)} %get-tuple-element.22), channel_id=1, source_target_pairs={{0,192},{8,200},{16,208},{24,216},{32,224},{40,232},{48,240},{56,2... | collective-permute-start | bytes 165896 | tf_op jit(solution)/shard_map/ppermute | solution.py:39
  117.8 14.6 %collective-permute-start.8 = (bf16[24,256]{1,0:T(8,128)(2,1)S(1)}, bf16[24,256]{1,0:T(8,128)(2,1)S(1)}, u32[]{:S(2)}, u32[]{:S(2)}) collective-permute-start(bf16[24,256]{1,0:T(8,128)(2,1)S(1)} %shard_map.180.refs_2_), channel_id=1, source_target_pairs={{0,64},{8,72},{16,80},{24,88},{32,96},{40,104},{48,112},{56,120},{... | collective-permute-start | bytes 36872 | tf_op jit(solution)/shard_map/ppermute | solution.py:39
  119.8 17.5 %collective-permute-start.10 = (bf16[24,256]{1,0:T(8,128)(2,1)S(1)}, bf16[24,256]{1,0:T(8,128)(2,1)S(1)}, u32[]{:S(2)}, u32[]{:S(2)}) collective-permute-start(bf16[24,256]{1,0:T(8,128)(2,1)S(1)} %shard_map.180.refs_2_), channel_id=1, source_target_pairs={{0,192},{8,200},{16,208},{24,216},{32,224},{40,232},{48,240},{56,2... | collective-permute-start | bytes 36872 | tf_op jit(solution)/shard_map/ppermute | solution.py:39
  132.5 14.3 %collective-permute-start.9 = (bf16[24,256]{1,0:T(8,128)(2,1)S(1)}, bf16[24,256]{1,0:T(8,128)(2,1)S(1)}, u32[]{:S(2)}, u32[]{:S(2)}) collective-permute-start(bf16[24,256]{1,0:T(8,128)(2,1)S(1)} %collective-permute-done.8.refs_1_), channel_id=1, source_target_pairs={{0,64},{8,72},{16,80},{24,88},{32,96},{40,104},{48,112},{56,120},{... | collective-permute-start | bytes 36872 | tf_op jit(solution)/shard_map/ppermute | solution.py:39
  146.8 7.6 %collective-permute-start.12 = (bf16[96,256]{1,0:T(8,128)(2,1)S(1)}, bf16[96,256]{1,0:T(8,128)(2,1)S(1)}, u32[]{:S(2)}, u32[]{:S(2)}) collective-permute-start(bf16[96,256]{1,0:T(8,128)(2,1)S(1)} %bitcast.8), channel_id=1, source_target_pairs={{0,248},{8,0},{16,8},{24,16},{32,24},{40,32},{48,40},{56,48},{64,5... | collective-permute-start | bytes 147464 | tf_op jit(solution)/shard_map/ppermute | solution.py:39
  152.5 7.2 %collective-permute-start.11 = (bf16[96,256]{1,0:T(8,128)(2,1)S(1)}, bf16[96,256]{1,0:T(8,128)(2,1)S(1)}, u32[]{:S(2)}, u32[]{:S(2)}) collective-permute-start(bf16[96,256]{1,0:T(8,128)(2,1)S(1)} %bitcast.9), channel_id=1, source_target_pairs={{0,8},{8,16},{16,24},{24,32},{32,40},{40,48},{48,56},{56,64},{64,7... | collective-permute-start | bytes 147464 | tf_op jit(solution)/shard_map/ppermute | solution.py:39
  159.7 13.3 %copy-start.1 = (bf16[256,128]{1,0:T(8,128)(2,1)S(1)}, bf16[256,128]{1,0:T(8,128)(2,1)}, u32[]{:S(2)}) copy-start(bf16[256,128]{1,0:T(8,128)(2,1)} %refs_0_.5) | copy-start | bytes 196612
  159.7 13.3 %collective-permute-start.13 = (bf16[3,96,256]{2,1,0:T(8,128)(2,1)S(1)}, bf16[3,96,256]{2,1,0:T(8,128)(2,1)S(1)}, u32[]{:S(2)}, u32[]{:S(2)}) collective-permute-start(bf16[3,96,256]{2,1,0:T(8,128)(2,1)S(1)} %shard_map.182.refs_2_), channel_id=1, source_target_pairs={{0,24},{8,32},{16,40},{24,48},{32,56},{40,64},{48,72},{56,80},{64,... | collective-permute-start | bytes 442376 | tf_op jit(solution)/shard_map/ppermute | solution.py:39
  161.8 11.2 %collective-permute-start.14 = (bf16[2,96,256]{2,1,0:T(8,128)(2,1)S(1)}, bf16[2,96,256]{2,1,0:T(8,128)(2,1)S(1)}, u32[]{:S(2)}, u32[]{:S(2)}) collective-permute-start(bf16[2,96,256]{2,1,0:T(8,128)(2,1)S(1)} %slice.9), channel_id=1, source_target_pairs={{0,232},{8,240},{16,248},{24,0},{32,8},{40,16},{48,24},{56,32},{64... | collective-permute-start | bytes 294920 | tf_op jit(solution)/shard_map/ppermute | solution.py:39
